TPU v7x, 128 devices: a whole 4x4x4 slice. The times are simulated.
128 devices in a mesh: sp: 16 (over z, y), dp: 8 (over x, core).
Axes of the slice: x: 4, y: 4, z: 4, core: 2. Of those that a mesh axis runs over, the one named last changes fastest.
Arguments:
- u_pre: bfloat16 [8, 16384, 2048], P('dp', 'sp'), may hold values from -6 to 6
- v_pre: bfloat16 [8, 16384, 2048], P('dp', 'sp'), may hold values from -6 to 6
- d_out: bfloat16 [8, 16384, 2048], P('dp', 'sp'), may hold values from -6 to 6
- w_mix: bfloat16 [16, 128, 128], replicated, may hold values from -0.5 to 0.5
- mix_bias: float32 [16, 128], replicated, may hold values from 0.1 to 1.9
- norm_gain: float32 [16, 128], replicated, may hold values from 0.1 to 1.9
- norm_shift: float32 [16, 128], replicated, may hold values from -3 to 3
- w_out: bfloat16 [2048, 2048], P('dp'), may hold values from -0.125 to 0.125
Outputs:
- grad_u: bfloat16 [8, 16384, 2048], P('dp', 'sp')
- grad_v: bfloat16 [8, 16384, 2048], P('dp', 'sp')
- grad_w_out: float32 [2048, 2048], P('dp')
- grad_w_mix: float32 [16, 128, 128], replicated
- grad_mix_bias: float32 [16, 128], replicated
- grad_gain: float32 [16, 128], replicated
- grad_shift: float32 [16, 128], replicated
All inputs are finite; a program needn't handle non-finite values.
Results may differ from a plain program's by a relative error of at most 0.012.
Values may be sent and summed in bfloat16 or wider, within the bound.
No kernel may reach another device: no remote copies, remote signals or barrier semaphores. Data moves between devices by JAX's collectives and lax.ppermute only.
A program may use at most 192 MiB of HBM per device.

v0:
```python
import jax
import jax.numpy as jnp
from jax import lax
from jax.sharding import PartitionSpec as P

EPS = 1e-05


def together(arrays, axis):
    ends = [0]
    for a in arrays:
        ends.append(ends[-1] + a.size)
    total = lax.psum(jnp.concatenate([a.ravel() for a in arrays]), axis)
    return tuple((total[b:e].reshape(a.shape) for a, b, e in zip(arrays, ends, ends[1:])))


def mechanism(grad_s, u_pre, v_pre, w_mix, mix_bias, gain, shift):
    items, length, width = grad_s.shape
    groups, span = (w_mix.shape[0], w_mix.shape[1])
    chans = width // groups
    shape = (items, length // span, span, groups, chans)
    u_val = u_pre.astype(jnp.float32).reshape(shape)
    v_val = v_pre.astype(jnp.float32).reshape(shape)
    cotan = grad_s.astype(jnp.float32).reshape(shape)
    upper, u_back = jax.vjp(jax.nn.gelu, u_val)
    gated, v_back = jax.vjp(jax.nn.gelu, v_val)
    centre = gated - jnp.mean(gated, axis=-1, keepdims=True)
    inverse = lax.rsqrt(jnp.mean(centre * centre, axis=-1, keepdims=True) + EPS)
    scaled = centre * inverse
    normed = (scaled * gain + shift).astype(jnp.bfloat16)
    lower = jnp.tril(jnp.ones((span, span), dtype=bool))
    w_low = jnp.where(lower[None], w_mix, jnp.zeros_like(w_mix))
    mixed = jnp.einsum("gts,insgc->intgc", w_low, normed, preferred_element_type=jnp.float32)
    mixed = mixed + jnp.transpose(mix_bias)[:, :, None]
    gated_out = (upper * mixed).astype(jnp.bfloat16)
    d_mixed = cotan * upper
    d_mixed_b = d_mixed.astype(jnp.bfloat16)
    grad_u = u_back(cotan * mixed)[0].astype(jnp.bfloat16).reshape(items, length, width)
    grad_bias = jnp.transpose(jnp.sum(d_mixed, axis=(0, 1, 4)))
    grad_w = jnp.einsum("intgc,insgc->gts", d_mixed_b, normed, preferred_element_type=jnp.float32)
    grad_w = jnp.where(lower[None], grad_w, jnp.zeros_like(grad_w))
    d_normed = jnp.einsum("gts,intgc->insgc", w_low, d_mixed_b, preferred_element_type=jnp.float32)
    grad_gain = jnp.sum(d_normed * scaled, axis=(0, 1, 2))
    grad_shift = jnp.sum(d_normed, axis=(0, 1, 2))
    d_scaled = d_normed * gain
    d_gated = inverse * (
        d_scaled
        - jnp.mean(d_scaled, axis=-1, keepdims=True)
        - scaled * jnp.mean(d_scaled * scaled, axis=-1, keepdims=True)
    )
    grad_v = v_back(d_gated)[0].astype(jnp.bfloat16).reshape(items, length, width)
    return (
        grad_u,
        grad_v,
        gated_out.reshape(items, length, width),
        grad_w,
        grad_bias,
        grad_gain,
        grad_shift,
    )


def on_device(u_pre, v_pre, d_out, w_mix, mix_bias, norm_gain, norm_shift, w_out):
    grad_s = lax.dot_general(
        d_out,
        lax.all_gather(w_out, "dp", axis=0, tiled=True),
        (((2,), (1,)), ((), ())),
        preferred_element_type=jnp.float32,
    ).astype(jnp.bfloat16)
    grad_u, grad_v, gated_out, grad_w, grad_bias, grad_gain, grad_shift = mechanism(
        grad_s, u_pre, v_pre, w_mix, mix_bias, norm_gain, norm_shift
    )
    grad_w, grad_bias, grad_gain, grad_shift = together(
        (grad_w, grad_bias, grad_gain, grad_shift), ("sp", "dp")
    )
    width = gated_out.shape[2]
    flat_d = d_out.reshape(-1, d_out.shape[2])
    flat_s = gated_out.reshape(-1, width)
    partial_rows = lax.psum_scatter(
        lax.dot_general(
            flat_s, flat_d, (((0,), (0,)), ((), ())), preferred_element_type=jnp.float32
        ),
        "dp",
        scatter_dimension=0,
        tiled=True,
    )
    grad_w_out = lax.psum(partial_rows, "sp")
    return (grad_u, grad_v, grad_w_out, grad_w, grad_bias, grad_gain, grad_shift)


def solution(mesh):
    return jax.shard_map(
        on_device,
        mesh=mesh,
        in_specs=(
            P("dp", "sp", None),
            P("dp", "sp", None),
            P("dp", "sp", None),
            P(),
            P(),
            P(),
            P(),
            P("dp", None),
        ),
        out_specs=(P("dp", "sp", None), P("dp", "sp", None), P("dp", None), P(), P(), P(), P()),
        check_vma=False,
    )
```

profile of v0, /device:TPU:0, one launch (start us, length us, event | category | flops | bytes accessed | tf_op | source)
XLA Modules:
  0.0 473.9 jit_solution(16673040196392679940)
XLA Ops:
  7.2 0.0 all-gather.2.cloned.1.call-start
  7.2 0.7 all-gather.2.cloned.1.call-update
  7.9 0.0 reduce-scatter.2.cloned.1.call-start
  7.9 3.2 convert_bitcast_fusion
  11.2 5.2 %copy.67 = f32[128,8,16,128]{3,2,1,0:T(8,128)} copy(f32[128,8,16,128]{3,1,2,0:T(8,128)S(1)} %convert_bitcast_fusion) | data formatting | bytes 16777216
  16.4 9.5 %copy.45 = f32[1,8,128,16,128]{2,4,1,3,0:T(8,128)} copy(f32[1,8,128,16,128]{4,3,0,2,1:T(8,128)} %bitcast.100) | data formatting | bytes 16777216 | tf_op jit(solution)/shard_map/reshape | solution.py:22
  25.9 3.2 convert_bitcast_fusion.1
  29.1 5.2 %copy.65 = f32[128,8,16,128]{3,2,1,0:T(8,128)} copy(f32[128,8,16,128]{3,1,2,0:T(8,128)S(1)} %convert_bitcast_fusion.1) | data formatting | bytes 16777216
  34.3 8.7 %copy.39 = f32[1,8,128,16,128]{2,4,1,3,0:T(8,128)} copy(f32[1,8,128,16,128]{4,3,0,2,1:T(8,128)} %bitcast.104) | data formatting | bytes 16777216 | tf_op jit(solution)/shard_map/reshape | solution.py:23
  43.0 0.0 copy-start.1
  43.1 0.0 copy-start.3
  43.1 0.0 copy-start.4
  43.1 5.9 %fusion.54 = f32[8,128,16]{1,0,2:T(8,128)S(1)} fusion(f32[1,8,128,16,128]{2,4,1,3,0:T(8,128)} %copy.39), kind=kLoop, calls=%fused_computation.83 | loop fusion | flops 18857984 | bytes 8454144 | tf_op jit(solution)/shard_map/reduce_sum | solution.py:27
  49.0 0.2 copy-done
  49.2 3.7 multiply_reduce_fusion.2
  53.0 0.0 copy-done.1
  53.0 0.0 copy-done.3
  53.0 0.0 copy-done.4
  53.0 6.5 %fusion.35 = bf16[8,128,16,128]{3,1,0,2:T(8,128)(2,1)} fusion(f32[8,128,16,128]{3,2,1,0:T(8,128)S(1)} %bitcast.105, f32[16,128]{1,0:T(8,128)S(1)} %copy-done.4, f32[16,128]{1,0:T(8,128)S(1)} %copy-done.3, f32[8,128,16]{1,0,2:T(8,128)S(1)} %add_rsqrt_fusion, f32[8,128,16]{1,0,2:T(8,128)S(1)} %broadcast_multiply_fusion.2), kind=kLoop, calls=%fused_computation.52 | loop fusion | flops 27262976 | bytes 12730368 | tf_op jit(solution)/shard_map/convert_element_type | solution.py:30
  59.5 2.4 all-gather.2.cloned.1.call-done
  61.8 12.7 %convert_bitcast_fusion.2 = f32[128,8,16,128]{3,1,2,0:T(8,128)S(1)} fusion(bf16[2048,2048]{1,0:T(8,128)(2,1)} %all-gather.2.cloned.1.call-done, bf16[1,1024,2048]{2,1,0:T(8,128)(2,1)} %param.10), kind=kOutput, calls=%fused_computation.51 | convolution fusion | flops 8594128896 | bytes 20971520 | tf_op jit(solution)/shard_map/dot_general | solution.py:64
  74.6 5.2 %copy.64 = f32[128,8,16,128]{3,2,1,0:T(8,128)} copy(f32[128,8,16,128]{3,1,2,0:T(8,128)S(1)} %convert_bitcast_fusion.2) | data formatting | bytes 16777216
  79.8 8.8 %copy.41 = f32[1,8,128,16,128]{2,4,1,3,0:T(8,128)} copy(f32[1,8,128,16,128]{4,3,2,1,0:T(8,128)} %bitcast.102) | data formatting | bytes 16777216 | tf_op jit(solution)/shard_map/reshape | solution.py:24
  88.5 0.0 copy-done.5
  88.5 14.8 %multiply_convert_fusion = (bf16[1,8,128,16,128]{2,4,1,3,0:T(8,128)(2,1)}, bf16[1,8,128,16,128]{2,4,1,3,0:T(8,128)(2,1)}, f32[128,16]{0,1:T(8,128)S(1)}) fusion(f32[128,16]{0,1:T(8,128)S(1)} %bitcast.112, f32[1,8,128,16,128]{2,4,1,3,0:T(8,128)} %copy.45, f32[1,8,128,16,128]{2,4,1,3,0:T(8,128)} %copy.41, bf16[8,128,16,128]{3,1,0,2:T(8,128)(2,1)} %fusion.35, ...), kind=kOutput, calls=%fused_computation.46 | convolution fusion | flops 593754112 | bytes 29917184 | tf_op jit(solution)/shard_map/gts,insgc->intgc/dot_general | solution.py:33
  103.3 6.8 %copy.58 = bf16[1,8,128,16,128]{4,3,2,1,0:T(8,128)(2,1)} copy(bf16[1,8,128,16,128]{2,4,1,3,0:T(8,128)(2,1)} %get-tuple-element.11) | data formatting | bytes 8388608 | tf_op jit(solution)/shard_map/convert_element_type | solution.py:35
  110.1 15.4 %fusion.37 = f32[2048,2048]{1,0:T(8,128)} fusion(bf16[128,8,16,128]{3,2,1,0:T(8,128)(2,1)} %bitcast.107, bf16[1,1024,2048]{2,1,0:T(8,128)(2,1)} %param.10), kind=kOutput, calls=%fused_computation.57 | convolution fusion | flops 8589934592 | bytes 25165824 | tf_op jit(solution)/shard_map/dot_general | solution.py:80
  125.5 0.0 reduce-scatter.2.cloned.1.call-update
  125.6 0.0 all-reduce.5.cloned.1.call-start
  125.6 0.0 copy-start.2
  125.6 10.2 %fusion.33 = bf16[8,128,16,128]{3,1,0,2:T(8,128)(2,1)S(1)} fusion(f32[8,128,16,128]{3,2,1,0:T(8,128)} %bitcast.103, f32[8,128,16,128]{3,2,1,0:T(8,128)} %bitcast.101), kind=kLoop, calls=%fused_computation.39 | loop fusion | flops 20971520 | bytes 20971520 | tf_op jit(solution)/shard_map/convert_element_type | solution.py:37
  135.8 1.3 fusion.45
  137.1 10.3 %fusion.34 = (f32[16,128]{1,0:T(8,128)S(1)}, f32[8,128,16]{1,0,2:T(8,128)S(1)}, f32[8,128,16]{1,0,2:T(8,128)S(1)}, f32[16,128]{1,0:T(8,128)S(1)}, f32[16,8,128,128]{3,2,1,0:T(8,128)}) fusion(f32[8,128,16]{1,0,2:T(8,128)S(1)} %add_rsqrt_fusion, f32[8,128,16]{1,0,2:T(8,128)S(1)} %broadcast_multiply_fusion.2, f32[1,8,128,16,128]{2,4,1,3,0:T(8,128)} %copy.39, ...), kind=kOutput, calls=%fused_computation.44 | convolution fusion | flops 572747776 | bytes 21798912 | tf_op jit(solution)/shard_map/gts,intgc->insgc/dot_general | solution.py:42
  147.4 1.0 pad_maximum_fusion
  148.5 0.0 all-reduce.5.cloned.1.call-update
  148.5 0.0 all-reduce.3.cloned.1.call-start
  148.6 7.0 %copy.47 = bf16[1,8,128,16,128]{4,3,2,1,0:T(8,128)(2,1)} copy(bf16[1,8,128,16,128]{2,4,1,3,0:T(8,128)(2,1)} %get-tuple-element.12) | data formatting | bytes 8388608 | tf_op jit(solution)/shard_map/convert_element_type | solution.py:38
  155.6 7.3 %reshape.497 = bf16[1,1024,2048]{2,1,0:T(8,128)(2,1)} reshape(bf16[1,8,128,16,128]{4,3,2,1,0:T(8,128)(2,1)} %copy.47) | data formatting | bytes 8388608 | tf_op jit(solution)/shard_map/reshape | solution.py:38
  162.9 54.8 %reduce-scatter.2.cloned.1.call-done = f32[256,2048]{1,0:T(8,128)} async-done(((f32[2048,2048]{1,0:T(8,128)}), f32[256,2048]{1,0:T(8,128)}) %reduce-scatter.2.cloned.1.call-update) | async-done | bytes 2097168 | tf_op jit(solution)/shard_map/reduce_scatter | solution.py:79
  217.7 0.0 all-reduce.3.cloned.1.call-update
  217.7 12.0 %fusion.6 = bf16[1,8,128,16,128]{2,4,1,3,0:T(8,128)(2,1)} fusion(f32[1,8,128,16,128]{2,4,1,3,0:T(8,128)} %copy.39, f32[16,8,128,128]{3,2,1,0:T(8,128)} %get-tuple-element.17, f32[8,128,16]{1,0,2:T(8,128)S(1)} %get-tuple-element.18, f32[8,128,16]{1,0,2:T(8,128)S(1)} %get-tuple-element.19, f32[16,128]{1,0:T(8,128)S(1)} %copy-done.3, ...), kind=kLoop, calls=%fused_computation.12 | loop fusion | flops 58720256 | bytes 21241856 | tf_op jit(solution)/shard_map/convert_element_type | solution.py:51
  229.8 6.7 %copy.56 = bf16[1,8,128,16,128]{4,3,2,1,0:T(8,128)(2,1)} copy(bf16[1,8,128,16,128]{2,4,1,3,0:T(8,128)(2,1)} %fusion.6) | data formatting | bytes 8388608 | tf_op jit(solution)/shard_map/convert_element_type | solution.py:51
  236.5 7.3 %reshape.500 = bf16[1,1024,2048]{2,1,0:T(8,128)(2,1)} reshape(bf16[1,8,128,16,128]{4,3,2,1,0:T(8,128)(2,1)} %copy.56) | data formatting | bytes 8388608 | tf_op jit(solution)/shard_map/reshape | solution.py:51
  243.8 127.2 %all-reduce.5.cloned.1.call-done = f32[268288]{0:T(1024)} async-done(((f32[268288]{0:T(1024)}), f32[268288]{0:T(1024)}) %all-reduce.5.cloned.1.call-update) | async-done | bytes 1073168 | tf_op jit(solution)/shard_map/psum | solution.py:13
  371.0 2.3 slice.49
  373.2 1.3 slice_bitcast_fusion
  374.6 89.4 %all-reduce.3.cloned.1.call-done = f32[256,2048]{1,0:T(8,128)} async-done(((f32[256,2048]{1,0:T(8,128)}), f32[256,2048]{1,0:T(8,128)}) %all-reduce.3.cloned.1.call-update) | async-done | bytes 2097168 | tf_op jit(solution)/shard_map/psum | solution.py:87
  464.0 3.1 copy.82
  (9 shorter events, 0.1 us)
Async XLA Ops:
  7.2 54.7 %all-gather.2.cloned.1.call-start = ((), (), s32[]{:S(2)}) async-start(), calls=%async_computation.1 | async-start | bytes 9437184 | tf_op jit(solution)/shard_map/all_gather | solution.py:66
  7.9 209.8 %reduce-scatter.2.cloned.1.call-start = ((), (), s32[]{:S(2)}) async-start(), calls=%async_computation.2 | async-start | bytes 18874368 | tf_op jit(solution)/shard_map/reduce_scatter | solution.py:79
  43.0 6.2 %copy-start = (f32[1,8,128,16,128]{2,4,1,3,0:T(8,128)S(1)}, f32[1,8,128,16,128]{2,4,1,3,0:T(8,128)}, u32[]{:S(2)}) copy-start(f32[1,8,128,16,128]{2,4,1,3,0:T(8,128)} %copy.39) | copy-start | bytes 25165828
  43.0 9.9 %copy-start.1 = (f32[128,8,16,128]{3,2,1,0:T(8,128)S(1)}, f32[128,8,16,128]{3,2,1,0:T(8,128)}, u32[]{:S(2)}) copy-start(f32[128,8,16,128]{3,2,1,0:T(8,128)} %copy.65) | copy-start | bytes 25165828
  43.1 9.9 %copy-start.3 = (f32[16,128]{1,0:T(8,128)S(1)}, f32[16,128]{1,0:T(8,128)}, u32[]{:S(2)}) copy-start(f32[16,128]{1,0:T(8,128)} %param.13) | copy-start | bytes 24580
  43.1 9.9 %copy-start.4 = (f32[16,128]{1,0:T(8,128)S(1)}, f32[16,128]{1,0:T(8,128)}, u32[]{:S(2)}) copy-start(f32[16,128]{1,0:T(8,128)} %param.14) | copy-start | bytes 24580
  79.7 8.8 %copy-start.5 = (bf16[16,128,128]{2,1,0:T(8,128)(2,1)S(1)}, bf16[16,128,128]{2,1,0:T(8,128)(2,1)}, u32[]{:S(2)}) copy-start(bf16[16,128,128]{2,1,0:T(8,128)(2,1)} %param.11) | copy-start | bytes 1572868
  79.8 8.8 %copy-start.6 = (f32[16,128]{1,0:T(8,128)S(1)}, f32[16,128]{1,0:T(8,128)}, u32[]{:S(2)}) copy-start(f32[16,128]{1,0:T(8,128)} %param.12) | copy-start | bytes 24580
  125.6 245.4 %all-reduce.5.cloned.1.call-start = ((), (), s32[]{:S(2)}) async-start(), calls=%async_computation.4 | async-start | bytes 2146304 | tf_op jit(solution)/shard_map/psum | solution.py:13
  125.6 10.2 %copy-start.2 = (bf16[8,128,16,128]{3,1,0,2:T(8,128)(2,1)S(1)}, bf16[8,128,16,128]{3,1,0,2:T(8,128)(2,1)}, u32[]{:S(2)}) copy-start(bf16[8,128,16,128]{3,1,0,2:T(8,128)(2,1)} %fusion.35) | copy-start | bytes 12582916
  148.5 315.5 %all-reduce.3.cloned.1.call-start = ((), (), s32[]{:S(2)}) async-start(), calls=%async_computation.3 | async-start | bytes 4194304 | tf_op jit(solution)/shard_map/psum | solution.py:87
Sparse Core Ops, SparseCore 0:
  9.7 52.0 all-gather.1
  125.7 91.9 reduce-scatter.1
  223.1 147.8 all-reduce.4
  374.2 89.7 all-reduce.2
where the time goes:
time: 478 us; the launch traced here: 474 us
  waiting for transfers between devices  274 us (57%)
  local copies, waits for them, and re-layouts  84.7 us (18%)
  matrix products  54.5 us (11%)
  other arithmetic  45.8 us (10%)
  between operations  14.2 us (3%)
    psum x1, waiting for transfers between devices, together(): total = lax.psum(jnp.concatenate([a.ravel() for a in arrays]), axis)  127 us
    psum x1, waiting for transfers between devices, on_device(): grad_w_out = lax.psum(partial_rows, 'sp')  89.4 us
    reduce_scatter x1, waiting for transfers between devices, on_device(): lax.psum_scatter(lax.dot_general(flat_s, flat_d, (((0,), (0,)), ((), ()))...  54.8 us
    unnamed x18, local copies, waits for them, and re-layouts  19 us
    dot_general x1, matrix products, on_device(): lax.dot_general(flat_s, flat_d, (((0,), (0,)), ((), ())), preferred_eleme...  15.4 us
    dot_general x1, matrix products, mechanism(): jnp.einsum('gts,insgc->intgc', w_low, normed, preferred_element_type=jnp....  14.8 us
    dot_general x1, matrix products, on_device(): lax.dot_general(d_out, lax.all_gather(w_out, 'dp', axis=0, tiled=True), (...  12.7 us
    convert_element_type x1, other arithmetic, mechanism(): v_back(d_gated)[0].astype(jnp.bfloat16).reshape(items, length, width)  12 us
  transfers between devices with their start and end apart: 4, of which 4 were waited for; matrix products, arithmetic and copies ran while one was open for 25% of the time, Pallas kernels for 0%

commit v1 on v0

v1 whole, which is shorter than its diff:
```python
import functools

import jax
import jax.numpy as jnp
from jax import lax
from jax.experimental import pallas as pl
from jax.experimental.pallas import tpu as pltpu
from jax.sharding import Mesh, PartitionSpec as P

EPS = 1e-05
C0 = 0.7978845608028654
C1 = C0 * 0.044715
F32 = jnp.float32
BF16 = jnp.bfloat16
BLK = 128
PAIR = 256
CHUNK = 24
ROOT = BLK**0.5


def tanh_of(a):
    a2 = a * a
    return jnp.tanh(a * (C0 + C1 * a2)), a2


def gelu(a):
    t, _ = tanh_of(a)
    return a * (0.5 + 0.5 * t)


def gelu_and_slope(a):
    t, a2 = tanh_of(a)
    half = 0.5 + 0.5 * t
    value = a * half
    return value, half + value * (1.0 - half) * (2.0 * C0 + (6.0 * C1) * a2)


def norm(gated):
    centre = gated - jnp.mean(gated, axis=-1, keepdims=True)
    inverse = lax.rsqrt(jnp.sum(centre * centre, axis=-1, keepdims=True) + BLK * EPS)
    return centre * inverse, inverse


def columns(ref, at, first=0, count=None):
    count = ref.shape[0] if count is None else count
    return jnp.concatenate([ref[first + k, at] for k in range(count)], axis=1)


def scatter_columns(src, dst, sem):
    @pl.loop(0, dst.shape[0])
    def _(k):
        at = pl.ds(pl.multiple_of(k * BLK, BLK), BLK)
        pltpu.make_async_copy(src.at[:, at], dst.at[k], sem).start()


def await_all(dst, sem):
    pltpu.make_async_copy(dst, dst, sem).wait()


def cols_of(g):
    return slice(g * BLK, (g + 1) * BLK)


def forward_kernel(
    order, u_ref, v_ref, d_hbm, w_ref, bias_ref, gain_ref, shift_ref, out_ref, d_ref, go_ref, bias_at, sem
):
    blocks, length, _ = d_ref.shape
    turns = length // PAIR
    step = pl.program_id(0)
    last = pl.num_programs(0) - 1
    now, before = lax.rem(step, 2), lax.rem(step + 1, 2)
    part = blocks // turns

    def multiply(i):
        out_ref[0, :, i * part * BLK : (i + 1) * part * BLK] = jnp.dot(
            go_ref[before],
            columns(d_ref, slice(None), i * part, part),
            preferred_element_type=F32,
        ).astype(out_ref.dtype)

    def gate(i):
        rows = [slice(i * PAIR + h * BLK, i * PAIR + (h + 1) * BLK) for h in range(2)]
        for g in range(2):
            gain, shift = ROOT * gain_ref[0, g : g + 1], shift_ref[0, g : g + 1]
            normed = []
            for at in rows:
                scaled, _ = norm(gelu(v_ref[at, cols_of(g)].astype(F32)))
                normed.append((scaled * gain + shift).astype(BF16))
            mixed = jnp.dot(
                w_ref[0, g], jnp.concatenate(normed, axis=1), preferred_element_type=F32
            )
            for h, at in enumerate(rows):
                upper = gelu(u_ref[at, cols_of(g)].astype(F32))
                gated_out = (upper * (mixed[:, cols_of(h)] + bias_at[g])).astype(BF16)
                go_ref[now, cols_of(g), at] = gated_out.T

    @pl.when(step == 0)
    def _():
        scatter_columns(d_hbm, d_ref, sem)

    for g in range(2):
        bias_at[g] = jnp.broadcast_to(bias_ref[0, :, g : g + 1], (BLK, BLK))

    @pl.when(step == 0)
    def _():
        for i in range(turns):
            gate(i)
        await_all(d_ref, sem)

    @pl.when((step > 0) & (step < last))
    def _():
        for i in range(turns):
            multiply(i)
            gate(i)

    @pl.when(step == last)
    def _():
        for i in range(turns):
            multiply(i)


def forward(order, u, v, d, w_low, bias, gain, shift):
    n = order.shape[0]
    length, width = u.shape
    last = n - 1
    cur = lambda j, o: (0, o[jnp.minimum(j, last)])
    par = lambda j, o: (o[jnp.minimum(j, last)], 0, 0)
    return pl.pallas_call(
        forward_kernel,
        grid_spec=pltpu.PrefetchScalarGridSpec(
            num_scalar_prefetch=1,
            grid=(n + 1,),
            in_specs=[
                pl.BlockSpec((length, PAIR), cur),
                pl.BlockSpec((length, PAIR), cur),
                pl.BlockSpec(memory_space=pl.ANY),
                pl.BlockSpec((1, 2, BLK, BLK), lambda j, o: (o[jnp.minimum(j, last)], 0, 0, 0)),
                pl.BlockSpec((1, BLK, 2), par),
                pl.BlockSpec((1, 2, BLK), par),
                pl.BlockSpec((1, 2, BLK), par),
            ],
            out_specs=pl.BlockSpec((1, PAIR, width), lambda j, o: (jnp.maximum(j - 1, 0), 0, 0)),
            scratch_shapes=[
                pltpu.VMEM((width // BLK, length, BLK), BF16),
                pltpu.VMEM((2, PAIR, length), BF16),
                pltpu.VMEM((2, BLK, BLK), F32),
                pltpu.SemaphoreType.DMA,
            ],
        ),
        out_shape=jax.ShapeDtypeStruct((n, PAIR, width), BF16),
        cost_estimate=pl.CostEstimate(
            flops=2 * n * PAIR * length * (width + BLK) * 2,
            bytes_accessed=length * width * 2 + n * PAIR * (4 * length + 2 * width),
            transcendentals=2 * n * PAIR * length,
        ),
        name="fwd",
    )(order, u, v, d, w_low, bias, gain, shift)


def backward_kernel(
    pieces, order, u_ref, v_ref, d_hbm, low_ref, lowt_ref, bias_ref, gain_ref, shift_ref, *rest
):
    count = len(pieces)
    w_hbm = rest[:count]
    gu_ref, gv_ref, pack_ref = rest[-12:-9]
    d_ref, w_ref, cot_ref, bias_at, b_acc, g_acc, s_acc, m_acc, sems = rest[-9:]
    turns = u_ref.shape[0] // PAIR
    step = pl.program_id(0)
    last = pl.num_programs(0) - 1

    def landing(k):
        slot, start, size = pieces[k]
        return w_ref.at[slot, :, pl.ds(start, size)]

    def cotangent(i, slot):
        return lax.dot_general(
            columns(d_ref, slice(i * PAIR, (i + 1) * PAIR)),
            columns(w_ref.at[slot], slice(None)),
            (((1,), (1,)), ((), ())),
            preferred_element_type=F32,
        )

    @pl.when(step == 0)
    def _():
        for k in range(count):
            if pieces[k][0] == 0:
                scatter_columns(w_hbm[k], landing(k), sems.at[k])
        scatter_columns(d_hbm, d_ref, sems.at[count])
        for k in range(count):
            if pieces[k][0] > 0:
                scatter_columns(w_hbm[k], landing(k), sems.at[k])
        for k in range(count):
            if pieces[k][0] == 0:
                await_all(landing(k), sems.at[k])
        await_all(d_ref, sems.at[count])
        cot_ref[0] = cotangent(0, 0)

    for k in range(count):
        if pieces[k][0] > 0:
            @pl.when(step == pieces[k][0] - 1)
            def _(k=k):
                await_all(landing(k), sems.at[k])

    for g in range(2):
        bias_at[g] = jnp.broadcast_to(bias_ref[0, :, g : g + 1], (BLK, BLK))
    b_acc[...] = jnp.zeros_like(b_acc)
    g_acc[...] = jnp.zeros_like(g_acc)
    s_acc[...] = jnp.zeros_like(s_acc)
    m_acc[...] = jnp.zeros_like(m_acc)
    for i in range(turns):
        if i + 1 < turns:
            cot_ref[(i + 1) % 2] = cotangent(i + 1, step)
        else:
            cot_ref[0] = cotangent(0, jnp.minimum(step + 1, last))
        for g in range(2):
            gain, shift = ROOT * gain_ref[0, g : g + 1], shift_ref[0, g : g + 1]
            rows = [slice(i * PAIR + h * BLK, i * PAIR + (h + 1) * BLK) for h in range(2)]
            kept, normed = [], []
            for at in rows:
                gated, slope = gelu_and_slope(v_ref[at, cols_of(g)].astype(F32))
                scaled, inverse = norm(gated)
                kept.append((scaled, inverse * slope))
                normed.append((scaled * gain + shift).astype(BF16))
            normed = jnp.concatenate(normed, axis=1)
            mixed = jnp.dot(low_ref[0, g], normed, preferred_element_type=F32)
            d_mixed_b = []
            for h, at in enumerate(rows):
                upper, slope = gelu_and_slope(u_ref[at, cols_of(g)].astype(F32))
                cot = cot_ref[i % 2, h * BLK : (h + 1) * BLK, cols_of(g)]
                d_mixed = cot * upper
                d_mixed_b.append(d_mixed.astype(BF16))
                b_acc[g] += d_mixed
                gu_ref[at, cols_of(g)] = (
                    cot * slope * (mixed[:, cols_of(h)] + bias_at[g])
                ).astype(BF16)
            d_mixed_b = jnp.concatenate(d_mixed_b, axis=1)
            m_acc[g] += lax.dot_general(
                d_mixed_b, normed, (((1,), (1,)), ((), ())), preferred_element_type=F32
            )
            d_normed = jnp.dot(lowt_ref[0, g], d_mixed_b, preferred_element_type=F32)
            for h, at in enumerate(rows):
                scaled, scale = kept[h]
                dn = d_normed[:, cols_of(h)]
                weighted = dn * scaled
                g_acc[g] += jnp.sum(weighted.reshape(BLK // 8, 8, BLK), axis=0)
                s_acc[g] += jnp.sum(dn.reshape(BLK // 8, 8, BLK), axis=0)
                e = dn * gain
                mean_e = jnp.mean(e, axis=-1, keepdims=True)
                sum_es = jnp.sum(weighted * gain, axis=-1, keepdims=True)
                gv_ref[at, cols_of(g)] = (scale * (e - mean_e - scaled * sum_es)).astype(BF16)

    row = lax.broadcasted_iota(jnp.int32, (BLK, BLK), 0)
    col = lax.broadcasted_iota(jnp.int32, (BLK, BLK), 1)
    filler = jnp.zeros((CHUNK - 17, BLK), F32)
    extra = []
    for g in range(2):
        extra.append(jnp.sum(b_acc[g].T, axis=0, keepdims=True))
        extra.append(ROOT * jnp.sum(g_acc[g], axis=0, keepdims=True))
        extra.append(jnp.sum(s_acc[g], axis=0, keepdims=True))
    for g in range(2):
        lower = jnp.where(row >= col, m_acc[g], 0.0)
        for r in range(8):
            k = g * 8 + r
            vector = extra[k] if k < len(extra) else jnp.zeros((1, BLK), F32)
            pack_ref[0, k] = jnp.concatenate(
                [lower[r * 16 : (r + 1) * 16], vector, filler], axis=0
            ).astype(BF16)


def backward(order, weights, u, v, d, w_low, w_low_t, bias, gain, shift, earlier):
    n = order.shape[0]
    length, width = u.shape
    pairs = width // PAIR
    pieces = tuple((slot, start, w.shape[0]) for slot, start, w in weights)
    cur = lambda j, o: (0, o[j])
    par = lambda j, o: (o[j], 0, 0)
    mat = pl.BlockSpec((1, 2, BLK, BLK), lambda j, o: (o[j], 0, 0, 0))
    tile = pl.BlockSpec((length, PAIR), cur)
    vec = pl.BlockSpec((1, 2, BLK), par)
    col = pl.BlockSpec((1, BLK, 2), par)
    hbm = pl.BlockSpec(memory_space=pl.ANY)
    shapes = [
        jax.ShapeDtypeStruct((length, width), BF16),
        jax.ShapeDtypeStruct((length, width), BF16),
        jax.ShapeDtypeStruct((pairs, 16, CHUNK, BLK), BF16),
    ]
    first = 9 + len(weights)
    alias = {first + k: k for k in range(len(earlier))}
    return pl.pallas_call(
        functools.partial(backward_kernel, pieces),
        grid_spec=pltpu.PrefetchScalarGridSpec(
            num_scalar_prefetch=1,
            grid=(n,),
            in_specs=[
                tile,
                tile,
                hbm,
                mat,
                mat,
                col,
                vec,
                vec,
                *[hbm] * len(weights),
                *[hbm] * len(earlier),
            ],
            out_specs=[
                tile,
                tile,
                pl.BlockSpec((1, 16, CHUNK, BLK), lambda j, o: (o[j], 0, 0, 0)),
            ],
            scratch_shapes=[
                pltpu.VMEM((width // BLK, length, BLK), BF16),
                pltpu.VMEM((n, width // BLK, PAIR, BLK), BF16),
                pltpu.VMEM((2, PAIR, PAIR), F32),
                pltpu.VMEM((2, BLK, BLK), F32),
                pltpu.VMEM((2, BLK, BLK), F32),
                pltpu.VMEM((2, 8, BLK), F32),
                pltpu.VMEM((2, 8, BLK), F32),
                pltpu.VMEM((2, BLK, BLK), F32),
                pltpu.SemaphoreType.DMA((len(weights) + 1,)),
            ],
        ),
        out_shape=shapes,
        input_output_aliases=alias,
        cost_estimate=pl.CostEstimate(
            flops=2 * n * PAIR * length * (width + 3 * BLK) * 2,
            bytes_accessed=length * width * 2 + n * PAIR * (8 * length + 2 * width),
            transcendentals=3 * n * PAIR * length,
        ),
        name="bwd",
    )(order, u, v, d, w_low, w_low_t, bias, gain, shift, *[w for _, _, w in weights], *earlier)


def hop(a, axis, size, by):
    return lax.ppermute(a, axis, [(i, (i + by) % size) for i in range(size)])


def added(a):
    return lax.optimization_barrier(jnp.sum(a.astype(F32), axis=0)).astype(BF16)


def spread(a, axes, count):
    return lax.all_to_all(jnp.broadcast_to(a[None], (count,) + a.shape), axes, 0, 0)


def on_device(u_pre, v_pre, d_out, w_mix, mix_bias, norm_gain, norm_shift, w_out, sizes=None):
    return everything(
        u_pre, v_pre, d_out, w_mix, mix_bias, norm_gain, norm_shift, w_out, sizes
    )


def everything(u_pre, v_pre, d_out, w_mix, mix_bias, norm_gain, norm_shift, w_out, sizes):
    nz, ny, nx, nc = sizes
    plane = nz * ny
    u, v, d = u_pre[0], v_pre[0], d_out[0]
    _, width = u.shape
    groups = w_mix.shape[0]
    pairs = groups // 2
    x, c = lax.axis_index("x"), lax.axis_index("c")
    xs = jnp.arange(nx, dtype=jnp.int32)

    swap = lambda a: hop(a, "c", nc, 1)
    half = w_out.shape[0] // 2
    own = swap(w_out)
    left = hop(w_out, "x", nx, 1)
    right = hop(w_out, "x", nx, -1)
    far0 = hop(left[:half], "x", nx, 1)
    far1 = hop(right[half:], "x", nx, -1)
    near = [swap(left), swap(right)]
    far = [swap(far0), swap(far1)]

    w_low = jnp.tril(w_mix)
    w_low_t = jnp.swapaxes(w_low, 1, 2).reshape(pairs, 2, BLK, BLK)
    w_low = w_low.reshape(pairs, 2, BLK, BLK)
    bias = jnp.swapaxes(mix_bias.reshape(pairs, 2, BLK), 1, 2)
    gain = norm_gain.reshape(pairs, 2, BLK)
    shift = norm_shift.reshape(pairs, 2, BLK)

    common = (u, v, d, w_low, bias, gain, shift)
    theirs = forward(xs * nc + (1 - c), *common)
    ours = forward(xs * nc + c, *common)
    traded = swap(theirs)
    joined = (ours.astype(F32) + traded.astype(F32)).astype(BF16)
    split = lax.all_to_all(joined.reshape(nx * plane, PAIR // plane, width), ("x", "z", "y"), 0, 0)

    backs = (u, v, d, w_low, w_low_t, bias, gain, shift)
    place = lambda k, core: lax.rem(x + k, nx) * nc + core
    order = jnp.stack([place(0, c), place(0, 1 - c)])
    out = backward(order, [(0, 0, w_out), (1, 0, own)], *backs, ())
    order = jnp.stack([place(3, c), place(1, c), place(3, 1 - c), place(1, 1 - c)])
    out = backward(
        order, [(0, 0, left), (1, 0, right), (2, 0, near[0]), (3, 0, near[1])], *backs, out
    )
    order = jnp.stack([place(2, c), place(2, 1 - c)])
    out = backward(
        order, [(0, 0, far0), (0, half, far1), (1, 0, far[0]), (1, half, far[1])], *backs, out
    )
    grad_u, grad_v, packed = out
    packed, split = lax.optimization_barrier((packed, split))
    grad_w_out = spread(added(split), ("z", "y"), plane)
    grad_w_out = grad_w_out.reshape(PAIR, width).astype(F32)
    devices = nz * ny * nx * nc
    every = ("z", "y", "x", "c")
    packed = lax.all_to_all(packed.reshape(devices, CHUNK, BLK), every, 0, 0)
    total = spread(added(packed), every, devices)
    grad_w = total[:, :16].astype(F32).reshape(groups, BLK, BLK)
    rest = total.reshape(pairs, 16, CHUNK, BLK)[:, :6, 16].astype(F32).reshape(groups, 3, BLK)
    vectors = [rest[:, k] for k in range(3)]
    return (grad_u[None], grad_v[None], grad_w_out, grad_w, *vectors)


def solution(mesh):
    devices = mesh.devices.reshape(4, -1, *[mesh.devices.shape[1] // 2, 2])
    grid = Mesh(devices, ("z", "y", "x", "c"))
    big = P(("x", "c"), ("z", "y"), None)
    rows = P(("x", "c"), None)
    return jax.shard_map(
        functools.partial(on_device, sizes=devices.shape),
        mesh=grid,
        in_specs=(big, big, big, P(), P(), P(), P(), rows),
        out_specs=(big, big, rows, P(), P(), P(), P()),
        check_vma=False,
    )
```

time: 478 us -> 250 us (0.52)
  waiting for transfers between devices: 274 us -> 117 us
  local copies, waits for them, and re-layouts: 84.7 us -> 8.87 us
  Pallas kernels: 0 us -> 67 us
  matrix products: 54.5 us -> 0 us
  starting transfers between devices: 0.16 us -> 37.4 us
  other arithmetic: 45.8 us -> 18.1 us
  between operations: 14.2 us -> 0.89 us
    psum x2 -> x0, waiting for transfers between devices: 217 us -> none  [the longest x1 127 us: together(): total = lax.psum(jnp.concatenate([a.ravel() for a in arrays]), axis)]
    ppermute x0 -> x10, waiting for transfers between devices: none -> 70.9 us  [hop(): return lax.ppermute(a, axis, [(i, (i + by) % size) for i in range(size)])]
    pallas_call x0 -> x5, Pallas kernels: none -> 67 us  [the longest x3 40.6 us: backward(): pl.pallas_call(functools.partial(backward_kernel, pieces), grid_spec=pltp...]
    reduce_scatter x1 -> x0, waiting for transfers between devices: 54.8 us -> none  [on_device(): lax.psum_scatter(lax.dot_general(flat_s, flat_d, (((0,), (0,)), ((), ()))...]
    dot_general x5 -> x0, matrix products: 54.5 us -> none  [the longest x1 15.4 us: on_device(): lax.dot_general(flat_s, flat_d, (((0,), (0,)), ((), ())), preferred_eleme...]
    all_to_all x0 -> x4, waiting for transfers between devices: none -> 45.6 us  [the longest x2 32.1 us: spread(): lax.all_to_all(jnp.broadcast_to(a[None], (count,) + a.shape), axes, 0, 0)]
    reshape x5 -> x1, local copies, waits for them, and re-layouts: 41.6 us -> 1.73 us  [everything(): bias = jnp.swapaxes(mix_bias.reshape(pairs, 2, BLK), 1, 2)]
    all_to_all x0 -> x4, starting transfers between devices: none -> 29.4 us  [the longest x1 11.9 us: everything(): lax.all_to_all(joined.reshape(nx * plane, PAIR // plane, width), ('x', 'z...]
  transfers between devices with their start and end apart: 4 -> 14, of which waited for: 4 -> 4; matrix products, arithmetic and copies ran while one was open for 25% -> 4% of each run, Pallas kernels for 0% -> 22%
where the time goes in v1:
time: 250 us; the launch traced here: 249 us
  waiting for transfers between devices  117 us (47%)
  Pallas kernels  67 us (27%)
  starting transfers between devices  37.4 us (15%)
  other arithmetic  18.1 us (7%)
  local copies, waits for them, and re-layouts  8.87 us (4%)
    ppermute x10, waiting for transfers between devices, hop(): return lax.ppermute(a, axis, [(i, (i + by) % size) for i in range(size)])  70.9 us
    pallas_call x3, Pallas kernels, backward(): pl.pallas_call(functools.partial(backward_kernel, pieces), grid_spec=pltp...  40.6 us
    all_to_all x2, waiting for transfers between devices, spread(): lax.all_to_all(jnp.broadcast_to(a[None], (count,) + a.shape), axes, 0, 0)  32.1 us
    pallas_call x2, Pallas kernels, forward(): pl.pallas_call(forward_kernel, grid_spec=pltpu.PrefetchScalarGridSpec(num...  26.4 us
    all_to_all x1, waiting for transfers between devices, everything(): packed = lax.all_to_all(packed.reshape(devices, CHUNK, BLK), every, 0, 0)  13.5 us
    all_to_all x1, starting transfers between devices, everything(): lax.all_to_all(joined.reshape(nx * plane, PAIR // plane, width), ('x', 'z...  11.9 us
    all_to_all x1, starting transfers between devices, everything(): packed = lax.all_to_all(packed.reshape(devices, CHUNK, BLK), every, 0, 0)  9.23 us
    all_to_all x2, starting transfers between devices, spread(): lax.all_to_all(jnp.broadcast_to(a[None], (count,) + a.shape), axes, 0, 0)  8.28 us
  transfers between devices with their start and end apart: 14, of which 4 were waited for; matrix products, arithmetic and copies ran while one was open for 4% of the time, Pallas kernels for 22%

profile of v1, /device:TPU:0, one launch (start us, length us, event | category | flops | bytes accessed | tf_op | source)
XLA Modules:
  0.0 248.8 jit_solution(9955441897309862908)
XLA Ops:
  0.7 1.7 copy.23
  2.4 0.5 fusion.order
  2.9 1.9 broadcast_select_fusion
  4.8 13.2 %fwd.3 = bf16[4,256,2048]{2,1,0:T(8,128)(2,1)} custom-call(s32[4]{0:T(128)} %fusion.order, bf16[1024,2048]{1,0:T(8,128)(2,1)} %bitcast.37, bf16[1024,2048]{1,0:T(8,128)(2,1)} %bitcast.42, bf16[1024,2048]{1,0:T(8,128)(2,1)} %bitcast.47, bf16[8,2,128,128]{3,2,1,0:T(8,128)(2,1)} %bitcast.60, f32[8,128,2]{2,1,0:T(8,128)} %bitcast.55, f32[8,2,128]{2,1,0:T(2,128)} %bitcast.70, ...), custom_call_target="tpu_custom_call" | custom-call | flops 9126805504 | bytes 12582912 | tf_op jit(solution)/shard_map/fwd/pallas_call | solution.py:128
  18.0 0.1 collective-permute-start.9
  18.1 0.5 fusion.1.order
  18.6 13.2 %fwd.2 = bf16[4,256,2048]{2,1,0:T(8,128)(2,1)} custom-call(s32[4]{0:T(128)} %fusion.1.order, bf16[1024,2048]{1,0:T(8,128)(2,1)} %bitcast.38, bf16[1024,2048]{1,0:T(8,128)(2,1)} %bitcast.43, bf16[1024,2048]{1,0:T(8,128)(2,1)} %bitcast.48, bf16[8,2,128,128]{3,2,1,0:T(8,128)(2,1)} %bitcast.61, f32[8,128,2]{2,1,0:T(8,128)} %bitcast.56, f32[8,2,128]{2,1,0:T(2,128)} %bitcast.71, ...), custom_call_target="tpu_custom_call" | custom-call | flops 9126805504 | bytes 12582912 | tf_op jit(solution)/shard_map/fwd/pallas_call | solution.py:128
  31.8 0.0 collective-permute-done.9
  31.8 7.7 %add_convert_fusion = bf16[4,256,2048]{2,1,0:T(8,128)(2,1)} fusion(bf16[4,256,2048]{2,1,0:T(8,128)(2,1)} %collective-permute-done.9, bf16[4,256,2048]{2,1,0:T(8,128)(2,1)} %fwd.2), kind=kLoop, calls=%fused_computation.1 | loop fusion | flops 8388608 | bytes 12582912 | tf_op jit(solution)/shard_map/convert_element_type | solution.py:383
  39.5 11.9 %all-to-all-start = ((bf16[64,16,2048]{2,1,0:T(8,128)(2,1)}), bf16[64,16,2048]{2,1,0:T(8,128)(2,1)}, u32[]{:S(2)}, u32[]{:S(2)}) async-start(bf16[64,16,2048]{2,1,0:T(8,128)(2,1)} %bitcast.36), calls=%async_computation | async-start | bytes 8388608 | tf_op jit(solution)/shard_map/all_to_all | solution.py:384
  51.4 1.8 collective-permute-start
  53.2 1.7 collective-permute-start.2
  54.9 70.8 %collective-permute-done.rest_0_ = bf16[256,2048]{1,0:T(8,128)(2,1)} collective-permute-done((bf16[256,2048]{1,0:T(8,128)(2,1)}, bf16[256,2048]{1,0:T(8,128)(2,1)}, u32[]{:S(2)}, u32[]{:S(2)}) %collective-permute-start) | collective-permute-done | bytes 1048608 | tf_op jit(solution)/shard_map/ppermute | solution.py:335
  125.7 0.0 collective-permute-done.2.rest_1_
  125.8 0.5 collective-permute-start.7
  126.3 0.6 pad_add_fusion.2.order
  126.9 0.6 pad_add_fusion.order
  127.5 1.1 slice.28
  128.6 0.1 collective-permute-start.1
  128.6 1.1 slice.29
  129.7 3.3 %collective-permute-start.3 = (bf16[128,2048]{1,0:T(8,128)(2,1)S(1)}, bf16[128,2048]{1,0:T(8,128)(2,1)S(1)}, u32[]{:S(2)}, u32[]{:S(2)}) collective-permute-start(bf16[128,2048]{1,0:T(8,128)(2,1)S(1)} %slice.29), channel_id=1, source_target_pairs={{0,6},{2,0},{4,2},{6,4},{1,7},{3,1},{5,3},{7,5},{8,14},{10,8},{12,... | collective-permute-start | bytes 1572872 | tf_op jit(solution)/shard_map/ppermute | solution.py:335
  133.0 0.6 pad_add_fusion.1.order
  133.6 1.0 copy.22
  134.6 11.6 %bwd.3 = (bf16[1024,2048]{1,0:T(8,128)(2,1)}, bf16[1024,2048]{1,0:T(8,128)(2,1)}, bf16[8,16,24,128]{3,2,1,0:T(8,128)(2,1)}) custom-call(s32[2]{0:T(128)} %pad_add_fusion.2.order, bf16[1024,2048]{1,0:T(8,128)(2,1)} %bitcast.39, bf16[1024,2048]{1,0:T(8,128)(2,1)} %bitcast.44, bf16[1024,2048]{1,0:T(8,128)(2,1)} %bitcast.49, bf16[8,2,128,128]{3,2,1,0:T(8,128)(2,1)} %bitcast.62, ...), custom_call_target="tpu_custom_call" | custom-call | flops 5100273664 | bytes 10485760 | tf_op jit(solution)/shard_map/bwd/pallas_call | solution.py:289
  146.3 0.1 collective-permute-start.4
  146.4 0.0 collective-permute-done.3.rest_1_
  146.4 0.5 collective-permute-start.5
  146.9 0.0 collective-permute-done.6.rest_2_
  146.9 0.0 collective-permute-done.7.rest_3_
  146.9 17.3 %bwd.4 = (bf16[1024,2048]{1,0:T(8,128)(2,1)}, bf16[1024,2048]{1,0:T(8,128)(2,1)}, bf16[8,16,24,128]{3,2,1,0:T(8,128)(2,1)}) custom-call(s32[4]{0:T(128)} %pad_add_fusion.1.order, bf16[1024,2048]{1,0:T(8,128)(2,1)} %bitcast.40, bf16[1024,2048]{1,0:T(8,128)(2,1)} %bitcast.45, ...), custom_call_target="tpu_custom_call", output_to_operand_aliasing={{0}: (13, {}), {1}: (14, {}), {2}: (15, {})} | custom-call | flops 10200547328 | bytes 16777216 | tf_op jit(solution)/shard_map/bwd/pallas_call | solution.py:289
  164.3 0.8 copy-done.3
  165.1 0.2 copy-done.4
  165.3 11.7 %bwd.5 = (bf16[1024,2048]{1,0:T(8,128)(2,1)}, bf16[1024,2048]{1,0:T(8,128)(2,1)}, bf16[8,16,24,128]{3,2,1,0:T(8,128)(2,1)}) custom-call(s32[2]{0:T(128)} %pad_add_fusion.order, bf16[1024,2048]{1,0:T(8,128)(2,1)} %bitcast.41, bf16[1024,2048]{1,0:T(8,128)(2,1)} %bitcast.46, ...), custom_call_target="tpu_custom_call", output_to_operand_aliasing={{0}: (13, {}), {1}: (14, {}), {2}: (15, {})} | custom-call | flops 5100273664 | bytes 10485760 | tf_op jit(solution)/shard_map/bwd/pallas_call | solution.py:289
  177.0 0.0 all-to-all-done
  177.0 9.2 %all-to-all-start.2 = ((bf16[128,24,128]{2,1,0:T(8,128)(2,1)}), bf16[128,24,128]{2,1,0:T(8,128)(2,1)S(1)}, u32[]{:S(2)}, u32[]{:S(2)}) async-start(bf16[128,24,128]{2,1,0:T(8,128)(2,1)} %bitcast.54), calls=%async_computation.2 | async-start | bytes 1572864 | tf_op jit(solution)/shard_map/all_to_all | solution.py:404
  186.3 2.8 %convert_reduce_fusion = bf16[16,2048]{1,0:T(8,128)(2,1)S(1)} fusion(bf16[64,16,2048]{2,1,0:T(8,128)(2,1)} %all-to-all-done), kind=kLoop, calls=%fused_computation | loop fusion | flops 4161536 | bytes 4259840 | tf_op jit(solution)/shard_map/reduce_sum | solution.py:339
  189.1 13.5 %all-to-all-done.2 = bf16[128,24,128]{2,1,0:T(8,128)(2,1)S(1)} async-done(((bf16[128,24,128]{2,1,0:T(8,128)(2,1)}), bf16[128,24,128]{2,1,0:T(8,128)(2,1)S(1)}, u32[]{:S(2)}, u32[]{:S(2)}) %all-to-all-start.2) | async-done | bytes 786464 | tf_op jit(solution)/shard_map/all_to_all | solution.py:404
  202.6 1.1 broadcast_in_dim.30
  203.7 3.7 %all-to-all-start.1 = ((bf16[16,16,2048]{2,1,0:T(8,128)(2,1)}), bf16[16,16,2048]{2,1,0:T(8,128)(2,1)S(1)}, u32[]{:S(2)}, u32[]{:S(2)}) async-start(bf16[16,16,2048]{2,1,0:T(8,128)(2,1)} %broadcast_in_dim.30), calls=%async_computation.1 | async-start | bytes 2097152 | tf_op jit(solution)/shard_map/all_to_all | solution.py:343
  207.3 0.2 convert_reduce_fusion.1
  207.5 17.5 %all-to-all-done.1 = bf16[16,16,2048]{2,1,0:T(8,128)(2,1)S(1)} async-done(((bf16[16,16,2048]{2,1,0:T(8,128)(2,1)}), bf16[16,16,2048]{2,1,0:T(8,128)(2,1)S(1)}, u32[]{:S(2)}, u32[]{:S(2)}) %all-to-all-start.1) | async-done | bytes 1048608 | tf_op jit(solution)/shard_map/all_to_all | solution.py:343
  225.0 1.0 broadcast_in_dim.31
  226.0 4.6 %all-to-all-start.3 = ((bf16[128,24,128]{2,1,0:T(8,128)(2,1)}), bf16[128,24,128]{2,1,0:T(8,128)(2,1)S(1)}, u32[]{:S(2)}, u32[]{:S(2)}) async-start(bf16[128,24,128]{2,1,0:T(8,128)(2,1)} %broadcast_in_dim.31), calls=%async_computation.3 | async-start | bytes 1572864 | tf_op jit(solution)/shard_map/all_to_all | solution.py:343
  230.6 1.6 bitcast_convert_fusion
  232.2 14.7 %all-to-all-done.3 = bf16[128,24,128]{2,1,0:T(8,128)(2,1)S(1)} async-done(((bf16[128,24,128]{2,1,0:T(8,128)(2,1)}), bf16[128,24,128]{2,1,0:T(8,128)(2,1)S(1)}, u32[]{:S(2)}, u32[]{:S(2)}) %all-to-all-start.3) | async-done | bytes 786464 | tf_op jit(solution)/shard_map/all_to_all | solution.py:343
  246.9 1.1 bitcast_convert_fusion.1
  248.0 0.2 copy.24
  248.2 0.6 fusion.2
  (19 shorter events, 0.1 us)
Async XLA Ops:
  18.0 13.8 %collective-permute-start.9 = (bf16[4,256,2048]{2,1,0:T(8,128)(2,1)}, bf16[4,256,2048]{2,1,0:T(8,128)(2,1)}, u32[]{:S(2)}, u32[]{:S(2)}) collective-permute-start(bf16[4,256,2048]{2,1,0:T(8,128)(2,1)} %fwd.3), channel_id=1, source_target_pairs={{0,1},{1,0},{2,3},{3,2},{4,5},{5,4},{6,7},{7,6},{8,9},{9,8},{10,11... | collective-permute-start | bytes 12582920 | tf_op jit(solution)/shard_map/ppermute | solution.py:335
  39.5 88.0 %copy-start = (bf16[16,128,128]{2,1,0:T(8,128)(2,1)S(1)}, bf16[16,128,128]{2,1,0:T(8,128)(2,1)}, u32[]{:S(2)}) copy-start(bf16[16,128,128]{2,1,0:T(8,128)(2,1)} %param.11) | copy-start | bytes 1572868
  39.5 137.5 %all-to-all-start = ((bf16[64,16,2048]{2,1,0:T(8,128)(2,1)}), bf16[64,16,2048]{2,1,0:T(8,128)(2,1)}, u32[]{:S(2)}, u32[]{:S(2)}) async-start(bf16[64,16,2048]{2,1,0:T(8,128)(2,1)} %bitcast.36), calls=%async_computation | async-start | bytes 8388608 | tf_op jit(solution)/shard_map/all_to_all | solution.py:384
  51.4 74.3 %collective-permute-start = (bf16[256,2048]{1,0:T(8,128)(2,1)}, bf16[256,2048]{1,0:T(8,128)(2,1)}, u32[]{:S(2)}, u32[]{:S(2)}) collective-permute-start(bf16[256,2048]{1,0:T(8,128)(2,1)} %rest_0_.1), channel_id=1, source_target_pairs={{0,2},{2,4},{4,6},{6,0},{1,3},{3,5},{5,7},{7,1},{8,10},{10,12},{12... | collective-permute-start | bytes 3145736 | tf_op jit(solution)/shard_map/ppermute | solution.py:335
  53.2 72.6 %collective-permute-start.2 = (bf16[256,2048]{1,0:T(8,128)(2,1)}, bf16[256,2048]{1,0:T(8,128)(2,1)}, u32[]{:S(2)}, u32[]{:S(2)}) collective-permute-start(bf16[256,2048]{1,0:T(8,128)(2,1)} %rest_0_.1), channel_id=1, source_target_pairs={{0,6},{2,0},{4,2},{6,4},{1,7},{3,1},{5,3},{7,5},{8,14},{10,8},{12,... | collective-permute-start | bytes 3145736 | tf_op jit(solution)/shard_map/ppermute | solution.py:335
  54.9 79.7 %collective-permute-start.8 = (bf16[256,2048]{1,0:T(8,128)(2,1)}, bf16[256,2048]{1,0:T(8,128)(2,1)}, u32[]{:S(2)}, u32[]{:S(2)}) collective-permute-start(bf16[256,2048]{1,0:T(8,128)(2,1)} %rest_0_.1), channel_id=1, source_target_pairs={{0,1},{1,0},{2,3},{3,2},{4,5},{5,4},{6,7},{7,6},{8,9},{9,8},{10,11... | collective-permute-start | bytes 3145736 | tf_op jit(solution)/shard_map/ppermute | solution.py:335
  125.7 21.1 %collective-permute-start.6 = (bf16[256,2048]{1,0:T(8,128)(2,1)}, bf16[256,2048]{1,0:T(8,128)(2,1)}, u32[]{:S(2)}, u32[]{:S(2)}) collective-permute-start(bf16[256,2048]{1,0:T(8,128)(2,1)} %collective-permute-done.rest_0_), channel_id=1, source_target_pairs={{0,1},{1,0},{2,3},{3,2},{4,5},{5,4},{6,7},{7,6},{8,9},{9,8},{10,11... | collective-permute-start | bytes 3145736 | tf_op jit(solution)/shard_map/ppermute | solution.py:335
  125.8 21.1 %collective-permute-start.7 = (bf16[256,2048]{1,0:T(8,128)(2,1)}, bf16[256,2048]{1,0:T(8,128)(2,1)}, u32[]{:S(2)}, u32[]{:S(2)}) collective-permute-start(bf16[256,2048]{1,0:T(8,128)(2,1)} %collective-permute-done.2.rest_1_), channel_id=1, source_target_pairs={{0,1},{1,0},{2,3},{3,2},{4,5},{5,4},{6,7},{7,6},{8,9},{9,8},{10,11... | collective-permute-start | bytes 3145736 | tf_op jit(solution)/shard_map/ppermute | solution.py:335
  128.6 17.7 %collective-permute-start.1 = (bf16[128,2048]{1,0:T(8,128)(2,1)S(1)}, bf16[128,2048]{1,0:T(8,128)(2,1)S(1)}, u32[]{:S(2)}, u32[]{:S(2)}) collective-permute-start(bf16[128,2048]{1,0:T(8,128)(2,1)S(1)} %slice.28), channel_id=1, source_target_pairs={{0,2},{2,4},{4,6},{6,0},{1,3},{3,5},{5,7},{7,1},{8,10},{10,12},{12... | collective-permute-start | bytes 1572872 | tf_op jit(solution)/shard_map/ppermute | solution.py:335
  129.7 16.6 %collective-permute-start.3 = (bf16[128,2048]{1,0:T(8,128)(2,1)S(1)}, bf16[128,2048]{1,0:T(8,128)(2,1)S(1)}, u32[]{:S(2)}, u32[]{:S(2)}) collective-permute-start(bf16[128,2048]{1,0:T(8,128)(2,1)S(1)} %slice.29), channel_id=1, source_target_pairs={{0,6},{2,0},{4,2},{6,4},{1,7},{3,1},{5,3},{7,5},{8,14},{10,8},{12,... | collective-permute-start | bytes 1572872 | tf_op jit(solution)/shard_map/ppermute | solution.py:335
  146.3 18.0 %copy-start.1 = (bf16[128,2048]{1,0:T(8,128)(2,1)}, bf16[128,2048]{1,0:T(8,128)(2,1)S(1)}, u32[]{:S(2)}) copy-start(bf16[128,2048]{1,0:T(8,128)(2,1)S(1)} %collective-permute-done.1.rest_0_) | copy-start | bytes 1572868
  146.3 18.0 %collective-permute-start.4 = (bf16[128,2048]{1,0:T(8,128)(2,1)S(1)}, bf16[128,2048]{1,0:T(8,128)(2,1)S(1)}, u32[]{:S(2)}, u32[]{:S(2)}) collective-permute-start(bf16[128,2048]{1,0:T(8,128)(2,1)S(1)} %collective-permute-done.1.rest_0_), channel_id=1, source_target_pairs={{0,1},{1,0},{2,3},{3,2},{4,5},{5,4},{6,7},{7,6},{8,9},{9,8},{10,11... | collective-permute-start | bytes 1572872 | tf_op jit(solution)/shard_map/ppermute | solution.py:335
  146.4 17.9 %copy-start.2 = (bf16[128,2048]{1,0:T(8,128)(2,1)}, bf16[128,2048]{1,0:T(8,128)(2,1)S(1)}, u32[]{:S(2)}) copy-start(bf16[128,2048]{1,0:T(8,128)(2,1)S(1)} %collective-permute-done.3.rest_1_) | copy-start | bytes 1572868
  146.4 17.9 %collective-permute-start.5 = (bf16[128,2048]{1,0:T(8,128)(2,1)S(1)}, bf16[128,2048]{1,0:T(8,128)(2,1)S(1)}, u32[]{:S(2)}, u32[]{:S(2)}) collective-permute-start(bf16[128,2048]{1,0:T(8,128)(2,1)S(1)} %collective-permute-done.3.rest_1_), channel_id=1, source_target_pairs={{0,1},{1,0},{2,3},{3,2},{4,5},{5,4},{6,7},{7,6},{8,9},{9,8},{10,11... | collective-permute-start | bytes 1572872 | tf_op jit(solution)/shard_map/ppermute | solution.py:335
  164.3 0.9 copy-start.3
  164.3 1.1 copy-start.4
  177.0 25.5 %all-to-all-start.2 = ((bf16[128,24,128]{2,1,0:T(8,128)(2,1)}), bf16[128,24,128]{2,1,0:T(8,128)(2,1)S(1)}, u32[]{:S(2)}, u32[]{:S(2)}) async-start(bf16[128,24,128]{2,1,0:T(8,128)(2,1)} %bitcast.54), calls=%async_computation.2 | async-start | bytes 1572864 | tf_op jit(solution)/shard_map/all_to_all | solution.py:404
  203.7 21.3 %all-to-all-start.1 = ((bf16[16,16,2048]{2,1,0:T(8,128)(2,1)}), bf16[16,16,2048]{2,1,0:T(8,128)(2,1)S(1)}, u32[]{:S(2)}, u32[]{:S(2)}) async-start(bf16[16,16,2048]{2,1,0:T(8,128)(2,1)} %broadcast_in_dim.30), calls=%async_computation.1 | async-start | bytes 2097152 | tf_op jit(solution)/shard_map/all_to_all | solution.py:343
  226.0 20.9 %all-to-all-start.3 = ((bf16[128,24,128]{2,1,0:T(8,128)(2,1)}), bf16[128,24,128]{2,1,0:T(8,128)(2,1)S(1)}, u32[]{:S(2)}, u32[]{:S(2)}) async-start(bf16[128,24,128]{2,1,0:T(8,128)(2,1)} %broadcast_in_dim.31), calls=%async_computation.3 | async-start | bytes 1572864 | tf_op jit(solution)/shard_map/all_to_all | solution.py:343

commit v2 on v1

--- a/solution.py
+++ b/solution.py
@@ -14,7 +14,7 @@
 BF16 = jnp.bfloat16
 BLK = 128
 PAIR = 256
-CHUNK = 24
+CHUNK = 16
 ROOT = BLK**0.5
 
 
@@ -41,6 +41,16 @@
     return centre * inverse, inverse
 
 
+def lower_of(a):
+    row = lax.broadcasted_iota(jnp.int32, a.shape, 0)
+    col = lax.broadcasted_iota(jnp.int32, a.shape, 1)
+    return jnp.where(row >= col, a, jnp.zeros_like(a))
+
+
+def upright(row):
+    return jnp.broadcast_to(row, (BLK, BLK)).T
+
+
 def columns(ref, at, first=0, count=None):
     count = ref.shape[0] if count is None else count
     return jnp.concatenate([ref[first + k, at] for k in range(count)], axis=1)
@@ -62,7 +72,7 @@
 
 
 def forward_kernel(
-    order, u_ref, v_ref, d_hbm, w_ref, bias_ref, gain_ref, shift_ref, out_ref, d_ref, go_ref, bias_at, sem
+    order, u_ref, v_ref, d_hbm, w_ref, bias_ref, gain_ref, shift_ref, out_ref, d_ref, go_ref, low_at, bias_at, sem
 ):
     blocks, length, _ = d_ref.shape
     turns = length // PAIR
@@ -87,7 +97,7 @@
                 scaled, _ = norm(gelu(v_ref[at, cols_of(g)].astype(F32)))
                 normed.append((scaled * gain + shift).astype(BF16))
             mixed = jnp.dot(
-                w_ref[0, g], jnp.concatenate(normed, axis=1), preferred_element_type=F32
+                low_at[g], jnp.concatenate(normed, axis=1), preferred_element_type=F32
             )
             for h, at in enumerate(rows):
                 upper = gelu(u_ref[at, cols_of(g)].astype(F32))
@@ -99,7 +109,8 @@
         scatter_columns(d_hbm, d_ref, sem)
 
     for g in range(2):
-        bias_at[g] = jnp.broadcast_to(bias_ref[0, :, g : g + 1], (BLK, BLK))
+        bias_at[g] = upright(bias_ref[0, g : g + 1])
+        low_at[g] = lower_of(w_ref[0, g].astype(F32)).astype(BF16)
 
     @pl.when(step == 0)
     def _():
@@ -119,7 +130,7 @@
             multiply(i)
 
 
-def forward(order, u, v, d, w_low, bias, gain, shift):
+def forward(order, u, v, d, mix, bias, gain, shift):
     n = order.shape[0]
     length, width = u.shape
     last = n - 1
@@ -135,7 +146,7 @@
                 pl.BlockSpec((length, PAIR), cur),
                 pl.BlockSpec(memory_space=pl.ANY),
                 pl.BlockSpec((1, 2, BLK, BLK), lambda j, o: (o[jnp.minimum(j, last)], 0, 0, 0)),
-                pl.BlockSpec((1, BLK, 2), par),
+                pl.BlockSpec((1, 2, BLK), par),
                 pl.BlockSpec((1, 2, BLK), par),
                 pl.BlockSpec((1, 2, BLK), par),
             ],
@@ -143,6 +154,7 @@
             scratch_shapes=[
                 pltpu.VMEM((width // BLK, length, BLK), BF16),
                 pltpu.VMEM((2, PAIR, length), BF16),
+                pltpu.VMEM((2, BLK, BLK), BF16),
                 pltpu.VMEM((2, BLK, BLK), F32),
                 pltpu.SemaphoreType.DMA,
             ],
@@ -154,16 +166,16 @@
             transcendentals=2 * n * PAIR * length,
         ),
         name="fwd",
-    )(order, u, v, d, w_low, bias, gain, shift)
+    )(order, u, v, d, mix, bias, gain, shift)
 
 
 def backward_kernel(
-    pieces, order, u_ref, v_ref, d_hbm, low_ref, lowt_ref, bias_ref, gain_ref, shift_ref, *rest
+    pieces, order, u_ref, v_ref, d_hbm, mix_ref, bias_ref, gain_ref, shift_ref, *rest
 ):
     count = len(pieces)
     w_hbm = rest[:count]
-    gu_ref, gv_ref, pack_ref = rest[-12:-9]
-    d_ref, w_ref, cot_ref, bias_at, b_acc, g_acc, s_acc, m_acc, sems = rest[-9:]
+    gu_ref, gv_ref, pack_ref = rest[-14:-11]
+    d_ref, w_ref, cot_ref, low_at, turned_at, bias_at, b_acc, g_acc, s_acc, m_acc, sems = rest[-11:]
     turns = u_ref.shape[0] // PAIR
     step = pl.program_id(0)
     last = pl.num_programs(0) - 1
@@ -202,7 +214,10 @@
                 await_all(landing(k), sems.at[k])
 
     for g in range(2):
-        bias_at[g] = jnp.broadcast_to(bias_ref[0, :, g : g + 1], (BLK, BLK))
+        lower = lower_of(mix_ref[0, g].astype(F32))
+        low_at[g] = lower.astype(BF16)
+        turned_at[g] = lower.T.astype(BF16)
+        bias_at[g] = upright(bias_ref[0, g : g + 1])
     b_acc[...] = jnp.zeros_like(b_acc)
     g_acc[...] = jnp.zeros_like(g_acc)
     s_acc[...] = jnp.zeros_like(s_acc)
@@ -222,7 +237,7 @@
                 kept.append((scaled, inverse * slope))
                 normed.append((scaled * gain + shift).astype(BF16))
             normed = jnp.concatenate(normed, axis=1)
-            mixed = jnp.dot(low_ref[0, g], normed, preferred_element_type=F32)
+            mixed = jnp.dot(low_at[g], normed, preferred_element_type=F32)
             d_mixed_b = []
             for h, at in enumerate(rows):
                 upper, slope = gelu_and_slope(u_ref[at, cols_of(g)].astype(F32))
@@ -237,7 +252,7 @@
             m_acc[g] += lax.dot_general(
                 d_mixed_b, normed, (((1,), (1,)), ((), ())), preferred_element_type=F32
             )
-            d_normed = jnp.dot(lowt_ref[0, g], d_mixed_b, preferred_element_type=F32)
+            d_normed = jnp.dot(turned_at[g], d_mixed_b, preferred_element_type=F32)
             for h, at in enumerate(rows):
                 scaled, scale = kept[h]
                 dn = d_normed[:, cols_of(h)]
@@ -249,25 +264,108 @@
                 sum_es = jnp.sum(weighted * gain, axis=-1, keepdims=True)
                 gv_ref[at, cols_of(g)] = (scale * (e - mean_e - scaled * sum_es)).astype(BF16)
 
-    row = lax.broadcasted_iota(jnp.int32, (BLK, BLK), 0)
-    col = lax.broadcasted_iota(jnp.int32, (BLK, BLK), 1)
-    filler = jnp.zeros((CHUNK - 17, BLK), F32)
     extra = []
     for g in range(2):
         extra.append(jnp.sum(b_acc[g].T, axis=0, keepdims=True))
         extra.append(ROOT * jnp.sum(g_acc[g], axis=0, keepdims=True))
         extra.append(jnp.sum(s_acc[g], axis=0, keepdims=True))
+    row = lax.broadcasted_iota(jnp.int32, (BLK, BLK), 0)
+    col = lax.broadcasted_iota(jnp.int32, (BLK, BLK), 1)
+    extra.append(jnp.sum(jnp.where(row == col, m_acc[1], 0.0), axis=0, keepdims=True))
+    both = jnp.where(row >= col, m_acc[0], m_acc[1].T)
+    filler = jnp.zeros((CHUNK - 9, BLK), F32)
+    blank = jnp.zeros((1, BLK), F32)
+    for k in range(16):
+        vector = extra[k] if k < len(extra) else blank
+        pack_ref[0, k] = jnp.concatenate(
+            [both[k * 8 : (k + 1) * 8], vector, filler], axis=0
+        ).astype(BF16)
+
+
+def unpack_kernel(x_ref, gw_ref, gb_ref, gg_ref, gs_ref):
+    pair = pl.program_id(0)
+    both = jnp.concatenate([x_ref[0, k, :8].astype(F32) for k in range(16)], axis=0)
+    vector = lambda k: x_ref[0, k].astype(F32)[8:9]
+    row = lax.broadcasted_iota(jnp.int32, (BLK, BLK), 0)
+    col = lax.broadcasted_iota(jnp.int32, (BLK, BLK), 1)
+    gw_ref[0] = jnp.where(row >= col, both, 0.0)
+    turned = both.T
+    gw_ref[1] = jnp.where(row > col, turned, jnp.where(row == col, vector(6), 0.0))
     for g in range(2):
-        lower = jnp.where(row >= col, m_acc[g], 0.0)
-        for r in range(8):
-            k = g * 8 + r
-            vector = extra[k] if k < len(extra) else jnp.zeros((1, BLK), F32)
-            pack_ref[0, k] = jnp.concatenate(
-                [lower[r * 16 : (r + 1) * 16], vector, filler], axis=0
-            ).astype(BF16)
-
-
-def backward(order, weights, u, v, d, w_low, w_low_t, bias, gain, shift, earlier):
+        at = pl.ds(2 * pair + g, 1)
+        gb_ref[at] = vector(3 * g)
+        gg_ref[at] = vector(3 * g + 1)
+        gs_ref[at] = vector(3 * g + 2)
+
+
+def unpack(total):
+    pairs = total.shape[0]
+    whole = pl.BlockSpec((2 * pairs, BLK), lambda j: (0, 0))
+    row = jax.ShapeDtypeStruct((2 * pairs, BLK), F32)
+    return pl.pallas_call(
+        unpack_kernel,
+        grid=(pairs,),
+        in_specs=[pl.BlockSpec((1, 16, CHUNK, BLK), lambda j: (j, 0, 0, 0))],
+        out_specs=[pl.BlockSpec((2, BLK, BLK), lambda j: (j, 0, 0)), whole, whole, whole],
+        out_shape=[jax.ShapeDtypeStruct((2 * pairs, BLK, BLK), F32), row, row, row],
+        cost_estimate=pl.CostEstimate(flops=10**6, bytes_accessed=10**6, transcendentals=0),
+        name="unpack",
+    )(total)
+
+
+def join_kernel(a_ref, b_ref, out_ref):
+    out_ref[...] = (a_ref[...].astype(F32) + b_ref[...].astype(F32)).astype(BF16)
+
+
+def join(a, b):
+    n, rows, width = a.shape
+    spec = pl.BlockSpec((1, rows // 2, width), lambda i, j: (i, j, 0))
+    return pl.pallas_call(
+        join_kernel,
+        grid=(n, 2),
+        in_specs=[spec, spec],
+        out_specs=spec,
+        out_shape=jax.ShapeDtypeStruct(a.shape, BF16),
+        cost_estimate=pl.CostEstimate(
+            flops=a.size, bytes_accessed=6 * a.size, transcendentals=0
+        ),
+        name="join",
+    )(a, b)
+
+
+def place_kernel(at, *refs):
+    out_ref = refs[-1]
+    for k, ref in enumerate(refs[:-1]):
+
+        @pl.when(pl.program_id(0) == k)
+        def _(ref=ref):
+            n = ref.shape[0]
+            for r in range(n):
+                out_ref[0, lax.rem(at[1] - r + n, n)] = ref[r].astype(F32)
+
+
+def place_rows(at, parts):
+    n, (m, rows, width) = len(parts), parts[0].shape
+    whole = pl.BlockSpec((m, rows, width), lambda k, at: (0, 0, 0))
+    return pl.pallas_call(
+        place_kernel,
+        grid_spec=pltpu.PrefetchScalarGridSpec(
+            num_scalar_prefetch=1,
+            grid=(n,),
+            in_specs=[whole] * n,
+            out_specs=pl.BlockSpec(
+                (1, m, rows, width), lambda k, at: (lax.rem(at[0] - k + n, n), 0, 0, 0)
+            ),
+        ),
+        out_shape=jax.ShapeDtypeStruct((n, m, rows, width), F32),
+        cost_estimate=pl.CostEstimate(
+            flops=10**6, bytes_accessed=6 * n * m * rows * width, transcendentals=0
+        ),
+        name="place",
+    )(at, *parts)
+
+
+def backward(order, weights, u, v, d, mix, bias, gain, shift):
     n = order.shape[0]
     length, width = u.shape
     pairs = width // PAIR
@@ -277,15 +375,12 @@
     mat = pl.BlockSpec((1, 2, BLK, BLK), lambda j, o: (o[j], 0, 0, 0))
     tile = pl.BlockSpec((length, PAIR), cur)
     vec = pl.BlockSpec((1, 2, BLK), par)
-    col = pl.BlockSpec((1, BLK, 2), par)
     hbm = pl.BlockSpec(memory_space=pl.ANY)
     shapes = [
         jax.ShapeDtypeStruct((length, width), BF16),
         jax.ShapeDtypeStruct((length, width), BF16),
         jax.ShapeDtypeStruct((pairs, 16, CHUNK, BLK), BF16),
     ]
-    first = 9 + len(weights)
-    alias = {first + k: k for k in range(len(earlier))}
     return pl.pallas_call(
         functools.partial(backward_kernel, pieces),
         grid_spec=pltpu.PrefetchScalarGridSpec(
@@ -296,12 +391,10 @@
                 tile,
                 hbm,
                 mat,
-                mat,
-                col,
+                vec,
                 vec,
                 vec,
                 *[hbm] * len(weights),
-                *[hbm] * len(earlier),
             ],
             out_specs=[
                 tile,
@@ -312,6 +405,8 @@
                 pltpu.VMEM((width // BLK, length, BLK), BF16),
                 pltpu.VMEM((n, width // BLK, PAIR, BLK), BF16),
                 pltpu.VMEM((2, PAIR, PAIR), F32),
+                pltpu.VMEM((2, BLK, BLK), BF16),
+                pltpu.VMEM((2, BLK, BLK), BF16),
                 pltpu.VMEM((2, BLK, BLK), F32),
                 pltpu.VMEM((2, BLK, BLK), F32),
                 pltpu.VMEM((2, 8, BLK), F32),
@@ -321,14 +416,13 @@
             ],
         ),
         out_shape=shapes,
-        input_output_aliases=alias,
         cost_estimate=pl.CostEstimate(
             flops=2 * n * PAIR * length * (width + 3 * BLK) * 2,
             bytes_accessed=length * width * 2 + n * PAIR * (8 * length + 2 * width),
             transcendentals=3 * n * PAIR * length,
         ),
         name="bwd",
-    )(order, u, v, d, w_low, w_low_t, bias, gain, shift, *[w for _, _, w in weights], *earlier)
+    )(order, u, v, d, mix, bias, gain, shift, *[w for _, _, w in weights])
 
 
 def hop(a, axis, size, by):
@@ -369,43 +463,48 @@
     near = [swap(left), swap(right)]
     far = [swap(far0), swap(far1)]
 
-    w_low = jnp.tril(w_mix)
-    w_low_t = jnp.swapaxes(w_low, 1, 2).reshape(pairs, 2, BLK, BLK)
-    w_low = w_low.reshape(pairs, 2, BLK, BLK)
-    bias = jnp.swapaxes(mix_bias.reshape(pairs, 2, BLK), 1, 2)
+    mix = w_mix.reshape(pairs, 2, BLK, BLK)
+    bias = mix_bias.reshape(pairs, 2, BLK)
     gain = norm_gain.reshape(pairs, 2, BLK)
     shift = norm_shift.reshape(pairs, 2, BLK)
 
-    common = (u, v, d, w_low, bias, gain, shift)
+    common = (u, v, d, mix, bias, gain, shift)
     theirs = forward(xs * nc + (1 - c), *common)
     ours = forward(xs * nc + c, *common)
     traded = swap(theirs)
-    joined = (ours.astype(F32) + traded.astype(F32)).astype(BF16)
+    joined = join(ours, traded)
     split = lax.all_to_all(joined.reshape(nx * plane, PAIR // plane, width), ("x", "z", "y"), 0, 0)
 
-    backs = (u, v, d, w_low, w_low_t, bias, gain, shift)
     place = lambda k, core: lax.rem(x + k, nx) * nc + core
-    order = jnp.stack([place(0, c), place(0, 1 - c)])
-    out = backward(order, [(0, 0, w_out), (1, 0, own)], *backs, ())
-    order = jnp.stack([place(3, c), place(1, c), place(3, 1 - c), place(1, 1 - c)])
-    out = backward(
-        order, [(0, 0, left), (1, 0, right), (2, 0, near[0]), (3, 0, near[1])], *backs, out
+    order = jnp.stack(
+        [place(k, core) for ks in ((0,), (nx - 1, 1), (2,)) for core in (c, 1 - c) for k in ks]
     )
-    order = jnp.stack([place(2, c), place(2, 1 - c)])
-    out = backward(
-        order, [(0, 0, far0), (0, half, far1), (1, 0, far[0]), (1, half, far[1])], *backs, out
-    )
-    grad_u, grad_v, packed = out
+    weights = [
+        (0, 0, w_out),
+        (1, 0, own),
+        (2, 0, left),
+        (3, 0, right),
+        (4, 0, near[0]),
+        (5, 0, near[1]),
+        (6, 0, far0),
+        (6, half, far1),
+        (7, 0, far[0]),
+        (7, half, far[1]),
+    ]
+    grad_u, grad_v, packed = backward(order, weights, *common)
+
     packed, split = lax.optimization_barrier((packed, split))
-    grad_w_out = spread(added(split), ("z", "y"), plane)
-    grad_w_out = grad_w_out.reshape(PAIR, width).astype(F32)
     devices = nz * ny * nx * nc
     every = ("z", "y", "x", "c")
     packed = lax.all_to_all(packed.reshape(devices, CHUNK, BLK), every, 0, 0)
+    rows = added(split)
+    column = [rows] + [hop(rows, "y", ny, k) for k in range(1, ny)]
+    column = jnp.stack(column)
+    parts = [column] + [hop(column, "z", nz, k) for k in range(1, nz)]
+    here = jnp.stack([lax.axis_index("z"), lax.axis_index("y")])
+    grad_w_out = place_rows(here, parts).reshape(PAIR, width)
     total = spread(added(packed), every, devices)
-    grad_w = total[:, :16].astype(F32).reshape(groups, BLK, BLK)
-    rest = total.reshape(pairs, 16, CHUNK, BLK)[:, :6, 16].astype(F32).reshape(groups, 3, BLK)
-    vectors = [rest[:, k] for k in range(3)]
+    grad_w, *vectors = unpack(total.reshape(pairs, 16, CHUNK, BLK))
     return (grad_u[None], grad_v[None], grad_w_out, grad_w, *vectors)
 
 

time: 250 us -> 231 us (0.924)
  other arithmetic: 18.1 us -> 4.61 us
  waiting for transfers between devices: 117 us -> 104 us
  starting transfers between devices: 37.4 us -> 43.7 us
  local copies, waits for them, and re-layouts: 8.87 us -> 3.75 us
  Pallas kernels: 67 us -> 71.9 us
    all_to_all x2 -> x1, waiting for transfers between devices: 32.1 us -> 0.01 us  [spread(): lax.all_to_all(jnp.broadcast_to(a[None], (count,) + a.shape), axes, 0, 0)]
    ppermute x10 -> x16, waiting for transfers between devices: 70.9 us -> 98.9 us  [hop(): return lax.ppermute(a, axis, [(i, (i + by) % size) for i in range(size)])]
    pallas_call x0 -> x3, Pallas kernels: none -> 16.8 us  [the longest x1 7.83 us: join(): pl.pallas_call(join_kernel, grid=(n, 2), in_specs=[spec, spec], out_specs...]
    pallas_call x3 -> x1, Pallas kernels: 40.6 us -> 28.7 us  [backward(): pl.pallas_call(functools.partial(backward_kernel, pieces), grid_spec=pltp...]
    ppermute x10 -> x16, starting transfers between devices: 7.98 us -> 18.5 us  [hop(): return lax.ppermute(a, axis, [(i, (i + by) % size) for i in range(size)])]
    convert_element_type x3 -> x0, other arithmetic: 9.34 us -> none  [the longest x1 7.7 us: everything(): joined = (ours.astype(F32) + traded.astype(F32)).astype(BF16)]
    all_to_all x1, waiting for transfers between devices: 13.5 us -> 5.53 us  [everything(): packed = lax.all_to_all(packed.reshape(devices, CHUNK, BLK), every, 0, 0)]
    all_to_all x2 -> x1, starting transfers between devices: 8.28 us -> 4.69 us  [spread(): lax.all_to_all(jnp.broadcast_to(a[None], (count,) + a.shape), axes, 0, 0)]
  transfers between devices with their start and end apart: 14 -> 19, of which waited for: 4 -> 7; matrix products, arithmetic and copies ran while one was open for 4% -> 2% of each run, Pallas kernels for 22% -> 20%
where the time goes in v2:
time: 231 us; the launch traced here: 229 us
  waiting for transfers between devices  104 us (45%)
  Pallas kernels  71.9 us (31%)
  starting transfers between devices  43.7 us (19%)
  other arithmetic  4.61 us (2%)
  local copies, waits for them, and re-layouts  3.75 us (2%)
    ppermute x16, waiting for transfers between devices, hop(): return lax.ppermute(a, axis, [(i, (i + by) % size) for i in range(size)])  98.9 us
    pallas_call x1, Pallas kernels, backward(): pl.pallas_call(functools.partial(backward_kernel, pieces), grid_spec=pltp...  28.7 us
    pallas_call x2, Pallas kernels, forward(): pl.pallas_call(forward_kernel, grid_spec=pltpu.PrefetchScalarGridSpec(num...  26.3 us
    ppermute x16, starting transfers between devices, hop(): return lax.ppermute(a, axis, [(i, (i + by) % size) for i in range(size)])  18.5 us
    all_to_all x1, starting transfers between devices, everything(): lax.all_to_all(joined.reshape(nx * plane, PAIR // plane, width), ('x', 'z...  11.9 us
    all_to_all x1, starting transfers between devices, everything(): packed = lax.all_to_all(packed.reshape(devices, CHUNK, BLK), every, 0, 0)  8.52 us
    pallas_call x1, Pallas kernels, join(): pl.pallas_call(join_kernel, grid=(n, 2), in_specs=[spec, spec], out_specs...  7.83 us
    all_to_all x1, waiting for transfers between devices, everything(): packed = lax.all_to_all(packed.reshape(devices, CHUNK, BLK), every, 0, 0)  5.53 us
  transfers between devices with their start and end apart: 19, of which 7 were waited for; matrix products, arithmetic and copies ran while one was open for 2% of the time, Pallas kernels for 20%

profile of v2, /device:TPU:0, one launch (start us, length us, event | category | flops | bytes accessed | tf_op | source)
XLA Modules:
  0.0 229.2 jit_solution(820670983378569954)
XLA Ops:
  0.6 0.5 fusion.order
  1.2 13.2 %fwd.3 = bf16[4,256,2048]{2,1,0:T(8,128)(2,1)} custom-call(s32[4]{0:T(128)} %fusion.order, bf16[1024,2048]{1,0:T(8,128)(2,1)} %bitcast.35, bf16[1024,2048]{1,0:T(8,128)(2,1)} %bitcast.38, bf16[1024,2048]{1,0:T(8,128)(2,1)} %bitcast.41, bf16[8,2,128,128]{3,2,1,0:T(8,128)(2,1)} %bitcast.44, f32[8,2,128]{2,1,0:T(2,128)} %bitcast.47, f32[8,2,128]{2,1,0:T(2,128)} %bitcast.50, ...), custom_call_target="tpu_custom_call" | custom-call | flops 9126805504 | bytes 12582912 | tf_op jit(solution)/shard_map/fwd/pallas_call | solution.py:139
  14.3 0.1 collective-permute-start.9
  14.4 0.5 fusion.1.order
  14.9 13.2 %fwd.2.a_ref = bf16[4,256,2048]{2,1,0:T(8,128)(2,1)} custom-call(s32[4]{0:T(128)} %fusion.1.order, bf16[1024,2048]{1,0:T(8,128)(2,1)} %bitcast.36, bf16[1024,2048]{1,0:T(8,128)(2,1)} %bitcast.39, bf16[1024,2048]{1,0:T(8,128)(2,1)} %bitcast.42, bf16[8,2,128,128]{3,2,1,0:T(8,128)(2,1)} %bitcast.45, f32[8,2,128]{2,1,0:T(2,128)} %bitcast.48, ...), custom_call_target="tpu_custom_call" | custom-call | flops 9126805504 | bytes 12582912 | tf_op jit(solution)/shard_map/fwd/pallas_call | solution.py:139
  28.1 7.8 %join.1 = bf16[4,256,2048]{2,1,0:T(8,128)(2,1)} custom-call(bf16[4,256,2048]{2,1,0:T(8,128)(2,1)} %fwd.2.a_ref, bf16[4,256,2048]{2,1,0:T(8,128)(2,1)} %collective-permute-done.9.b_ref), custom_call_target="tpu_custom_call" | custom-call | flops 2097152 | bytes 12582912 | tf_op jit(solution)/shard_map/join/pallas_call | solution.py:323
  36.0 11.9 %all-to-all-start = ((bf16[64,16,2048]{2,1,0:T(8,128)(2,1)}), bf16[64,16,2048]{2,1,0:T(8,128)(2,1)}, u32[]{:S(2)}, u32[]{:S(2)}) async-start(bf16[64,16,2048]{2,1,0:T(8,128)(2,1)} %bitcast.27), calls=%async_computation | async-start | bytes 8388608 | tf_op jit(solution)/shard_map/all_to_all | solution.py:476
  47.9 1.6 collective-permute-start.1
  49.5 1.7 collective-permute-start.2
  51.2 0.0 collective-permute-start
  51.2 70.9 %collective-permute-done.1.rest_2_ = bf16[256,2048]{1,0:T(8,128)(2,1)S(1)} collective-permute-done((bf16[256,2048]{1,0:T(8,128)(2,1)S(1)}, bf16[256,2048]{1,0:T(8,128)(2,1)S(1)}, u32[]{:S(2)}, u32[]{:S(2)}) %collective-permute-start.1) | collective-permute-done | bytes 1048608 | tf_op jit(solution)/shard_map/ppermute | solution.py:429
  122.2 0.1 collective-permute-start.5
  122.2 0.0 copy-start.3
  122.3 3.3 %collective-permute-start.6 = (bf16[128,2048]{1,0:T(8,128)(2,1)S(1)}, bf16[128,2048]{1,0:T(8,128)(2,1)}, u32[]{:S(2)}, u32[]{:S(2)}) collective-permute-start(bf16[128,2048]{1,0:T(8,128)(2,1)S(1)} %slice.9), channel_id=1, source_target_pairs={{0,6},{2,0},{4,2},{6,4},{1,7},{3,1},{5,3},{7,5},{8,14},{10,8},{12,... | collective-permute-start | bytes 1572872 | tf_op jit(solution)/shard_map/ppermute | solution.py:429
  125.6 0.0 collective-permute-start.3
  125.6 0.5 collective-permute-start.4
  126.1 11.1 %collective-permute-done.5.rest_6_ = bf16[128,2048]{1,0:T(8,128)(2,1)} collective-permute-done((bf16[128,2048]{1,0:T(8,128)(2,1)S(1)}, bf16[128,2048]{1,0:T(8,128)(2,1)}, u32[]{:S(2)}, u32[]{:S(2)}) %collective-permute-start.5) | collective-permute-done | bytes 524320 | tf_op jit(solution)/shard_map/ppermute | solution.py:429
  137.2 0.0 collective-permute-start.7
  137.2 0.0 collective-permute-done.6.rest_7_
  137.2 0.5 collective-permute-start.8
  137.7 0.6 stack.59.order
  138.3 0.0 collective-permute-done.rest_1_
  138.3 1.1 collective-permute-done.7.rest_8_
  139.4 0.7 collective-permute-done.8.rest_9_
  140.2 0.0 collective-permute-done.3.rest_4_
  140.2 0.0 collective-permute-done.4.rest_5_
  140.2 28.7 %bwd.1 = (bf16[1024,2048]{1,0:T(8,128)(2,1)}, bf16[1024,2048]{1,0:T(8,128)(2,1)}, bf16[8,16,16,128]{3,2,1,0:T(8,128)(2,1)}) custom-call(s32[8]{0:T(128)} %stack.59.order, bf16[1024,2048]{1,0:T(8,128)(2,1)} %bitcast.37, bf16[1024,2048]{1,0:T(8,128)(2,1)} %bitcast.40, bf16[1024,2048]{1,0:T(8,128)(2,1)} %bitcast.43, bf16[8,2,128,128]{3,2,1,0:T(8,128)(2,1)} %bitcast.46, ...), custom_call_target="tpu_custom_call" | custom-call | flops 20401094656 | bytes 29360128 | tf_op jit(solution)/shard_map/bwd/pallas_call | solution.py:384
  169.0 8.5 %all-to-all-start.1 = ((bf16[128,16,128]{2,1,0:T(8,128)(2,1)}), bf16[128,16,128]{2,1,0:T(8,128)(2,1)S(1)}, u32[]{:S(2)}, u32[]{:S(2)}) async-start(bf16[128,16,128]{2,1,0:T(8,128)(2,1)} %bitcast.30), calls=%async_computation.1 | async-start | bytes 1048576 | tf_op jit(solution)/shard_map/all_to_all | solution.py:499
  177.5 2.8 %convert_reduce_fusion = bf16[16,2048]{1,0:T(8,128)(2,1)S(1)} fusion(bf16[64,16,2048]{2,1,0:T(8,128)(2,1)} %all-to-all-done), kind=kLoop, calls=%fused_computation | loop fusion | flops 4161536 | bytes 4259840 | tf_op jit(solution)/shard_map/reduce_sum | solution.py:433
  180.3 1.0 collective-permute-start.10
  181.3 2.7 %collective-permute-start.11 = (bf16[16,2048]{1,0:T(8,128)(2,1)S(1)}, bf16[16,2048]{1,0:T(8,128)(2,1)S(1)}, u32[]{:S(2)}, u32[]{:S(2)}) collective-permute-start(bf16[16,2048]{1,0:T(8,128)(2,1)S(1)} %convert_reduce_fusion), channel_id=1, source_target_pairs={{0,16},{8,24},{16,0},{24,8},{1,17},{9,25},{17,1},{25,9},{2,18},{10... | collective-permute-start | bytes 196616 | tf_op jit(solution)/shard_map/ppermute | solution.py:429
  184.1 1.4 collective-permute-start.12
  185.5 5.5 %all-to-all-done.1 = bf16[128,16,128]{2,1,0:T(8,128)(2,1)S(1)} async-done(((bf16[128,16,128]{2,1,0:T(8,128)(2,1)}), bf16[128,16,128]{2,1,0:T(8,128)(2,1)S(1)}, u32[]{:S(2)}, u32[]{:S(2)}) %all-to-all-start.1) | async-done | bytes 524320 | tf_op jit(solution)/shard_map/all_to_all | solution.py:499
  191.0 0.1 convert_reduce_fusion.1
  191.1 0.9 broadcast_in_dim.14
  192.0 4.7 %all-to-all-start.2 = ((bf16[128,16,128]{2,1,0:T(8,128)(2,1)}), bf16[128,16,128]{2,1,0:T(8,128)(2,1)S(1)}, u32[]{:S(2)}, u32[]{:S(2)}) async-start(bf16[128,16,128]{2,1,0:T(8,128)(2,1)} %broadcast_in_dim.14), calls=%async_computation.2 | async-start | bytes 1048576 | tf_op jit(solution)/shard_map/all_to_all | solution.py:437
  196.7 0.0 collective-permute-done.10
  196.8 1.1 collective-permute-start.13
  197.9 3.2 %collective-permute-start.14 = (bf16[4,16,2048]{2,1,0:T(8,128)(2,1)S(1)}, bf16[4,16,2048]{2,1,0:T(8,128)(2,1)S(1)}, u32[]{:S(2)}, u32[]{:S(2)}) collective-permute-start(bf16[4,16,2048]{2,1,0:T(8,128)(2,1)S(1)} %pad_maximum_fusion.refs_0_), channel_id=1, source_target_pairs={{0,64},{32,96},{64,0},{96,32},{1,65},{33,97},{65,1},{97,33},{2,66}... | collective-permute-start | bytes 786440 | tf_op jit(solution)/shard_map/ppermute | solution.py:429
  201.2 1.2 collective-permute-start.15
  202.4 0.6 pad_add_fusion.at
  202.9 8.7 %collective-permute-done.13.refs_1_ = bf16[4,16,2048]{2,1,0:T(8,128)(2,1)S(1)} collective-permute-done((bf16[4,16,2048]{2,1,0:T(8,128)(2,1)S(1)}, bf16[4,16,2048]{2,1,0:T(8,128)(2,1)S(1)}, u32[]{:S(2)}, u32[]{:S(2)}) %collective-permute-start.13) | collective-permute-done | bytes 262176 | tf_op jit(solution)/shard_map/ppermute | solution.py:429
  211.6 6.4 %collective-permute-done.14.refs_2_ = bf16[4,16,2048]{2,1,0:T(8,128)(2,1)S(1)} collective-permute-done((bf16[4,16,2048]{2,1,0:T(8,128)(2,1)S(1)}, bf16[4,16,2048]{2,1,0:T(8,128)(2,1)S(1)}, u32[]{:S(2)}, u32[]{:S(2)}) %collective-permute-start.14) | collective-permute-done | bytes 262176 | tf_op jit(solution)/shard_map/ppermute | solution.py:429
  218.0 0.7 copy-done.5
  218.7 0.7 copy-done.6
  219.4 3.8 %place.1 = f32[4,4,16,2048]{3,2,1,0:T(8,128)} custom-call(s32[2]{0:T(128)} %pad_add_fusion.at, bf16[4,16,2048]{2,1,0:T(8,128)(2,1)} %copy-done.1, bf16[4,16,2048]{2,1,0:T(8,128)(2,1)} %copy-done.4, bf16[4,16,2048]{2,1,0:T(8,128)(2,1)} %copy-done.5, bf16[4,16,2048]{2,1,0:T(8,128)(2,1)} %copy-done.6), custom_call_target="tpu_custom_call" | custom-call | flops 1000000 | bytes 3145728 | tf_op jit(solution)/shard_map/place/pallas_call | solution.py:350
  223.2 0.8 copy-done
  224.0 5.2 %unpack.1 = (f32[16,128,128]{2,1,0:T(8,128)}, f32[16,128]{1,0:T(8,128)}, f32[16,128]{1,0:T(8,128)}, f32[16,128]{1,0:T(8,128)}) custom-call(bf16[8,16,16,128]{3,2,1,0:T(8,128)(2,1)} %bitcast.29), custom_call_target="tpu_custom_call" | custom-call | flops 1000000 | bytes 1000000 | tf_op jit(solution)/shard_map/unpack/pallas_call | solution.py:305
  (22 shorter events, 0.2 us)
Async XLA Ops:
  14.3 13.8 %collective-permute-start.9 = (bf16[4,256,2048]{2,1,0:T(8,128)(2,1)}, bf16[4,256,2048]{2,1,0:T(8,128)(2,1)}, u32[]{:S(2)}, u32[]{:S(2)}) collective-permute-start(bf16[4,256,2048]{2,1,0:T(8,128)(2,1)} %fwd.3), channel_id=1, source_target_pairs={{0,1},{1,0},{2,3},{3,2},{4,5},{5,4},{6,7},{7,6},{8,9},{9,8},{10,11... | collective-permute-start | bytes 12582920 | tf_op jit(solution)/shard_map/ppermute | solution.py:429
  36.0 12.0 %copy-start.7 = (bf16[256,2048]{1,0:T(8,128)(2,1)S(1)}, bf16[256,2048]{1,0:T(8,128)(2,1)}, u32[]{:S(2)}) copy-start(bf16[256,2048]{1,0:T(8,128)(2,1)} %rest_0_.1) | copy-start | bytes 3145732
  36.0 133.0 %all-to-all-start = ((bf16[64,16,2048]{2,1,0:T(8,128)(2,1)}), bf16[64,16,2048]{2,1,0:T(8,128)(2,1)}, u32[]{:S(2)}, u32[]{:S(2)}) async-start(bf16[64,16,2048]{2,1,0:T(8,128)(2,1)} %bitcast.27), calls=%async_computation | async-start | bytes 8388608 | tf_op jit(solution)/shard_map/all_to_all | solution.py:476
  47.9 74.2 %collective-permute-start.1 = (bf16[256,2048]{1,0:T(8,128)(2,1)S(1)}, bf16[256,2048]{1,0:T(8,128)(2,1)S(1)}, u32[]{:S(2)}, u32[]{:S(2)}) collective-permute-start(bf16[256,2048]{1,0:T(8,128)(2,1)S(1)} %copy-done.7), channel_id=1, source_target_pairs={{0,2},{2,4},{4,6},{6,0},{1,3},{3,5},{5,7},{7,1},{8,10},{10,12},{12... | collective-permute-start | bytes 3145736 | tf_op jit(solution)/shard_map/ppermute | solution.py:429
  49.5 72.7 %collective-permute-start.2 = (bf16[256,2048]{1,0:T(8,128)(2,1)S(1)}, bf16[256,2048]{1,0:T(8,128)(2,1)S(1)}, u32[]{:S(2)}, u32[]{:S(2)}) collective-permute-start(bf16[256,2048]{1,0:T(8,128)(2,1)S(1)} %copy-done.7), channel_id=1, source_target_pairs={{0,6},{2,0},{4,2},{6,4},{1,7},{3,1},{5,3},{7,5},{8,14},{10,8},{12,... | collective-permute-start | bytes 3145736 | tf_op jit(solution)/shard_map/ppermute | solution.py:429
  51.2 87.1 %collective-permute-start = (bf16[256,2048]{1,0:T(8,128)(2,1)S(1)}, bf16[256,2048]{1,0:T(8,128)(2,1)}, u32[]{:S(2)}, u32[]{:S(2)}) collective-permute-start(bf16[256,2048]{1,0:T(8,128)(2,1)S(1)} %copy-done.7), channel_id=1, source_target_pairs={{0,1},{1,0},{2,3},{3,2},{4,5},{5,4},{6,7},{7,6},{8,9},{9,8},{10,11... | collective-permute-start | bytes 3145736 | tf_op jit(solution)/shard_map/ppermute | solution.py:429
  122.1 18.1 %copy-start.2 = (bf16[256,2048]{1,0:T(8,128)(2,1)}, bf16[256,2048]{1,0:T(8,128)(2,1)S(1)}, u32[]{:S(2)}) copy-start(bf16[256,2048]{1,0:T(8,128)(2,1)S(1)} %collective-permute-done.1.rest_2_) | copy-start | bytes 3145732
  122.2 15.0 %collective-permute-start.5 = (bf16[128,2048]{1,0:T(8,128)(2,1)S(1)}, bf16[128,2048]{1,0:T(8,128)(2,1)}, u32[]{:S(2)}, u32[]{:S(2)}) collective-permute-start(bf16[128,2048]{1,0:T(8,128)(2,1)S(1)} %slice.8), channel_id=1, source_target_pairs={{0,2},{2,4},{4,6},{6,0},{1,3},{3,5},{5,7},{7,1},{8,10},{10,12},{12... | collective-permute-start | bytes 1572872 | tf_op jit(solution)/shard_map/ppermute | solution.py:429
  122.2 18.0 %copy-start.3 = (bf16[256,2048]{1,0:T(8,128)(2,1)}, bf16[256,2048]{1,0:T(8,128)(2,1)S(1)}, u32[]{:S(2)}) copy-start(bf16[256,2048]{1,0:T(8,128)(2,1)S(1)} %collective-permute-done.2.rest_3_) | copy-start | bytes 3145732
  122.3 14.9 %collective-permute-start.6 = (bf16[128,2048]{1,0:T(8,128)(2,1)S(1)}, bf16[128,2048]{1,0:T(8,128)(2,1)}, u32[]{:S(2)}, u32[]{:S(2)}) collective-permute-start(bf16[128,2048]{1,0:T(8,128)(2,1)S(1)} %slice.9), channel_id=1, source_target_pairs={{0,6},{2,0},{4,2},{6,4},{1,7},{3,1},{5,3},{7,5},{8,14},{10,8},{12,... | collective-permute-start | bytes 1572872 | tf_op jit(solution)/shard_map/ppermute | solution.py:429
  125.6 14.6 %collective-permute-start.3 = (bf16[256,2048]{1,0:T(8,128)(2,1)S(1)}, bf16[256,2048]{1,0:T(8,128)(2,1)}, u32[]{:S(2)}, u32[]{:S(2)}) collective-permute-start(bf16[256,2048]{1,0:T(8,128)(2,1)S(1)} %collective-permute-done.1.rest_2_), channel_id=1, source_target_pairs={{0,1},{1,0},{2,3},{3,2},{4,5},{5,4},{6,7},{7,6},{8,9},{9,8},{10,11... | collective-permute-start | bytes 3145736 | tf_op jit(solution)/shard_map/ppermute | solution.py:429
  125.6 14.6 %collective-permute-start.4 = (bf16[256,2048]{1,0:T(8,128)(2,1)S(1)}, bf16[256,2048]{1,0:T(8,128)(2,1)}, u32[]{:S(2)}, u32[]{:S(2)}) collective-permute-start(bf16[256,2048]{1,0:T(8,128)(2,1)S(1)} %collective-permute-done.2.rest_3_), channel_id=1, source_target_pairs={{0,1},{1,0},{2,3},{3,2},{4,5},{5,4},{6,7},{7,6},{8,9},{9,8},{10,11... | collective-permute-start | bytes 3145736 | tf_op jit(solution)/shard_map/ppermute | solution.py:429
  137.2 2.3 collective-permute-start.7
  137.2 3.0 %collective-permute-start.8 = (bf16[128,2048]{1,0:T(8,128)(2,1)}, bf16[128,2048]{1,0:T(8,128)(2,1)}, u32[]{:S(2)}, u32[]{:S(2)}) collective-permute-start(bf16[128,2048]{1,0:T(8,128)(2,1)} %collective-permute-done.6.rest_7_), channel_id=1, source_target_pairs={{0,1},{1,0},{2,3},{3,2},{4,5},{5,4},{6,7},{7,6},{8,9},{9,8},{10,11... | collective-permute-start | bytes 1572872 | tf_op jit(solution)/shard_map/ppermute | solution.py:429
  169.0 22.1 %all-to-all-start.1 = ((bf16[128,16,128]{2,1,0:T(8,128)(2,1)}), bf16[128,16,128]{2,1,0:T(8,128)(2,1)S(1)}, u32[]{:S(2)}, u32[]{:S(2)}) async-start(bf16[128,16,128]{2,1,0:T(8,128)(2,1)} %bitcast.30), calls=%async_computation.1 | async-start | bytes 1048576 | tf_op jit(solution)/shard_map/all_to_all | solution.py:499
  180.3 16.4 %collective-permute-start.10 = (bf16[16,2048]{1,0:T(8,128)(2,1)S(1)}, bf16[16,2048]{1,0:T(8,128)(2,1)S(1)}, u32[]{:S(2)}, u32[]{:S(2)}) collective-permute-start(bf16[16,2048]{1,0:T(8,128)(2,1)S(1)} %convert_reduce_fusion), channel_id=1, source_target_pairs={{0,8},{8,16},{16,24},{24,0},{1,9},{9,17},{17,25},{25,1},{2,10},{10... | collective-permute-start | bytes 196616 | tf_op jit(solution)/shard_map/ppermute | solution.py:429
  181.3 15.4 %collective-permute-start.11 = (bf16[16,2048]{1,0:T(8,128)(2,1)S(1)}, bf16[16,2048]{1,0:T(8,128)(2,1)S(1)}, u32[]{:S(2)}, u32[]{:S(2)}) collective-permute-start(bf16[16,2048]{1,0:T(8,128)(2,1)S(1)} %convert_reduce_fusion), channel_id=1, source_target_pairs={{0,16},{8,24},{16,0},{24,8},{1,17},{9,25},{17,1},{25,9},{2,18},{10... | collective-permute-start | bytes 196616 | tf_op jit(solution)/shard_map/ppermute | solution.py:429
  184.1 12.7 %collective-permute-start.12 = (bf16[16,2048]{1,0:T(8,128)(2,1)S(1)}, bf16[16,2048]{1,0:T(8,128)(2,1)S(1)}, u32[]{:S(2)}, u32[]{:S(2)}) collective-permute-start(bf16[16,2048]{1,0:T(8,128)(2,1)S(1)} %convert_reduce_fusion), channel_id=1, source_target_pairs={{0,24},{8,0},{16,8},{24,16},{1,25},{9,1},{17,9},{25,17},{2,26},{10... | collective-permute-start | bytes 196616 | tf_op jit(solution)/shard_map/ppermute | solution.py:429
  192.0 31.1 %all-to-all-start.2 = ((bf16[128,16,128]{2,1,0:T(8,128)(2,1)}), bf16[128,16,128]{2,1,0:T(8,128)(2,1)S(1)}, u32[]{:S(2)}, u32[]{:S(2)}) async-start(bf16[128,16,128]{2,1,0:T(8,128)(2,1)} %broadcast_in_dim.14), calls=%async_computation.2 | async-start | bytes 1048576 | tf_op jit(solution)/shard_map/all_to_all | solution.py:437
  196.8 21.2 %copy-start.1 = (bf16[4,16,2048]{2,1,0:T(8,128)(2,1)}, bf16[4,16,2048]{2,1,0:T(8,128)(2,1)S(1)}, u32[]{:S(2)}) copy-start(bf16[4,16,2048]{2,1,0:T(8,128)(2,1)S(1)} %pad_maximum_fusion.refs_0_) | copy-start | bytes 786436
  196.8 14.8 %collective-permute-start.13 = (bf16[4,16,2048]{2,1,0:T(8,128)(2,1)S(1)}, bf16[4,16,2048]{2,1,0:T(8,128)(2,1)S(1)}, u32[]{:S(2)}, u32[]{:S(2)}) collective-permute-start(bf16[4,16,2048]{2,1,0:T(8,128)(2,1)S(1)} %pad_maximum_fusion.refs_0_), channel_id=1, source_target_pairs={{0,32},{32,64},{64,96},{96,0},{1,33},{33,65},{65,97},{97,1},{2,34}... | collective-permute-start | bytes 786440 | tf_op jit(solution)/shard_map/ppermute | solution.py:429
  197.9 20.1 %collective-permute-start.14 = (bf16[4,16,2048]{2,1,0:T(8,128)(2,1)S(1)}, bf16[4,16,2048]{2,1,0:T(8,128)(2,1)S(1)}, u32[]{:S(2)}, u32[]{:S(2)}) collective-permute-start(bf16[4,16,2048]{2,1,0:T(8,128)(2,1)S(1)} %pad_maximum_fusion.refs_0_), channel_id=1, source_target_pairs={{0,64},{32,96},{64,0},{96,32},{1,65},{33,97},{65,1},{97,33},{2,66}... | collective-permute-start | bytes 786440 | tf_op jit(solution)/shard_map/ppermute | solution.py:429
  201.2 16.8 %collective-permute-start.15 = (bf16[4,16,2048]{2,1,0:T(8,128)(2,1)S(1)}, bf16[4,16,2048]{2,1,0:T(8,128)(2,1)S(1)}, u32[]{:S(2)}, u32[]{:S(2)}) collective-permute-start(bf16[4,16,2048]{2,1,0:T(8,128)(2,1)S(1)} %pad_maximum_fusion.refs_0_), channel_id=1, source_target_pairs={{0,96},{32,0},{64,32},{96,64},{1,97},{33,1},{65,33},{97,65},{2,98}... | collective-permute-start | bytes 786440 | tf_op jit(solution)/shard_map/ppermute | solution.py:429
  211.6 6.4 %copy-start.4 = (bf16[4,16,2048]{2,1,0:T(8,128)(2,1)}, bf16[4,16,2048]{2,1,0:T(8,128)(2,1)S(1)}, u32[]{:S(2)}) copy-start(bf16[4,16,2048]{2,1,0:T(8,128)(2,1)S(1)} %collective-permute-done.13.refs_1_) | copy-start | bytes 786436
  218.0 0.7 copy-start.5
  218.7 0.7 copy-start.6
  223.2 0.8 copy-start

commit v3 on v2

--- a/solution.py
+++ b/solution.py
@@ -283,54 +283,74 @@
 
 
 def unpack_kernel(x_ref, gw_ref, gb_ref, gg_ref, gs_ref):
-    pair = pl.program_id(0)
-    both = jnp.concatenate([x_ref[0, k, :8].astype(F32) for k in range(16)], axis=0)
-    vector = lambda k: x_ref[0, k].astype(F32)[8:9]
+    chunks, pairs = x_ref.shape[:2]
     row = lax.broadcasted_iota(jnp.int32, (BLK, BLK), 0)
     col = lax.broadcasted_iota(jnp.int32, (BLK, BLK), 1)
-    gw_ref[0] = jnp.where(row >= col, both, 0.0)
-    turned = both.T
-    gw_ref[1] = jnp.where(row > col, turned, jnp.where(row == col, vector(6), 0.0))
-    for g in range(2):
-        at = pl.ds(2 * pair + g, 1)
-        gb_ref[at] = vector(3 * g)
-        gg_ref[at] = vector(3 * g + 1)
-        gs_ref[at] = vector(3 * g + 2)
+
+    @pl.loop(0, pairs)
+    def _(pair):
+        part = [x_ref[k, pair].astype(F32) for k in range(chunks)]
+        both = jnp.concatenate([p[:8] for p in part], axis=0)
+        vector = lambda k: part[k][8:9]
+        gw_ref[2 * pair] = jnp.where(row >= col, both, 0.0)
+        gw_ref[2 * pair + 1] = jnp.where(
+            row > col, both.T, jnp.where(row == col, vector(6), 0.0)
+        )
+        for g in range(2):
+            at = pl.ds(2 * pair + g, 1)
+            gb_ref[at] = vector(3 * g)
+            gg_ref[at] = vector(3 * g + 1)
+            gs_ref[at] = vector(3 * g + 2)
 
 
 def unpack(total):
-    pairs = total.shape[0]
-    whole = pl.BlockSpec((2 * pairs, BLK), lambda j: (0, 0))
+    pairs = total.shape[1]
     row = jax.ShapeDtypeStruct((2 * pairs, BLK), F32)
     return pl.pallas_call(
         unpack_kernel,
-        grid=(pairs,),
-        in_specs=[pl.BlockSpec((1, 16, CHUNK, BLK), lambda j: (j, 0, 0, 0))],
-        out_specs=[pl.BlockSpec((2, BLK, BLK), lambda j: (j, 0, 0)), whole, whole, whole],
         out_shape=[jax.ShapeDtypeStruct((2 * pairs, BLK, BLK), F32), row, row, row],
         cost_estimate=pl.CostEstimate(flops=10**6, bytes_accessed=10**6, transcendentals=0),
         name="unpack",
     )(total)
 
 
-def join_kernel(a_ref, b_ref, out_ref):
-    out_ref[...] = (a_ref[...].astype(F32) + b_ref[...].astype(F32)).astype(BF16)
+def join_kernel(a_hbm, b_hbm, out_hbm, a_ref, b_ref, out_ref, sems):
+    count = a_hbm.shape[0]
+    hbm = (a_hbm, b_hbm, out_hbm)
+    vmem = (a_ref, b_ref, out_ref)
+    read = lambda s, k: pltpu.make_async_copy(hbm[s].at[k], vmem[s].at[k], sems.at[s, k])
+    write = lambda k: pltpu.make_async_copy(out_ref.at[k], out_hbm.at[k], sems.at[2, k])
+
+    for k in range(count):
+        read(0, k).start()
+        read(1, k).start()
+
+    @pl.loop(0, count)
+    def _(k):
+        read(0, k).wait()
+        read(1, k).wait()
+        out_ref[k] = (a_ref[k].astype(F32) + b_ref[k].astype(F32)).astype(BF16)
+        write(k).start()
+
+    for k in range(count):
+        write(k).wait()
 
 
 def join(a, b):
     n, rows, width = a.shape
-    spec = pl.BlockSpec((1, rows // 2, width), lambda i, j: (i, j, 0))
+    parts = (4 * n, rows // 4, width)
+    hbm = pl.BlockSpec(memory_space=pl.ANY)
     return pl.pallas_call(
         join_kernel,
-        grid=(n, 2),
-        in_specs=[spec, spec],
-        out_specs=spec,
-        out_shape=jax.ShapeDtypeStruct(a.shape, BF16),
+        in_specs=[hbm, hbm],
+        out_specs=hbm,
+        out_shape=jax.ShapeDtypeStruct(parts, BF16),
+        scratch_shapes=[pltpu.VMEM(parts, BF16)] * 3 + [pltpu.SemaphoreType.DMA((3, 4 * n))],
         cost_estimate=pl.CostEstimate(
             flops=a.size, bytes_accessed=6 * a.size, transcendentals=0
         ),
         name="join",
-    )(a, b)
+    )(a.reshape(parts), b.reshape(parts)).reshape(a.shape)
 
 
 def place_kernel(at, *refs):
@@ -399,7 +419,7 @@
             out_specs=[
                 tile,
                 tile,
-                pl.BlockSpec((1, 16, CHUNK, BLK), lambda j, o: (o[j], 0, 0, 0)),
+                pl.BlockSpec((1, 16, CHUNK, BLK), lambda j, o: (j, 0, 0, 0)),
             ],
             scratch_shapes=[
                 pltpu.VMEM((width // BLK, length, BLK), BF16),
@@ -476,35 +496,41 @@
     split = lax.all_to_all(joined.reshape(nx * plane, PAIR // plane, width), ("x", "z", "y"), 0, 0)
 
     place = lambda k, core: lax.rem(x + k, nx) * nc + core
-    order = jnp.stack(
-        [place(k, core) for ks in ((0,), (nx - 1, 1), (2,)) for core in (c, 1 - c) for k in ks]
-    )
+    hops = (0, nx - 1, 1, 2)
+    order = jnp.stack([place(k, core) for core in (1 - c, c) for k in hops])
     weights = [
-        (0, 0, w_out),
-        (1, 0, own),
-        (2, 0, left),
-        (3, 0, right),
-        (4, 0, near[0]),
-        (5, 0, near[1]),
-        (6, 0, far0),
-        (6, half, far1),
-        (7, 0, far[0]),
-        (7, half, far[1]),
+        (0, 0, own),
+        (1, 0, near[0]),
+        (2, 0, near[1]),
+        (3, 0, far[0]),
+        (3, half, far[1]),
+        (4, 0, w_out),
+        (5, 0, left),
+        (6, 0, right),
+        (7, 0, far0),
+        (7, half, far1),
     ]
     grad_u, grad_v, packed = backward(order, weights, *common)
 
-    packed, split = lax.optimization_barrier((packed, split))
+    mine = packed[nx:].astype(F32) + swap(packed[:nx]).astype(F32)
+    mine = lax.optimization_barrier(mine).astype(BF16)
+    arrived = [hop(mine[1], "x", nx, -1), hop(mine[2], "x", nx, 1), hop(mine[3], "x", nx, 2)]
+    ours = mine[0].astype(F32)
+    for a in arrived:
+        ours = ours + a.astype(F32)
+    ours = lax.optimization_barrier(ours).astype(BF16)
+
+    ours, split = lax.optimization_barrier((ours, split))
     devices = nz * ny * nx * nc
-    every = ("z", "y", "x", "c")
-    packed = lax.all_to_all(packed.reshape(devices, CHUNK, BLK), every, 0, 0)
     rows = added(split)
     column = [rows] + [hop(rows, "y", ny, k) for k in range(1, ny)]
     column = jnp.stack(column)
     parts = [column] + [hop(column, "z", nz, k) for k in range(1, nz)]
     here = jnp.stack([lax.axis_index("z"), lax.axis_index("y")])
     grad_w_out = place_rows(here, parts).reshape(PAIR, width)
-    total = spread(added(packed), every, devices)
-    grad_w, *vectors = unpack(total.reshape(pairs, 16, CHUNK, BLK))
+    ours = lax.all_to_all(ours, ("z", "y"), 0, 0)
+    total = spread(added(ours), ("z", "y", "x", "c"), devices)
+    grad_w, *vectors = unpack(total.reshape(plane, pairs, CHUNK, BLK))
     return (grad_u[None], grad_v[None], grad_w_out, grad_w, *vectors)
 
 

time: 231 us -> 210 us (0.909)
  waiting for transfers between devices: 104 us -> 80.6 us
  starting transfers between devices: 43.7 us -> 49.3 us
  Pallas kernels: 71.9 us -> 67.4 us
    ppermute x16 -> x20, waiting for transfers between devices: 98.9 us -> 80.6 us  [hop(): return lax.ppermute(a, axis, [(i, (i + by) % size) for i in range(size)])]
    all_to_all x1, waiting for transfers between devices: 5.53 us -> 0.01 us  [everything(): ours = lax.all_to_all(ours, ('z', 'y'), 0, 0)]
    ppermute x16 -> x20, starting transfers between devices: 18.5 us -> 23.7 us  [hop(): return lax.ppermute(a, axis, [(i, (i + by) % size) for i in range(size)])]
    pallas_call x2, Pallas kernels: 13.1 us -> 8.42 us  [the longest x1 5.58 us: join(): pl.pallas_call(join_kernel, in_specs=[hbm, hbm], out_specs=hbm, out_shape...]
  transfers between devices with their start and end apart: 19 -> 23, of which waited for: 7 -> 9; matrix products, arithmetic and copies ran while one was open for 2% -> 4% of each run, Pallas kernels for 20% -> 24%
where the time goes in v3:
time: 210 us; the launch traced here: 209 us
  waiting for transfers between devices  80.6 us (38%)
  Pallas kernels  67.4 us (32%)
  starting transfers between devices  49.3 us (23%)
  other arithmetic  6.17 us (3%)
  local copies, waits for them, and re-layouts  4.83 us (2%)
    ppermute x20, waiting for transfers between devices, hop(): return lax.ppermute(a, axis, [(i, (i + by) % size) for i in range(size)])  80.6 us
    pallas_call x1, Pallas kernels, backward(): pl.pallas_call(functools.partial(backward_kernel, pieces), grid_spec=pltp...  28.7 us
    pallas_call x2, Pallas kernels, forward(): pl.pallas_call(forward_kernel, grid_spec=pltpu.PrefetchScalarGridSpec(num...  26.5 us
    ppermute x20, starting transfers between devices, hop(): return lax.ppermute(a, axis, [(i, (i + by) % size) for i in range(size)])  23.7 us
    all_to_all x1, starting transfers between devices, everything(): lax.all_to_all(joined.reshape(nx * plane, PAIR // plane, width), ('x', 'z...  10.6 us
    all_to_all x1, starting transfers between devices, everything(): ours = lax.all_to_all(ours, ('z', 'y'), 0, 0)  9 us
    all_to_all x1, starting transfers between devices, spread(): lax.all_to_all(jnp.broadcast_to(a[None], (count,) + a.shape), axes, 0, 0)  6.02 us
    pallas_call x1, Pallas kernels, join(): pl.pallas_call(join_kernel, in_specs=[hbm, hbm], out_specs=hbm, out_shape...  5.58 us
  transfers between devices with their start and end apart: 23, of which 9 were waited for; matrix products, arithmetic and copies ran while one was open for 4% of the time, Pallas kernels for 24%

profile of v3, /device:TPU:0, one launch (start us, length us, event | category | flops | bytes accessed | tf_op | source)
XLA Modules:
  0.0 209.2 jit_solution(16062544807841345828)
XLA Ops:
  0.6 0.5 fusion.2.order
  1.2 13.3 %fwd.3 = bf16[4,256,2048]{2,1,0:T(8,128)(2,1)} custom-call(s32[4]{0:T(128)} %fusion.2.order, bf16[1024,2048]{1,0:T(8,128)(2,1)} %bitcast.47, bf16[1024,2048]{1,0:T(8,128)(2,1)} %bitcast.50, bf16[1024,2048]{1,0:T(8,128)(2,1)} %bitcast.53, bf16[8,2,128,128]{3,2,1,0:T(8,128)(2,1)} %bitcast.56, f32[8,2,128]{2,1,0:T(2,128)} %bitcast.59, f32[8,2,128]{2,1,0:T(2,128)} %bitcast.62, ...), custom_call_target="tpu_custom_call" | custom-call | flops 9126805504 | bytes 12582912 | tf_op jit(solution)/shard_map/fwd/pallas_call | solution.py:139
  14.5 0.1 collective-permute-start.13
  14.6 1.6 collective-permute-start.1
  16.2 1.7 collective-permute-start.3
  17.9 0.5 fusion.3.order
  18.4 13.2 %fwd.2 = bf16[4,256,2048]{2,1,0:T(8,128)(2,1)} custom-call(s32[4]{0:T(128)} %fusion.3.order, bf16[1024,2048]{1,0:T(8,128)(2,1)} %bitcast.48, bf16[1024,2048]{1,0:T(8,128)(2,1)} %bitcast.51, bf16[1024,2048]{1,0:T(8,128)(2,1)} %bitcast.54, bf16[8,2,128,128]{3,2,1,0:T(8,128)(2,1)} %bitcast.57, f32[8,2,128]{2,1,0:T(2,128)} %bitcast.60, f32[8,2,128]{2,1,0:T(2,128)} %bitcast.63, ...), custom_call_target="tpu_custom_call" | custom-call | flops 9126805504 | bytes 12582912 | tf_op jit(solution)/shard_map/fwd/pallas_call | solution.py:139
  31.6 5.6 %join.1 = bf16[16,64,2048]{2,1,0:T(8,128)(2,1)} custom-call(bf16[16,64,2048]{2,1,0:T(8,128)(2,1)} %bitcast.40, bf16[16,64,2048]{2,1,0:T(8,128)(2,1)} %bitcast.24.b_hbm), custom_call_target="tpu_custom_call" | custom-call | flops 2097152 | bytes 12582912 | tf_op jit(solution)/shard_map/join/pallas_call | solution.py:343
  37.2 10.6 %all-to-all-start = ((bf16[64,16,2048]{2,1,0:T(8,128)(2,1)}), bf16[64,16,2048]{2,1,0:T(8,128)(2,1)}, u32[]{:S(2)}, u32[]{:S(2)}) async-start(bf16[64,16,2048]{2,1,0:T(8,128)(2,1)} %bitcast.39), calls=%async_computation | async-start | bytes 8388608 | tf_op jit(solution)/shard_map/all_to_all | solution.py:496
  47.8 0.1 collective-permute-start
  47.9 1.6 collective-permute-start.5
  49.5 1.8 collective-permute-start.7
  51.3 0.5 collective-permute-start.4
  51.8 58.4 %collective-permute-done.5.rest_8_ = bf16[128,2048]{1,0:T(8,128)(2,1)} collective-permute-done((bf16[128,2048]{1,0:T(8,128)(2,1)S(1)}, bf16[128,2048]{1,0:T(8,128)(2,1)}, u32[]{:S(2)}, u32[]{:S(2)}) %collective-permute-start.5) | collective-permute-done | bytes 524320 | tf_op jit(solution)/shard_map/ppermute | solution.py:449
  110.3 0.5 collective-permute-start.8
  110.8 0.7 stack.59.order
  111.5 1.1 collective-permute-done.6.rest_3_
  112.5 0.7 collective-permute-done.8.rest_4_
  113.3 28.7 %bwd.1 = (bf16[1024,2048]{1,0:T(8,128)(2,1)}, bf16[1024,2048]{1,0:T(8,128)(2,1)}, bf16[8,16,16,128]{3,2,1,0:T(8,128)(2,1)}) custom-call(s32[8]{0:T(128)} %stack.59.order, bf16[1024,2048]{1,0:T(8,128)(2,1)} %bitcast.49, bf16[1024,2048]{1,0:T(8,128)(2,1)} %bitcast.52, bf16[1024,2048]{1,0:T(8,128)(2,1)} %bitcast.55, bf16[8,2,128,128]{3,2,1,0:T(8,128)(2,1)} %bitcast.58, ...), custom_call_target="tpu_custom_call" | custom-call | flops 20401094656 | bytes 29360128 | tf_op jit(solution)/shard_map/bwd/pallas_call | solution.py:404
  142.0 1.0 slice.27
  143.0 0.2 collective-permute-start.9
  143.2 1.4 collective-permute-done.9
  144.6 1.0 convert_add_fusion
  145.6 0.1 collective-permute-start.10
  145.7 2.0 collective-permute-start.11
  147.7 1.9 collective-permute-start.12
  149.6 0.3 collective-permute-done.10
  150.0 1.3 collective-permute-done.11
  151.3 2.2 %collective-permute-done.12 = bf16[16,16,128]{2,1,0:T(8,128)(2,1)S(1)} collective-permute-done((bf16[16,16,128]{2,1,0:T(8,128)(2,1)S(1)}, bf16[16,16,128]{2,1,0:T(8,128)(2,1)S(1)}, u32[]{:S(2)}, u32[]{:S(2)}) %collective-permute-start.12) | collective-permute-done | bytes 65568 | tf_op jit(solution)/shard_map/ppermute | solution.py:449
  153.5 0.7 fusion.1
  154.2 9.0 %all-to-all-start.1 = ((bf16[16,16,128]{2,1,0:T(8,128)(2,1)}), bf16[16,16,128]{2,1,0:T(8,128)(2,1)S(1)}, u32[]{:S(2)}, u32[]{:S(2)}) async-start(bf16[16,16,128]{2,1,0:T(8,128)(2,1)} %fusion.1), calls=%async_computation.1 | async-start | bytes 131072 | tf_op jit(solution)/shard_map/all_to_all | solution.py:531
  163.2 2.8 %convert_reduce_fusion = bf16[16,2048]{1,0:T(8,128)(2,1)S(1)} fusion(bf16[64,16,2048]{2,1,0:T(8,128)(2,1)} %all-to-all-done), kind=kLoop, calls=%fused_computation | loop fusion | flops 4161536 | bytes 4259840 | tf_op jit(solution)/shard_map/reduce_sum | solution.py:453
  166.0 2.0 collective-permute-start.14
  168.0 2.7 %collective-permute-start.15 = (bf16[16,2048]{1,0:T(8,128)(2,1)S(1)}, bf16[16,2048]{1,0:T(8,128)(2,1)S(1)}, u32[]{:S(2)}, u32[]{:S(2)}) collective-permute-start(bf16[16,2048]{1,0:T(8,128)(2,1)S(1)} %convert_reduce_fusion), channel_id=1, source_target_pairs={{0,16},{8,24},{16,0},{24,8},{1,17},{9,25},{17,1},{25,9},{2,18},{10... | collective-permute-start | bytes 196616 | tf_op jit(solution)/shard_map/ppermute | solution.py:449
  170.7 1.5 collective-permute-start.16
  172.2 0.9 broadcast_in_dim.14
  173.0 6.0 %all-to-all-start.2 = ((bf16[128,16,128]{2,1,0:T(8,128)(2,1)}), bf16[128,16,128]{2,1,0:T(8,128)(2,1)S(1)}, u32[]{:S(2)}, u32[]{:S(2)}) async-start(bf16[128,16,128]{2,1,0:T(8,128)(2,1)} %broadcast_in_dim.14), calls=%async_computation.2 | async-start | bytes 1048576 | tf_op jit(solution)/shard_map/all_to_all | solution.py:457
  179.1 1.1 collective-permute-start.17
  180.3 3.2 %collective-permute-start.18 = (bf16[4,16,2048]{2,1,0:T(8,128)(2,1)S(1)}, bf16[4,16,2048]{2,1,0:T(8,128)(2,1)S(1)}, u32[]{:S(2)}, u32[]{:S(2)}) collective-permute-start(bf16[4,16,2048]{2,1,0:T(8,128)(2,1)S(1)} %pad_maximum_fusion.refs_0_), channel_id=1, source_target_pairs={{0,64},{32,96},{64,0},{96,32},{1,65},{33,97},{65,1},{97,33},{2,66}... | collective-permute-start | bytes 786440 | tf_op jit(solution)/shard_map/ppermute | solution.py:449
  183.5 1.2 collective-permute-start.19
  184.7 0.6 pad_add_fusion.at
  185.3 8.7 %collective-permute-done.17.refs_1_ = bf16[4,16,2048]{2,1,0:T(8,128)(2,1)S(1)} collective-permute-done((bf16[4,16,2048]{2,1,0:T(8,128)(2,1)S(1)}, bf16[4,16,2048]{2,1,0:T(8,128)(2,1)S(1)}, u32[]{:S(2)}, u32[]{:S(2)}) %collective-permute-start.17) | collective-permute-done | bytes 262176 | tf_op jit(solution)/shard_map/ppermute | solution.py:449
  194.0 6.4 %collective-permute-done.18.refs_2_ = bf16[4,16,2048]{2,1,0:T(8,128)(2,1)S(1)} collective-permute-done((bf16[4,16,2048]{2,1,0:T(8,128)(2,1)S(1)}, bf16[4,16,2048]{2,1,0:T(8,128)(2,1)S(1)}, u32[]{:S(2)}, u32[]{:S(2)}) %collective-permute-start.18) | collective-permute-done | bytes 262176 | tf_op jit(solution)/shard_map/ppermute | solution.py:449
  200.4 0.7 copy-done.5
  201.1 0.7 copy-done.6
  201.8 3.8 %place.1 = f32[4,4,16,2048]{3,2,1,0:T(8,128)} custom-call(s32[2]{0:T(128)} %pad_add_fusion.at, bf16[4,16,2048]{2,1,0:T(8,128)(2,1)} %copy-done.1, bf16[4,16,2048]{2,1,0:T(8,128)(2,1)} %copy-done.4, bf16[4,16,2048]{2,1,0:T(8,128)(2,1)} %copy-done.5, bf16[4,16,2048]{2,1,0:T(8,128)(2,1)} %copy-done.6), custom_call_target="tpu_custom_call" | custom-call | flops 1000000 | bytes 3145728 | tf_op jit(solution)/shard_map/place/pallas_call | solution.py:370
  205.5 0.8 copy-done
  206.4 2.8 %unpack.1 = (f32[16,128,128]{2,1,0:T(8,128)}, f32[16,128]{1,0:T(8,128)}, f32[16,128]{1,0:T(8,128)}, f32[16,128]{1,0:T(8,128)}) custom-call(bf16[16,8,16,128]{3,2,1,0:T(8,128)(2,1)} %bitcast.42), custom_call_target="tpu_custom_call" | custom-call | flops 1000000 | bytes 1000000 | tf_op jit(solution)/shard_map/unpack/pallas_call | solution.py:309
  (34 shorter events, 0.2 us)
Async XLA Ops:
  1.2 13.4 %copy-start.7 = (bf16[256,2048]{1,0:T(8,128)(2,1)S(1)}, bf16[256,2048]{1,0:T(8,128)(2,1)}, u32[]{:S(2)}) copy-start(bf16[256,2048]{1,0:T(8,128)(2,1)} %rest_5_.1) | copy-start | bytes 3145732
  14.5 17.1 %collective-permute-start.13 = (bf16[4,256,2048]{2,1,0:T(8,128)(2,1)}, bf16[4,256,2048]{2,1,0:T(8,128)(2,1)}, u32[]{:S(2)}, u32[]{:S(2)}) collective-permute-start(bf16[4,256,2048]{2,1,0:T(8,128)(2,1)} %fwd.3), channel_id=1, source_target_pairs={{0,1},{1,0},{2,3},{3,2},{4,5},{5,4},{6,7},{7,6},{8,9},{9,8},{10,11... | collective-permute-start | bytes 12582920 | tf_op jit(solution)/shard_map/ppermute | solution.py:449
  14.6 33.3 %collective-permute-start.1 = (bf16[256,2048]{1,0:T(8,128)(2,1)S(1)}, bf16[256,2048]{1,0:T(8,128)(2,1)S(1)}, u32[]{:S(2)}, u32[]{:S(2)}) collective-permute-start(bf16[256,2048]{1,0:T(8,128)(2,1)S(1)} %copy-done.7), channel_id=1, source_target_pairs={{0,2},{2,4},{4,6},{6,0},{1,3},{3,5},{5,7},{7,1},{8,10},{10,12},{12... | collective-permute-start | bytes 3145736 | tf_op jit(solution)/shard_map/ppermute | solution.py:449
  16.2 33.3 %collective-permute-start.3 = (bf16[256,2048]{1,0:T(8,128)(2,1)S(1)}, bf16[256,2048]{1,0:T(8,128)(2,1)S(1)}, u32[]{:S(2)}, u32[]{:S(2)}) collective-permute-start(bf16[256,2048]{1,0:T(8,128)(2,1)S(1)} %copy-done.7), channel_id=1, source_target_pairs={{0,6},{2,0},{4,2},{6,4},{1,7},{3,1},{5,3},{7,5},{8,14},{10,8},{12,... | collective-permute-start | bytes 3145736 | tf_op jit(solution)/shard_map/ppermute | solution.py:449
  37.2 117.0 %all-to-all-start = ((bf16[64,16,2048]{2,1,0:T(8,128)(2,1)}), bf16[64,16,2048]{2,1,0:T(8,128)(2,1)}, u32[]{:S(2)}, u32[]{:S(2)}) async-start(bf16[64,16,2048]{2,1,0:T(8,128)(2,1)} %bitcast.39), calls=%async_computation | async-start | bytes 8388608 | tf_op jit(solution)/shard_map/all_to_all | solution.py:496
  47.8 63.7 %collective-permute-start = (bf16[256,2048]{1,0:T(8,128)(2,1)S(1)}, bf16[256,2048]{1,0:T(8,128)(2,1)}, u32[]{:S(2)}, u32[]{:S(2)}) collective-permute-start(bf16[256,2048]{1,0:T(8,128)(2,1)S(1)} %copy-done.7), channel_id=1, source_target_pairs={{0,1},{1,0},{2,3},{3,2},{4,5},{5,4},{6,7},{7,6},{8,9},{9,8},{10,11... | collective-permute-start | bytes 3145736 | tf_op jit(solution)/shard_map/ppermute | solution.py:449
  47.9 65.4 %copy-start.2 = (bf16[256,2048]{1,0:T(8,128)(2,1)}, bf16[256,2048]{1,0:T(8,128)(2,1)S(1)}, u32[]{:S(2)}) copy-start(bf16[256,2048]{1,0:T(8,128)(2,1)S(1)} %collective-permute-done.1.rest_6_) | copy-start | bytes 3145732
  47.9 62.4 %collective-permute-start.5 = (bf16[128,2048]{1,0:T(8,128)(2,1)S(1)}, bf16[128,2048]{1,0:T(8,128)(2,1)}, u32[]{:S(2)}, u32[]{:S(2)}) collective-permute-start(bf16[128,2048]{1,0:T(8,128)(2,1)S(1)} %slice.32), channel_id=1, source_target_pairs={{0,2},{2,4},{4,6},{6,0},{1,3},{3,5},{5,7},{7,1},{8,10},{10,12},{12... | collective-permute-start | bytes 1572872 | tf_op jit(solution)/shard_map/ppermute | solution.py:449
  49.5 63.8 %copy-start.3 = (bf16[256,2048]{1,0:T(8,128)(2,1)}, bf16[256,2048]{1,0:T(8,128)(2,1)S(1)}, u32[]{:S(2)}) copy-start(bf16[256,2048]{1,0:T(8,128)(2,1)S(1)} %collective-permute-done.3.rest_7_) | copy-start | bytes 3145732
  49.5 60.8 %collective-permute-start.7 = (bf16[128,2048]{1,0:T(8,128)(2,1)S(1)}, bf16[128,2048]{1,0:T(8,128)(2,1)}, u32[]{:S(2)}, u32[]{:S(2)}) collective-permute-start(bf16[128,2048]{1,0:T(8,128)(2,1)S(1)} %slice.33), channel_id=1, source_target_pairs={{0,6},{2,0},{4,2},{6,4},{1,7},{3,1},{5,3},{7,5},{8,14},{10,8},{12,... | collective-permute-start | bytes 1572872 | tf_op jit(solution)/shard_map/ppermute | solution.py:449
  51.3 62.0 %collective-permute-start.2 = (bf16[256,2048]{1,0:T(8,128)(2,1)S(1)}, bf16[256,2048]{1,0:T(8,128)(2,1)}, u32[]{:S(2)}, u32[]{:S(2)}) collective-permute-start(bf16[256,2048]{1,0:T(8,128)(2,1)S(1)} %collective-permute-done.1.rest_6_), channel_id=1, source_target_pairs={{0,1},{1,0},{2,3},{3,2},{4,5},{5,4},{6,7},{7,6},{8,9},{9,8},{10,11... | collective-permute-start | bytes 3145736 | tf_op jit(solution)/shard_map/ppermute | solution.py:449
  51.3 62.0 %collective-permute-start.4 = (bf16[256,2048]{1,0:T(8,128)(2,1)S(1)}, bf16[256,2048]{1,0:T(8,128)(2,1)}, u32[]{:S(2)}, u32[]{:S(2)}) collective-permute-start(bf16[256,2048]{1,0:T(8,128)(2,1)S(1)} %collective-permute-done.3.rest_7_), channel_id=1, source_target_pairs={{0,1},{1,0},{2,3},{3,2},{4,5},{5,4},{6,7},{7,6},{8,9},{9,8},{10,11... | collective-permute-start | bytes 3145736 | tf_op jit(solution)/shard_map/ppermute | solution.py:449
  110.3 2.3 %collective-permute-start.6 = (bf16[128,2048]{1,0:T(8,128)(2,1)}, bf16[128,2048]{1,0:T(8,128)(2,1)}, u32[]{:S(2)}, u32[]{:S(2)}) collective-permute-start(bf16[128,2048]{1,0:T(8,128)(2,1)} %collective-permute-done.5.rest_8_), channel_id=1, source_target_pairs={{0,1},{1,0},{2,3},{3,2},{4,5},{5,4},{6,7},{7,6},{8,9},{9,8},{10,11... | collective-permute-start | bytes 1572872 | tf_op jit(solution)/shard_map/ppermute | solution.py:449
  110.3 3.0 %collective-permute-start.8 = (bf16[128,2048]{1,0:T(8,128)(2,1)}, bf16[128,2048]{1,0:T(8,128)(2,1)}, u32[]{:S(2)}, u32[]{:S(2)}) collective-permute-start(bf16[128,2048]{1,0:T(8,128)(2,1)} %collective-permute-done.7.rest_9_), channel_id=1, source_target_pairs={{0,1},{1,0},{2,3},{3,2},{4,5},{5,4},{6,7},{7,6},{8,9},{9,8},{10,11... | collective-permute-start | bytes 1572872 | tf_op jit(solution)/shard_map/ppermute | solution.py:449
  143.0 1.6 collective-permute-start.9
  145.6 4.3 %collective-permute-start.10 = (bf16[16,16,128]{2,1,0:T(8,128)(2,1)S(1)}, bf16[16,16,128]{2,1,0:T(8,128)(2,1)S(1)}, u32[]{:S(2)}, u32[]{:S(2)}) collective-permute-start(bf16[16,16,128]{2,1,0:T(8,128)(2,1)S(1)} %get-tuple-element.25), channel_id=1, source_target_pairs={{0,6},{2,0},{4,2},{6,4},{1,7},{3,1},{5,3},{7,5},{8,14},{10,8},{12,... | collective-permute-start | bytes 196616 | tf_op jit(solution)/shard_map/ppermute | solution.py:449
  145.7 5.5 %collective-permute-start.11 = (bf16[16,16,128]{2,1,0:T(8,128)(2,1)S(1)}, bf16[16,16,128]{2,1,0:T(8,128)(2,1)S(1)}, u32[]{:S(2)}, u32[]{:S(2)}) collective-permute-start(bf16[16,16,128]{2,1,0:T(8,128)(2,1)S(1)} %get-tuple-element.26), channel_id=1, source_target_pairs={{0,2},{2,4},{4,6},{6,0},{1,3},{3,5},{5,7},{7,1},{8,10},{10,12},{12... | collective-permute-start | bytes 196616 | tf_op jit(solution)/shard_map/ppermute | solution.py:449
  147.7 5.8 %collective-permute-start.12 = (bf16[16,16,128]{2,1,0:T(8,128)(2,1)S(1)}, bf16[16,16,128]{2,1,0:T(8,128)(2,1)S(1)}, u32[]{:S(2)}, u32[]{:S(2)}) collective-permute-start(bf16[16,16,128]{2,1,0:T(8,128)(2,1)S(1)} %get-tuple-element.27), channel_id=1, source_target_pairs={{0,4},{2,6},{4,0},{6,2},{1,5},{3,7},{5,1},{7,3},{8,12},{10,14},{12... | collective-permute-start | bytes 196616 | tf_op jit(solution)/shard_map/ppermute | solution.py:449
  154.2 18.0 %all-to-all-start.1 = ((bf16[16,16,128]{2,1,0:T(8,128)(2,1)}), bf16[16,16,128]{2,1,0:T(8,128)(2,1)S(1)}, u32[]{:S(2)}, u32[]{:S(2)}) async-start(bf16[16,16,128]{2,1,0:T(8,128)(2,1)} %fusion.1), calls=%async_computation.1 | async-start | bytes 131072 | tf_op jit(solution)/shard_map/all_to_all | solution.py:531
  166.0 13.1 %collective-permute-start.14 = (bf16[16,2048]{1,0:T(8,128)(2,1)S(1)}, bf16[16,2048]{1,0:T(8,128)(2,1)S(1)}, u32[]{:S(2)}, u32[]{:S(2)}) collective-permute-start(bf16[16,2048]{1,0:T(8,128)(2,1)S(1)} %convert_reduce_fusion), channel_id=1, source_target_pairs={{0,8},{8,16},{16,24},{24,0},{1,9},{9,17},{17,25},{25,1},{2,10},{10... | collective-permute-start | bytes 196616 | tf_op jit(solution)/shard_map/ppermute | solution.py:449
  168.0 11.1 %collective-permute-start.15 = (bf16[16,2048]{1,0:T(8,128)(2,1)S(1)}, bf16[16,2048]{1,0:T(8,128)(2,1)S(1)}, u32[]{:S(2)}, u32[]{:S(2)}) collective-permute-start(bf16[16,2048]{1,0:T(8,128)(2,1)S(1)} %convert_reduce_fusion), channel_id=1, source_target_pairs={{0,16},{8,24},{16,0},{24,8},{1,17},{9,25},{17,1},{25,9},{2,18},{10... | collective-permute-start | bytes 196616 | tf_op jit(solution)/shard_map/ppermute | solution.py:449
  170.7 8.4 %collective-permute-start.16 = (bf16[16,2048]{1,0:T(8,128)(2,1)S(1)}, bf16[16,2048]{1,0:T(8,128)(2,1)S(1)}, u32[]{:S(2)}, u32[]{:S(2)}) collective-permute-start(bf16[16,2048]{1,0:T(8,128)(2,1)S(1)} %convert_reduce_fusion), channel_id=1, source_target_pairs={{0,24},{8,0},{16,8},{24,16},{1,25},{9,1},{17,9},{25,17},{2,26},{10... | collective-permute-start | bytes 196616 | tf_op jit(solution)/shard_map/ppermute | solution.py:449
  173.0 32.5 %all-to-all-start.2 = ((bf16[128,16,128]{2,1,0:T(8,128)(2,1)}), bf16[128,16,128]{2,1,0:T(8,128)(2,1)S(1)}, u32[]{:S(2)}, u32[]{:S(2)}) async-start(bf16[128,16,128]{2,1,0:T(8,128)(2,1)} %broadcast_in_dim.14), calls=%async_computation.2 | async-start | bytes 1048576 | tf_op jit(solution)/shard_map/all_to_all | solution.py:457
  179.1 21.2 %copy-start.1 = (bf16[4,16,2048]{2,1,0:T(8,128)(2,1)}, bf16[4,16,2048]{2,1,0:T(8,128)(2,1)S(1)}, u32[]{:S(2)}) copy-start(bf16[4,16,2048]{2,1,0:T(8,128)(2,1)S(1)} %pad_maximum_fusion.refs_0_) | copy-start | bytes 786436
  179.1 14.8 %collective-permute-start.17 = (bf16[4,16,2048]{2,1,0:T(8,128)(2,1)S(1)}, bf16[4,16,2048]{2,1,0:T(8,128)(2,1)S(1)}, u32[]{:S(2)}, u32[]{:S(2)}) collective-permute-start(bf16[4,16,2048]{2,1,0:T(8,128)(2,1)S(1)} %pad_maximum_fusion.refs_0_), channel_id=1, source_target_pairs={{0,32},{32,64},{64,96},{96,0},{1,33},{33,65},{65,97},{97,1},{2,34}... | collective-permute-start | bytes 786440 | tf_op jit(solution)/shard_map/ppermute | solution.py:449
  180.3 20.1 %collective-permute-start.18 = (bf16[4,16,2048]{2,1,0:T(8,128)(2,1)S(1)}, bf16[4,16,2048]{2,1,0:T(8,128)(2,1)S(1)}, u32[]{:S(2)}, u32[]{:S(2)}) collective-permute-start(bf16[4,16,2048]{2,1,0:T(8,128)(2,1)S(1)} %pad_maximum_fusion.refs_0_), channel_id=1, source_target_pairs={{0,64},{32,96},{64,0},{96,32},{1,65},{33,97},{65,1},{97,33},{2,66}... | collective-permute-start | bytes 786440 | tf_op jit(solution)/shard_map/ppermute | solution.py:449
  183.5 16.8 %collective-permute-start.19 = (bf16[4,16,2048]{2,1,0:T(8,128)(2,1)S(1)}, bf16[4,16,2048]{2,1,0:T(8,128)(2,1)S(1)}, u32[]{:S(2)}, u32[]{:S(2)}) collective-permute-start(bf16[4,16,2048]{2,1,0:T(8,128)(2,1)S(1)} %pad_maximum_fusion.refs_0_), channel_id=1, source_target_pairs={{0,96},{32,0},{64,32},{96,64},{1,97},{33,1},{65,33},{97,65},{2,98}... | collective-permute-start | bytes 786440 | tf_op jit(solution)/shard_map/ppermute | solution.py:449
  194.0 6.4 %copy-start.4 = (bf16[4,16,2048]{2,1,0:T(8,128)(2,1)}, bf16[4,16,2048]{2,1,0:T(8,128)(2,1)S(1)}, u32[]{:S(2)}) copy-start(bf16[4,16,2048]{2,1,0:T(8,128)(2,1)S(1)} %collective-permute-done.17.refs_1_) | copy-start | bytes 786436
  200.4 0.7 copy-start.5
  201.1 0.7 copy-start.6
  205.5 0.8 copy-start

commit v4 on v3

--- a/solution.py
+++ b/solution.py
@@ -351,38 +351,6 @@
         ),
         name="join",
     )(a.reshape(parts), b.reshape(parts)).reshape(a.shape)
-
-
-def place_kernel(at, *refs):
-    out_ref = refs[-1]
-    for k, ref in enumerate(refs[:-1]):
-
-        @pl.when(pl.program_id(0) == k)
-        def _(ref=ref):
-            n = ref.shape[0]
-            for r in range(n):
-                out_ref[0, lax.rem(at[1] - r + n, n)] = ref[r].astype(F32)
-
-
-def place_rows(at, parts):
-    n, (m, rows, width) = len(parts), parts[0].shape
-    whole = pl.BlockSpec((m, rows, width), lambda k, at: (0, 0, 0))
-    return pl.pallas_call(
-        place_kernel,
-        grid_spec=pltpu.PrefetchScalarGridSpec(
-            num_scalar_prefetch=1,
-            grid=(n,),
-            in_specs=[whole] * n,
-            out_specs=pl.BlockSpec(
-                (1, m, rows, width), lambda k, at: (lax.rem(at[0] - k + n, n), 0, 0, 0)
-            ),
-        ),
-        out_shape=jax.ShapeDtypeStruct((n, m, rows, width), F32),
-        cost_estimate=pl.CostEstimate(
-            flops=10**6, bytes_accessed=6 * n * m * rows * width, transcendentals=0
-        ),
-        name="place",
-    )(at, *parts)
 
 
 def backward(order, weights, u, v, d, mix, bias, gain, shift):
@@ -523,13 +491,10 @@
     ours, split = lax.optimization_barrier((ours, split))
     devices = nz * ny * nx * nc
     rows = added(split)
-    column = [rows] + [hop(rows, "y", ny, k) for k in range(1, ny)]
-    column = jnp.stack(column)
-    parts = [column] + [hop(column, "z", nz, k) for k in range(1, nz)]
-    here = jnp.stack([lax.axis_index("z"), lax.axis_index("y")])
-    grad_w_out = place_rows(here, parts).reshape(PAIR, width)
-    ours = lax.all_to_all(ours, ("z", "y"), 0, 0)
-    total = spread(added(ours), ("z", "y", "x", "c"), devices)
+    both = jnp.concatenate([jnp.broadcast_to(rows[None], (plane,) + rows.shape), ours], axis=2)
+    both = lax.all_to_all(both, ("z", "y"), 0, 0)
+    total = spread(added(both[:, :, width:]), ("z", "y", "x", "c"), devices)
+    grad_w_out = both[:, :, :width].astype(F32).reshape(PAIR, width)
     grad_w, *vectors = unpack(total.reshape(plane, pairs, CHUNK, BLK))
     return (grad_u[None], grad_v[None], grad_w_out, grad_w, *vectors)
 

time: 210 us -> 206 us (0.981)
  blocking collectives: 0 us -> 25.7 us
  starting transfers between devices: 49.3 us -> 27.7 us
  Pallas kernels: 67.4 us -> 63.6 us
  waiting for transfers between devices: 80.6 us -> 77.3 us
    all_to_all x0 -> x1, blocking collectives: none -> 25.7 us  [everything(): both = lax.all_to_all(both, ('z', 'y'), 0, 0)]
    ppermute x20 -> x14, waiting for transfers between devices: 80.6 us -> 65.5 us  [hop(): return lax.ppermute(a, axis, [(i, (i + by) % size) for i in range(size)])]
    all_to_all x1, waiting for transfers between devices: 0.01 us -> 11.7 us  [spread(): lax.all_to_all(jnp.broadcast_to(a[None], (count,) + a.shape), axes, 0, 0)]
    ppermute x20 -> x14, starting transfers between devices: 23.7 us -> 12.1 us  [hop(): return lax.ppermute(a, axis, [(i, (i + by) % size) for i in range(size)])]
    all_to_all x1 -> x0, starting transfers between devices: 9 us -> none  [everything(): ours = lax.all_to_all(ours, ('z', 'y'), 0, 0)]
    pallas_call x1 -> x0, Pallas kernels: 3.75 us -> none  [place_rows(): pl.pallas_call(place_kernel, grid_spec=pltpu.PrefetchScalarGridSpec(num_s...]
  transfers between devices with their start and end apart: 23 -> 16, of which waited for: 9 -> 8; matrix products, arithmetic and copies ran while one was open for 4% -> 2% of each run, Pallas kernels for 24% -> 23%
where the time goes in v4:
time: 206 us; the launch traced here: 205 us
  waiting for transfers between devices  77.3 us (38%)
  Pallas kernels  63.6 us (31%)
  starting transfers between devices  27.7 us (13%)
  blocking collectives  25.7 us (12%)
  other arithmetic  6.65 us (3%)
  local copies, waits for them, and re-layouts  3.62 us (2%)
    ppermute x14, waiting for transfers between devices, hop(): return lax.ppermute(a, axis, [(i, (i + by) % size) for i in range(size)])  65.5 us
    pallas_call x1, Pallas kernels, backward(): pl.pallas_call(functools.partial(backward_kernel, pieces), grid_spec=pltp...  28.7 us
    pallas_call x2, Pallas kernels, forward(): pl.pallas_call(forward_kernel, grid_spec=pltpu.PrefetchScalarGridSpec(num...  26.5 us
    all_to_all x1, blocking collectives, everything(): both = lax.all_to_all(both, ('z', 'y'), 0, 0)  25.7 us
    ppermute x14, starting transfers between devices, hop(): return lax.ppermute(a, axis, [(i, (i + by) % size) for i in range(size)])  12.1 us
    all_to_all x1, waiting for transfers between devices, spread(): lax.all_to_all(jnp.broadcast_to(a[None], (count,) + a.shape), axes, 0, 0)  11.7 us
    all_to_all x1, starting transfers between devices, everything(): lax.all_to_all(joined.reshape(nx * plane, PAIR // plane, width), ('x', 'z...  10.6 us
    pallas_call x1, Pallas kernels, join(): pl.pallas_call(join_kernel, in_specs=[hbm, hbm], out_specs=hbm, out_shape...  5.58 us
  transfers between devices with their start and end apart: 16, of which 8 were waited for; matrix products, arithmetic and copies ran while one was open for 2% of the time, Pallas kernels for 23%

profile of v4, /device:TPU:0, one launch (start us, length us, event | category | flops | bytes accessed | tf_op | source)
XLA Modules:
  0.0 205.4 jit_solution(851255127395637466)
XLA Ops:
  0.6 0.5 fusion.2.order
  1.2 13.3 %fwd.3 = bf16[4,256,2048]{2,1,0:T(8,128)(2,1)} custom-call(s32[4]{0:T(128)} %fusion.2.order, bf16[1024,2048]{1,0:T(8,128)(2,1)} %bitcast.38, bf16[1024,2048]{1,0:T(8,128)(2,1)} %bitcast.41, bf16[1024,2048]{1,0:T(8,128)(2,1)} %bitcast.44, bf16[8,2,128,128]{3,2,1,0:T(8,128)(2,1)} %bitcast.47, f32[8,2,128]{2,1,0:T(2,128)} %bitcast.50, f32[8,2,128]{2,1,0:T(2,128)} %bitcast.53, ...), custom_call_target="tpu_custom_call" | custom-call | flops 9126805504 | bytes 12582912 | tf_op jit(solution)/shard_map/fwd/pallas_call | solution.py:139
  14.5 0.1 collective-permute-start.13
  14.6 1.6 collective-permute-start.1
  16.2 1.7 collective-permute-start.3
  17.9 0.5 fusion.3.order
  18.4 13.2 %fwd.2 = bf16[4,256,2048]{2,1,0:T(8,128)(2,1)} custom-call(s32[4]{0:T(128)} %fusion.3.order, bf16[1024,2048]{1,0:T(8,128)(2,1)} %bitcast.39, bf16[1024,2048]{1,0:T(8,128)(2,1)} %bitcast.42, bf16[1024,2048]{1,0:T(8,128)(2,1)} %bitcast.45, bf16[8,2,128,128]{3,2,1,0:T(8,128)(2,1)} %bitcast.48, f32[8,2,128]{2,1,0:T(2,128)} %bitcast.51, f32[8,2,128]{2,1,0:T(2,128)} %bitcast.54, ...), custom_call_target="tpu_custom_call" | custom-call | flops 9126805504 | bytes 12582912 | tf_op jit(solution)/shard_map/fwd/pallas_call | solution.py:139
  31.6 0.0 collective-permute-done.13
  31.6 5.6 %join.1 = bf16[16,64,2048]{2,1,0:T(8,128)(2,1)} custom-call(bf16[16,64,2048]{2,1,0:T(8,128)(2,1)} %bitcast.36, bf16[16,64,2048]{2,1,0:T(8,128)(2,1)} %bitcast.22.b_hbm), custom_call_target="tpu_custom_call" | custom-call | flops 2097152 | bytes 12582912 | tf_op jit(solution)/shard_map/join/pallas_call | solution.py:343
  37.2 10.6 %all-to-all-start = ((bf16[64,16,2048]{2,1,0:T(8,128)(2,1)}), bf16[64,16,2048]{2,1,0:T(8,128)(2,1)}, u32[]{:S(2)}, u32[]{:S(2)}) async-start(bf16[64,16,2048]{2,1,0:T(8,128)(2,1)} %bitcast.35), calls=%async_computation | async-start | bytes 8388608 | tf_op jit(solution)/shard_map/all_to_all | solution.py:464
  47.7 0.1 collective-permute-start
  47.8 0.0 collective-permute-done.1.rest_6_
  47.9 0.0 copy-start.1
  47.9 1.6 collective-permute-start.5
  49.5 0.0 collective-permute-done.3.rest_7_
  49.5 1.8 collective-permute-start.7
  51.3 0.0 collective-permute-start.2
  51.3 0.5 collective-permute-start.4
  51.8 58.4 %collective-permute-done.5.rest_8_ = bf16[128,2048]{1,0:T(8,128)(2,1)} collective-permute-done((bf16[128,2048]{1,0:T(8,128)(2,1)S(1)}, bf16[128,2048]{1,0:T(8,128)(2,1)}, u32[]{:S(2)}, u32[]{:S(2)}) %collective-permute-start.5) | collective-permute-done | bytes 524320 | tf_op jit(solution)/shard_map/ppermute | solution.py:417
  110.3 0.0 collective-permute-start.6
  110.3 0.0 collective-permute-done.7.rest_9_
  110.3 0.5 collective-permute-start.8
  110.8 0.7 stack.35.order
  111.5 0.0 collective-permute-done.rest_0_
  111.5 1.1 collective-permute-done.6.rest_3_
  112.5 0.7 collective-permute-done.8.rest_4_
  113.3 28.7 %bwd.1 = (bf16[1024,2048]{1,0:T(8,128)(2,1)}, bf16[1024,2048]{1,0:T(8,128)(2,1)}, bf16[8,16,16,128]{3,2,1,0:T(8,128)(2,1)}) custom-call(s32[8]{0:T(128)} %stack.35.order, bf16[1024,2048]{1,0:T(8,128)(2,1)} %bitcast.40, bf16[1024,2048]{1,0:T(8,128)(2,1)} %bitcast.43, bf16[1024,2048]{1,0:T(8,128)(2,1)} %bitcast.46, bf16[8,2,128,128]{3,2,1,0:T(8,128)(2,1)} %bitcast.49, ...), custom_call_target="tpu_custom_call" | custom-call | flops 20401094656 | bytes 29360128 | tf_op jit(solution)/shard_map/bwd/pallas_call | solution.py:372
  142.0 1.0 slice.33
  143.0 0.2 collective-permute-start.9
  143.2 1.4 collective-permute-done.9
  144.6 1.0 convert_add_fusion
  145.6 0.1 collective-permute-start.10
  145.7 2.0 collective-permute-start.11
  147.7 1.9 collective-permute-start.12
  149.6 0.3 collective-permute-done.10
  150.0 1.3 collective-permute-done.11
  151.3 2.2 %collective-permute-done.12 = bf16[16,16,128]{2,1,0:T(8,128)(2,1)S(1)} collective-permute-done((bf16[16,16,128]{2,1,0:T(8,128)(2,1)S(1)}, bf16[16,16,128]{2,1,0:T(8,128)(2,1)S(1)}, u32[]{:S(2)}, u32[]{:S(2)}) %collective-permute-start.12) | collective-permute-done | bytes 65568 | tf_op jit(solution)/shard_map/ppermute | solution.py:417
  153.6 2.8 %convert_reduce_fusion = bf16[16,2048]{1,0:T(8,128)(2,1)S(1)} fusion(bf16[64,16,2048]{2,1,0:T(8,128)(2,1)} %all-to-all-done), kind=kLoop, calls=%fused_computation | loop fusion | flops 4161536 | bytes 4259840 | tf_op jit(solution)/shard_map/reduce_sum | solution.py:421
  156.4 0.1 broadcast_in_dim.20
  156.5 0.1 pad_maximum_fusion
  156.6 25.7 %all_to_all.15 = bf16[16,16,2176]{2,1,0:T(8,128)(2,1)S(1)} all-to-all(bf16[16,16,2176]{2,1,0:T(8,128)(2,1)S(1)} %pad_maximum_fusion), channel_id=1, replica_groups=mesh['z'=4,'y'=4,'x'=4,'c'=2] {'z','y'}, dimensions={0} | all-to-all | bytes 2228224 | tf_op jit(solution)/shard_map/all_to_all | solution.py:495
  182.3 0.9 broadcast_in_dim.21
  183.2 5.1 %all-to-all-start.2 = ((bf16[128,16,128]{2,1,0:T(8,128)(2,1)}), bf16[128,16,128]{2,1,0:T(8,128)(2,1)S(1)}, u32[]{:S(2)}, u32[]{:S(2)}) async-start(bf16[128,16,128]{2,1,0:T(8,128)(2,1)} %broadcast_in_dim.21), calls=%async_computation.2 | async-start | bytes 1048576 | tf_op jit(solution)/shard_map/all_to_all | solution.py:425
  188.3 0.1 slice.46
  188.4 1.6 bitcast_convert_fusion
  190.0 11.7 %all-to-all-done.2 = bf16[128,16,128]{2,1,0:T(8,128)(2,1)S(1)} async-done(((bf16[128,16,128]{2,1,0:T(8,128)(2,1)}), bf16[128,16,128]{2,1,0:T(8,128)(2,1)S(1)}, u32[]{:S(2)}, u32[]{:S(2)}) %all-to-all-start.2) | async-done | bytes 524320 | tf_op jit(solution)/shard_map/all_to_all | solution.py:425
  201.8 0.8 copy-done
  202.6 2.8 %unpack.1 = (f32[16,128,128]{2,1,0:T(8,128)}, f32[16,128]{1,0:T(8,128)}, f32[16,128]{1,0:T(8,128)}, f32[16,128]{1,0:T(8,128)}) custom-call(bf16[16,8,16,128]{3,2,1,0:T(8,128)(2,1)} %bitcast.37), custom_call_target="tpu_custom_call" | custom-call | flops 1000000 | bytes 1000000 | tf_op jit(solution)/shard_map/unpack/pallas_call | solution.py:309
  (14 shorter events, 0.2 us)
Async XLA Ops:
  1.2 13.4 %copy-start.3 = (bf16[256,2048]{1,0:T(8,128)(2,1)S(1)}, bf16[256,2048]{1,0:T(8,128)(2,1)}, u32[]{:S(2)}) copy-start(bf16[256,2048]{1,0:T(8,128)(2,1)} %rest_5_.1) | copy-start | bytes 3145732
  14.5 17.1 %collective-permute-start.13 = (bf16[4,256,2048]{2,1,0:T(8,128)(2,1)}, bf16[4,256,2048]{2,1,0:T(8,128)(2,1)}, u32[]{:S(2)}, u32[]{:S(2)}) collective-permute-start(bf16[4,256,2048]{2,1,0:T(8,128)(2,1)} %fwd.3), channel_id=1, source_target_pairs={{0,1},{1,0},{2,3},{3,2},{4,5},{5,4},{6,7},{7,6},{8,9},{9,8},{10,11... | collective-permute-start | bytes 12582920 | tf_op jit(solution)/shard_map/ppermute | solution.py:417
  14.6 33.3 %collective-permute-start.1 = (bf16[256,2048]{1,0:T(8,128)(2,1)S(1)}, bf16[256,2048]{1,0:T(8,128)(2,1)S(1)}, u32[]{:S(2)}, u32[]{:S(2)}) collective-permute-start(bf16[256,2048]{1,0:T(8,128)(2,1)S(1)} %copy-done.3), channel_id=1, source_target_pairs={{0,2},{2,4},{4,6},{6,0},{1,3},{3,5},{5,7},{7,1},{8,10},{10,12},{12... | collective-permute-start | bytes 3145736 | tf_op jit(solution)/shard_map/ppermute | solution.py:417
  16.2 33.3 %collective-permute-start.3 = (bf16[256,2048]{1,0:T(8,128)(2,1)S(1)}, bf16[256,2048]{1,0:T(8,128)(2,1)S(1)}, u32[]{:S(2)}, u32[]{:S(2)}) collective-permute-start(bf16[256,2048]{1,0:T(8,128)(2,1)S(1)} %copy-done.3), channel_id=1, source_target_pairs={{0,6},{2,0},{4,2},{6,4},{1,7},{3,1},{5,3},{7,5},{8,14},{10,8},{12,... | collective-permute-start | bytes 3145736 | tf_op jit(solution)/shard_map/ppermute | solution.py:417
  37.2 116.4 %all-to-all-start = ((bf16[64,16,2048]{2,1,0:T(8,128)(2,1)}), bf16[64,16,2048]{2,1,0:T(8,128)(2,1)}, u32[]{:S(2)}, u32[]{:S(2)}) async-start(bf16[64,16,2048]{2,1,0:T(8,128)(2,1)} %bitcast.35), calls=%async_computation | async-start | bytes 8388608 | tf_op jit(solution)/shard_map/all_to_all | solution.py:464
  47.7 63.7 %collective-permute-start = (bf16[256,2048]{1,0:T(8,128)(2,1)S(1)}, bf16[256,2048]{1,0:T(8,128)(2,1)}, u32[]{:S(2)}, u32[]{:S(2)}) collective-permute-start(bf16[256,2048]{1,0:T(8,128)(2,1)S(1)} %copy-done.3), channel_id=1, source_target_pairs={{0,1},{1,0},{2,3},{3,2},{4,5},{5,4},{6,7},{7,6},{8,9},{9,8},{10,11... | collective-permute-start | bytes 3145736 | tf_op jit(solution)/shard_map/ppermute | solution.py:417
  47.9 65.4 %copy-start.1 = (bf16[256,2048]{1,0:T(8,128)(2,1)}, bf16[256,2048]{1,0:T(8,128)(2,1)S(1)}, u32[]{:S(2)}) copy-start(bf16[256,2048]{1,0:T(8,128)(2,1)S(1)} %collective-permute-done.1.rest_6_) | copy-start | bytes 3145732
  47.9 62.4 %collective-permute-start.5 = (bf16[128,2048]{1,0:T(8,128)(2,1)S(1)}, bf16[128,2048]{1,0:T(8,128)(2,1)}, u32[]{:S(2)}, u32[]{:S(2)}) collective-permute-start(bf16[128,2048]{1,0:T(8,128)(2,1)S(1)} %slice.40), channel_id=1, source_target_pairs={{0,2},{2,4},{4,6},{6,0},{1,3},{3,5},{5,7},{7,1},{8,10},{10,12},{12... | collective-permute-start | bytes 1572872 | tf_op jit(solution)/shard_map/ppermute | solution.py:417
  49.5 63.8 %copy-start.2 = (bf16[256,2048]{1,0:T(8,128)(2,1)}, bf16[256,2048]{1,0:T(8,128)(2,1)S(1)}, u32[]{:S(2)}) copy-start(bf16[256,2048]{1,0:T(8,128)(2,1)S(1)} %collective-permute-done.3.rest_7_) | copy-start | bytes 3145732
  49.5 60.8 %collective-permute-start.7 = (bf16[128,2048]{1,0:T(8,128)(2,1)S(1)}, bf16[128,2048]{1,0:T(8,128)(2,1)}, u32[]{:S(2)}, u32[]{:S(2)}) collective-permute-start(bf16[128,2048]{1,0:T(8,128)(2,1)S(1)} %slice.41), channel_id=1, source_target_pairs={{0,6},{2,0},{4,2},{6,4},{1,7},{3,1},{5,3},{7,5},{8,14},{10,8},{12,... | collective-permute-start | bytes 1572872 | tf_op jit(solution)/shard_map/ppermute | solution.py:417
  51.3 62.0 %collective-permute-start.2 = (bf16[256,2048]{1,0:T(8,128)(2,1)S(1)}, bf16[256,2048]{1,0:T(8,128)(2,1)}, u32[]{:S(2)}, u32[]{:S(2)}) collective-permute-start(bf16[256,2048]{1,0:T(8,128)(2,1)S(1)} %collective-permute-done.1.rest_6_), channel_id=1, source_target_pairs={{0,1},{1,0},{2,3},{3,2},{4,5},{5,4},{6,7},{7,6},{8,9},{9,8},{10,11... | collective-permute-start | bytes 3145736 | tf_op jit(solution)/shard_map/ppermute | solution.py:417
  51.3 62.0 %collective-permute-start.4 = (bf16[256,2048]{1,0:T(8,128)(2,1)S(1)}, bf16[256,2048]{1,0:T(8,128)(2,1)}, u32[]{:S(2)}, u32[]{:S(2)}) collective-permute-start(bf16[256,2048]{1,0:T(8,128)(2,1)S(1)} %collective-permute-done.3.rest_7_), channel_id=1, source_target_pairs={{0,1},{1,0},{2,3},{3,2},{4,5},{5,4},{6,7},{7,6},{8,9},{9,8},{10,11... | collective-permute-start | bytes 3145736 | tf_op jit(solution)/shard_map/ppermute | solution.py:417
  110.3 2.3 %collective-permute-start.6 = (bf16[128,2048]{1,0:T(8,128)(2,1)}, bf16[128,2048]{1,0:T(8,128)(2,1)}, u32[]{:S(2)}, u32[]{:S(2)}) collective-permute-start(bf16[128,2048]{1,0:T(8,128)(2,1)} %collective-permute-done.5.rest_8_), channel_id=1, source_target_pairs={{0,1},{1,0},{2,3},{3,2},{4,5},{5,4},{6,7},{7,6},{8,9},{9,8},{10,11... | collective-permute-start | bytes 1572872 | tf_op jit(solution)/shard_map/ppermute | solution.py:417
  110.3 3.0 %collective-permute-start.8 = (bf16[128,2048]{1,0:T(8,128)(2,1)}, bf16[128,2048]{1,0:T(8,128)(2,1)}, u32[]{:S(2)}, u32[]{:S(2)}) collective-permute-start(bf16[128,2048]{1,0:T(8,128)(2,1)} %collective-permute-done.7.rest_9_), channel_id=1, source_target_pairs={{0,1},{1,0},{2,3},{3,2},{4,5},{5,4},{6,7},{7,6},{8,9},{9,8},{10,11... | collective-permute-start | bytes 1572872 | tf_op jit(solution)/shard_map/ppermute | solution.py:417
  143.0 1.6 collective-permute-start.9
  145.6 4.3 %collective-permute-start.10 = (bf16[16,16,128]{2,1,0:T(8,128)(2,1)S(1)}, bf16[16,16,128]{2,1,0:T(8,128)(2,1)S(1)}, u32[]{:S(2)}, u32[]{:S(2)}) collective-permute-start(bf16[16,16,128]{2,1,0:T(8,128)(2,1)S(1)} %get-tuple-element.25), channel_id=1, source_target_pairs={{0,6},{2,0},{4,2},{6,4},{1,7},{3,1},{5,3},{7,5},{8,14},{10,8},{12,... | collective-permute-start | bytes 196616 | tf_op jit(solution)/shard_map/ppermute | solution.py:417
  145.7 5.5 %collective-permute-start.11 = (bf16[16,16,128]{2,1,0:T(8,128)(2,1)S(1)}, bf16[16,16,128]{2,1,0:T(8,128)(2,1)S(1)}, u32[]{:S(2)}, u32[]{:S(2)}) collective-permute-start(bf16[16,16,128]{2,1,0:T(8,128)(2,1)S(1)} %get-tuple-element.26), channel_id=1, source_target_pairs={{0,2},{2,4},{4,6},{6,0},{1,3},{3,5},{5,7},{7,1},{8,10},{10,12},{12... | collective-permute-start | bytes 196616 | tf_op jit(solution)/shard_map/ppermute | solution.py:417
  147.7 5.8 %collective-permute-start.12 = (bf16[16,16,128]{2,1,0:T(8,128)(2,1)S(1)}, bf16[16,16,128]{2,1,0:T(8,128)(2,1)S(1)}, u32[]{:S(2)}, u32[]{:S(2)}) collective-permute-start(bf16[16,16,128]{2,1,0:T(8,128)(2,1)S(1)} %get-tuple-element.27), channel_id=1, source_target_pairs={{0,4},{2,6},{4,0},{6,2},{1,5},{3,7},{5,1},{7,3},{8,12},{10,14},{12... | collective-permute-start | bytes 196616 | tf_op jit(solution)/shard_map/ppermute | solution.py:417
  183.2 18.6 %all-to-all-start.2 = ((bf16[128,16,128]{2,1,0:T(8,128)(2,1)}), bf16[128,16,128]{2,1,0:T(8,128)(2,1)S(1)}, u32[]{:S(2)}, u32[]{:S(2)}) async-start(bf16[128,16,128]{2,1,0:T(8,128)(2,1)} %broadcast_in_dim.21), calls=%async_computation.2 | async-start | bytes 1048576 | tf_op jit(solution)/shard_map/all_to_all | solution.py:425
  201.8 0.8 copy-start

commit v5 on v4

--- a/solution.py
+++ b/solution.py
@@ -14,7 +14,8 @@
 BF16 = jnp.bfloat16
 BLK = 128
 PAIR = 256
-CHUNK = 16
+SIDE = 16
+PACK = 9 * BLK
 ROOT = BLK**0.5
 
 
@@ -130,12 +131,13 @@
             multiply(i)
 
 
-def forward(order, u, v, d, mix, bias, gain, shift):
-    n = order.shape[0]
+def forward(here, theirs, u, v, d, mix, bias, gain, shift):
     length, width = u.shape
+    n = width // PAIR // 2
     last = n - 1
-    cur = lambda j, o: (0, o[jnp.minimum(j, last)])
-    par = lambda j, o: (o[jnp.minimum(j, last)], 0, 0)
+    pair_at = lambda j, o: 2 * jnp.minimum(j, last) + (1 - o[1] if theirs else o[1])
+    cur = lambda j, o: (0, pair_at(j, o))
+    par = lambda j, o: (pair_at(j, o), 0, 0)
     return pl.pallas_call(
         forward_kernel,
         grid_spec=pltpu.PrefetchScalarGridSpec(
@@ -145,7 +147,7 @@
                 pl.BlockSpec((length, PAIR), cur),
                 pl.BlockSpec((length, PAIR), cur),
                 pl.BlockSpec(memory_space=pl.ANY),
-                pl.BlockSpec((1, 2, BLK, BLK), lambda j, o: (o[jnp.minimum(j, last)], 0, 0, 0)),
+                pl.BlockSpec((1, 2, BLK, BLK), lambda j, o: (pair_at(j, o), 0, 0, 0)),
                 pl.BlockSpec((1, 2, BLK), par),
                 pl.BlockSpec((1, 2, BLK), par),
                 pl.BlockSpec((1, 2, BLK), par),
@@ -166,7 +168,7 @@
             transcendentals=2 * n * PAIR * length,
         ),
         name="fwd",
-    )(order, u, v, d, mix, bias, gain, shift)
+    )(here, u, v, d, mix, bias, gain, shift)
 
 
 def backward_kernel(
@@ -273,25 +275,23 @@
     col = lax.broadcasted_iota(jnp.int32, (BLK, BLK), 1)
     extra.append(jnp.sum(jnp.where(row == col, m_acc[1], 0.0), axis=0, keepdims=True))
     both = jnp.where(row >= col, m_acc[0], m_acc[1].T)
-    filler = jnp.zeros((CHUNK - 9, BLK), F32)
-    blank = jnp.zeros((1, BLK), F32)
-    for k in range(16):
-        vector = extra[k] if k < len(extra) else blank
-        pack_ref[0, k] = jnp.concatenate(
-            [both[k * 8 : (k + 1) * 8], vector, filler], axis=0
-        ).astype(BF16)
+    while len(extra) < SIDE:
+        extra.append(jnp.zeros((1, BLK), F32))
+    tiles = [both[k * SIDE : (k + 1) * SIDE] for k in range(BLK // SIDE)]
+    tiles.append(jnp.concatenate(extra, axis=0))
+    pack_ref[0] = jnp.concatenate(tiles, axis=1).astype(BF16)
 
 
 def unpack_kernel(x_ref, gw_ref, gb_ref, gg_ref, gs_ref):
-    chunks, pairs = x_ref.shape[:2]
+    pairs = x_ref.shape[0]
     row = lax.broadcasted_iota(jnp.int32, (BLK, BLK), 0)
     col = lax.broadcasted_iota(jnp.int32, (BLK, BLK), 1)
 
     @pl.loop(0, pairs)
     def _(pair):
-        part = [x_ref[k, pair].astype(F32) for k in range(chunks)]
-        both = jnp.concatenate([p[:8] for p in part], axis=0)
-        vector = lambda k: part[k][8:9]
+        x = x_ref[pair].astype(F32)
+        both = jnp.concatenate([x[:, cols_of(k)] for k in range(BLK // SIDE)], axis=0)
+        vector = lambda k: x[k : k + 1, cols_of(BLK // SIDE)]
         gw_ref[2 * pair] = jnp.where(row >= col, both, 0.0)
         gw_ref[2 * pair + 1] = jnp.where(
             row > col, both.T, jnp.where(row == col, vector(6), 0.0)
@@ -304,7 +304,7 @@
 
 
 def unpack(total):
-    pairs = total.shape[1]
+    pairs = total.shape[0]
     row = jax.ShapeDtypeStruct((2 * pairs, BLK), F32)
     return pl.pallas_call(
         unpack_kernel,
@@ -353,21 +353,26 @@
     )(a.reshape(parts), b.reshape(parts)).reshape(a.shape)
 
 
-def backward(order, weights, u, v, d, mix, bias, gain, shift):
-    n = order.shape[0]
+def backward(here, weights, u, v, d, mix, bias, gain, shift):
     length, width = u.shape
-    pairs = width // PAIR
+    n = pairs = width // PAIR
+    half = n // 2
+
+    def pair_at(j, o):
+        core = jnp.where(j < half, 1 - o[1], o[1])
+        return lax.rem(o[0] + o[2 + lax.rem(j, half)], half) * 2 + core
+
     pieces = tuple((slot, start, w.shape[0]) for slot, start, w in weights)
-    cur = lambda j, o: (0, o[j])
-    par = lambda j, o: (o[j], 0, 0)
-    mat = pl.BlockSpec((1, 2, BLK, BLK), lambda j, o: (o[j], 0, 0, 0))
+    cur = lambda j, o: (0, pair_at(j, o))
+    par = lambda j, o: (pair_at(j, o), 0, 0)
+    mat = pl.BlockSpec((1, 2, BLK, BLK), lambda j, o: (pair_at(j, o), 0, 0, 0))
     tile = pl.BlockSpec((length, PAIR), cur)
     vec = pl.BlockSpec((1, 2, BLK), par)
     hbm = pl.BlockSpec(memory_space=pl.ANY)
     shapes = [
         jax.ShapeDtypeStruct((length, width), BF16),
         jax.ShapeDtypeStruct((length, width), BF16),
-        jax.ShapeDtypeStruct((pairs, 16, CHUNK, BLK), BF16),
+        jax.ShapeDtypeStruct((pairs, SIDE, PACK), BF16),
     ]
     return pl.pallas_call(
         functools.partial(backward_kernel, pieces),
@@ -387,7 +392,7 @@
             out_specs=[
                 tile,
                 tile,
-                pl.BlockSpec((1, 16, CHUNK, BLK), lambda j, o: (j, 0, 0, 0)),
+                pl.BlockSpec((1, SIDE, PACK), lambda j, o: (j, 0, 0)),
             ],
             scratch_shapes=[
                 pltpu.VMEM((width // BLK, length, BLK), BF16),
@@ -410,7 +415,7 @@
             transcendentals=3 * n * PAIR * length,
         ),
         name="bwd",
-    )(order, u, v, d, mix, bias, gain, shift, *[w for _, _, w in weights])
+    )(here, u, v, d, mix, bias, gain, shift, *[w for _, _, w in weights])
 
 
 def hop(a, axis, size, by):
@@ -439,7 +444,8 @@
     groups = w_mix.shape[0]
     pairs = groups // 2
     x, c = lax.axis_index("x"), lax.axis_index("c")
-    xs = jnp.arange(nx, dtype=jnp.int32)
+    hops = jnp.array([0, nx - 1, 1, 2], jnp.int32)
+    here = jnp.concatenate([jnp.stack([x, c]).astype(jnp.int32), hops])
 
     swap = lambda a: hop(a, "c", nc, 1)
     half = w_out.shape[0] // 2
@@ -457,15 +463,12 @@
     shift = norm_shift.reshape(pairs, 2, BLK)
 
     common = (u, v, d, mix, bias, gain, shift)
-    theirs = forward(xs * nc + (1 - c), *common)
-    ours = forward(xs * nc + c, *common)
+    theirs = forward(here, True, *common)
+    ours = forward(here, False, *common)
     traded = swap(theirs)
     joined = join(ours, traded)
     split = lax.all_to_all(joined.reshape(nx * plane, PAIR // plane, width), ("x", "z", "y"), 0, 0)
 
-    place = lambda k, core: lax.rem(x + k, nx) * nc + core
-    hops = (0, nx - 1, 1, 2)
-    order = jnp.stack([place(k, core) for core in (1 - c, c) for k in hops])
     weights = [
         (0, 0, own),
         (1, 0, near[0]),
@@ -478,7 +481,7 @@
         (7, 0, far0),
         (7, half, far1),
     ]
-    grad_u, grad_v, packed = backward(order, weights, *common)
+    grad_u, grad_v, packed = backward(here, weights, *common)
 
     mine = packed[nx:].astype(F32) + swap(packed[:nx]).astype(F32)
     mine = lax.optimization_barrier(mine).astype(BF16)
@@ -489,13 +492,11 @@
     ours = lax.optimization_barrier(ours).astype(BF16)
 
     ours, split = lax.optimization_barrier((ours, split))
-    devices = nz * ny * nx * nc
-    rows = added(split)
-    both = jnp.concatenate([jnp.broadcast_to(rows[None], (plane,) + rows.shape), ours], axis=2)
-    both = lax.all_to_all(both, ("z", "y"), 0, 0)
-    total = spread(added(both[:, :, width:]), ("z", "y", "x", "c"), devices)
+    both = jnp.concatenate([added(split), ours], axis=1)
+    both = spread(both, ("z", "y"), plane)
+    total = spread(added(both[:, :, width:]), ("x", "c"), nx * nc)
     grad_w_out = both[:, :, :width].astype(F32).reshape(PAIR, width)
-    grad_w, *vectors = unpack(total.reshape(plane, pairs, CHUNK, BLK))
+    grad_w, *vectors = unpack(total)
     return (grad_u[None], grad_v[None], grad_w_out, grad_w, *vectors)
 
 

time: 206 us -> 183 us (0.89)
  waiting for transfers between devices: 77.3 us -> 46 us
  starting transfers between devices: 27.7 us -> 32.9 us
  blocking collectives: 25.7 us -> 28.7 us
    ppermute x14, waiting for transfers between devices: 65.5 us -> 39 us  [hop(): return lax.ppermute(a, axis, [(i, (i + by) % size) for i in range(size)])]
    all_to_all x1, waiting for transfers between devices: 11.7 us -> 6.1 us  [spread(): lax.all_to_all(jnp.broadcast_to(a[None], (count,) + a.shape), axes, 0, 0)]
    all_to_all x1, starting transfers between devices: 5.08 us -> 10.2 us  [spread(): lax.all_to_all(jnp.broadcast_to(a[None], (count,) + a.shape), axes, 0, 0)]
    all_to_all x1, blocking collectives: 25.7 us -> 28.7 us  [spread(): lax.all_to_all(jnp.broadcast_to(a[None], (count,) + a.shape), axes, 0, 0)]
  transfers between devices with their start and end apart: 16 -> 16, of which waited for: 8 -> 8; matrix products, arithmetic and copies ran while one was open for 2% -> 2% of each run, Pallas kernels for 23% -> 26%
where the time goes in v5:
time: 183 us; the launch traced here: 182 us
  Pallas kernels  63.7 us (35%)
  waiting for transfers between devices  46 us (25%)
  starting transfers between devices  32.9 us (18%)
  blocking collectives  28.7 us (16%)
  other arithmetic  6.77 us (4%)
  local copies, waits for them, and re-layouts  3.51 us (2%)
    ppermute x14, waiting for transfers between devices, hop(): return lax.ppermute(a, axis, [(i, (i + by) % size) for i in range(size)])  39 us
    pallas_call x1, Pallas kernels, backward(): pl.pallas_call(functools.partial(backward_kernel, pieces), grid_spec=pltp...  29.1 us
    all_to_all x1, blocking collectives, spread(): lax.all_to_all(jnp.broadcast_to(a[None], (count,) + a.shape), axes, 0, 0)  28.7 us
    pallas_call x2, Pallas kernels, forward(): pl.pallas_call(forward_kernel, grid_spec=pltpu.PrefetchScalarGridSpec(num...  26.2 us
    ppermute x14, starting transfers between devices, hop(): return lax.ppermute(a, axis, [(i, (i + by) % size) for i in range(size)])  13.3 us
    all_to_all x1, starting transfers between devices, spread(): lax.all_to_all(jnp.broadcast_to(a[None], (count,) + a.shape), axes, 0, 0)  10.2 us
    all_to_all x1, starting transfers between devices, everything(): lax.all_to_all(joined.reshape(nx * plane, PAIR // plane, width), ('x', 'z...  9.38 us
    all_to_all x1, waiting for transfers between devices, spread(): lax.all_to_all(jnp.broadcast_to(a[None], (count,) + a.shape), axes, 0, 0)  6.1 us
  transfers between devices with their start and end apart: 16, of which 8 were waited for; matrix products, arithmetic and copies ran while one was open for 2% of the time, Pallas kernels for 26%

profile of v5, /device:TPU:0, one launch (start us, length us, event | category | flops | bytes accessed | tf_op | source)
XLA Modules:
  0.0 182.3 jit_solution(7474953646862094072)
XLA Ops:
  0.6 1.2 pad_add_fusion.order
  1.9 13.1 %fwd.3 = bf16[4,256,2048]{2,1,0:T(8,128)(2,1)} custom-call(s32[6]{0:T(128)} %pad_add_fusion.order, bf16[1024,2048]{1,0:T(8,128)(2,1)} %bitcast.30, bf16[1024,2048]{1,0:T(8,128)(2,1)} %bitcast.33, bf16[1024,2048]{1,0:T(8,128)(2,1)} %bitcast.36, bf16[8,2,128,128]{3,2,1,0:T(8,128)(2,1)} %bitcast.39, f32[8,2,128]{2,1,0:T(2,128)} %bitcast.42, ...), custom_call_target="tpu_custom_call" | custom-call | flops 9126805504 | bytes 12582912 | tf_op jit(solution)/shard_map/fwd/pallas_call | solution.py:141
  15.0 0.1 collective-permute-start.13
  15.1 1.7 collective-permute-start.1
  16.8 1.6 collective-permute-start.3
  18.4 0.0 collective-permute-start
  18.4 23.7 %collective-permute-done.1.rest_6_ = bf16[256,2048]{1,0:T(8,128)(2,1)S(1)} collective-permute-done((bf16[256,2048]{1,0:T(8,128)(2,1)}, bf16[256,2048]{1,0:T(8,128)(2,1)S(1)}, u32[]{:S(2)}, u32[]{:S(2)}) %collective-permute-start.1) | collective-permute-done | bytes 1048608 | tf_op jit(solution)/shard_map/ppermute | solution.py:422
  42.1 0.5 collective-permute-start.5
  42.6 0.0 collective-permute-done.3.rest_7_
  42.7 2.9 %collective-permute-start.7 = (bf16[128,2048]{1,0:T(8,128)(2,1)S(1)}, bf16[128,2048]{1,0:T(8,128)(2,1)}, u32[]{:S(2)}, u32[]{:S(2)}) collective-permute-start(bf16[128,2048]{1,0:T(8,128)(2,1)S(1)} %slice.41), channel_id=1, source_target_pairs={{0,6},{2,0},{4,2},{6,4},{1,7},{3,1},{5,3},{7,5},{8,14},{10,8},{12,... | collective-permute-start | bytes 1572872 | tf_op jit(solution)/shard_map/ppermute | solution.py:422
  45.6 0.0 collective-permute-start.2
  45.6 0.0 collective-permute-done.13
  45.6 0.5 collective-permute-start.4
  46.1 13.1 %fwd.2 = bf16[4,256,2048]{2,1,0:T(8,128)(2,1)} custom-call(s32[6]{0:T(128)} %pad_add_fusion.order, bf16[1024,2048]{1,0:T(8,128)(2,1)} %bitcast.31, bf16[1024,2048]{1,0:T(8,128)(2,1)} %bitcast.34, bf16[1024,2048]{1,0:T(8,128)(2,1)} %bitcast.37, bf16[8,2,128,128]{3,2,1,0:T(8,128)(2,1)} %bitcast.40, f32[8,2,128]{2,1,0:T(2,128)} %bitcast.43, ...), custom_call_target="tpu_custom_call" | custom-call | flops 9126805504 | bytes 12582912 | tf_op jit(solution)/shard_map/fwd/pallas_call | solution.py:141
  59.2 5.6 %join.1 = bf16[16,64,2048]{2,1,0:T(8,128)(2,1)} custom-call(bf16[16,64,2048]{2,1,0:T(8,128)(2,1)} %bitcast.29, bf16[16,64,2048]{2,1,0:T(8,128)(2,1)} %bitcast.16.b_hbm), custom_call_target="tpu_custom_call" | custom-call | flops 2097152 | bytes 12582912 | tf_op jit(solution)/shard_map/join/pallas_call | solution.py:343
  64.8 9.4 %all-to-all-start = ((bf16[64,16,2048]{2,1,0:T(8,128)(2,1)}), bf16[64,16,2048]{2,1,0:T(8,128)(2,1)}, u32[]{:S(2)}, u32[]{:S(2)}) async-start(bf16[64,16,2048]{2,1,0:T(8,128)(2,1)} %bitcast.28), calls=%async_computation | async-start | bytes 8388608 | tf_op jit(solution)/shard_map/all_to_all | solution.py:470
  74.2 0.0 collective-permute-done.5.rest_8_
  74.2 0.1 collective-permute-start.6
  74.3 0.0 collective-permute-done.7.rest_9_
  74.3 0.5 collective-permute-start.8
  74.8 1.6 collective-permute-done.6.rest_3_
  76.4 0.7 collective-permute-done.8.rest_4_
  77.2 0.0 collective-permute-done.2.rest_1_
  77.2 0.0 collective-permute-done.4.rest_2_
  77.2 0.1 copy-done.3
  77.3 0.7 copy-done.4
  78.0 29.1 %bwd.1 = (bf16[1024,2048]{1,0:T(8,128)(2,1)}, bf16[1024,2048]{1,0:T(8,128)(2,1)}, bf16[8,16,1152]{2,1,0:T(8,128)(2,1)}) custom-call(s32[6]{0:T(128)} %pad_add_fusion.order, bf16[1024,2048]{1,0:T(8,128)(2,1)} %bitcast.32, bf16[1024,2048]{1,0:T(8,128)(2,1)} %bitcast.35, bf16[1024,2048]{1,0:T(8,128)(2,1)} %bitcast.38, bf16[8,2,128,128]{3,2,1,0:T(8,128)(2,1)} %bitcast.41, ...), custom_call_target="tpu_custom_call" | custom-call | flops 20401094656 | bytes 29360128 | tf_op jit(solution)/shard_map/bwd/pallas_call | solution.py:377
  107.1 0.9 slice.33
  108.0 0.2 collective-permute-start.9
  108.3 1.2 collective-permute-done.9
  109.5 1.0 convert_add_fusion
  110.5 3.0 %collective-permute-start.10 = (bf16[16,1152]{1,0:T(8,128)(2,1)S(1)}, bf16[16,1152]{1,0:T(8,128)(2,1)S(1)}, u32[]{:S(2)}, u32[]{:S(2)}) collective-permute-start(bf16[16,1152]{1,0:T(8,128)(2,1)S(1)} %get-tuple-element.25), channel_id=1, source_target_pairs={{0,6},{2,0},{4,2},{6,4},{1,7},{3,1},{5,3},{7,5},{8,14},{10,8},{12,... | collective-permute-start | bytes 110600 | tf_op jit(solution)/shard_map/ppermute | solution.py:422
  113.5 0.0 collective-permute-start.11
  113.5 2.2 %collective-permute-start.12 = (bf16[16,1152]{1,0:T(8,128)(2,1)S(1)}, bf16[16,1152]{1,0:T(8,128)(2,1)S(1)}, u32[]{:S(2)}, u32[]{:S(2)}) collective-permute-start(bf16[16,1152]{1,0:T(8,128)(2,1)S(1)} %get-tuple-element.27), channel_id=1, source_target_pairs={{0,4},{2,6},{4,0},{6,2},{1,5},{3,7},{5,1},{7,3},{8,12},{10,14},{12... | collective-permute-start | bytes 110600 | tf_op jit(solution)/shard_map/ppermute | solution.py:422
  115.7 9.9 %collective-permute-done.10 = bf16[16,1152]{1,0:T(8,128)(2,1)S(1)} collective-permute-done((bf16[16,1152]{1,0:T(8,128)(2,1)S(1)}, bf16[16,1152]{1,0:T(8,128)(2,1)S(1)}, u32[]{:S(2)}, u32[]{:S(2)}) %collective-permute-start.10) | collective-permute-done | bytes 36896 | tf_op jit(solution)/shard_map/ppermute | solution.py:422
  125.6 1.8 collective-permute-done.11
  127.4 0.9 all-to-all-done
  128.3 2.8 %convert_reduce_fusion = bf16[16,2048]{1,0:T(8,128)(2,1)S(1)} fusion(bf16[64,16,2048]{2,1,0:T(8,128)(2,1)} %all-to-all-done), kind=kLoop, calls=%fused_computation | loop fusion | flops 4161536 | bytes 4259840 | tf_op jit(solution)/shard_map/reduce_sum | solution.py:426
  131.1 0.1 broadcast_in_dim.20
  131.3 28.7 %all_to_all.15 = bf16[16,16,3200]{2,1,0:T(8,128)(2,1)S(1)} all-to-all(bf16[16,16,3200]{2,1,0:T(8,128)(2,1)S(1)} %broadcast_in_dim.20), channel_id=1, replica_groups=mesh['z'=4,'y'=4,'x'=4,'c'=2] {'z','y'}, dimensions={0} | all-to-all | bytes 3276800 | tf_op jit(solution)/shard_map/all_to_all | solution.py:430
  159.9 0.1 convert_reduce_fusion.1
  160.0 0.7 broadcast_in_dim.21
  160.8 10.2 %all-to-all-start.2 = ((bf16[8,16,1152]{2,1,0:T(8,128)(2,1)}), bf16[8,16,1152]{2,1,0:T(8,128)(2,1)S(1)}, u32[]{:S(2)}, u32[]{:S(2)}) async-start(bf16[8,16,1152]{2,1,0:T(8,128)(2,1)} %broadcast_in_dim.21), calls=%async_computation.2 | async-start | bytes 589824 | tf_op jit(solution)/shard_map/all_to_all | solution.py:430
  171.0 0.1 slice.46
  171.1 1.6 bitcast_convert_fusion
  172.7 6.1 %all-to-all-done.2.x_ref = bf16[8,16,1152]{2,1,0:T(8,128)(2,1)S(1)} async-done(((bf16[8,16,1152]{2,1,0:T(8,128)(2,1)}), bf16[8,16,1152]{2,1,0:T(8,128)(2,1)S(1)}, u32[]{:S(2)}, u32[]{:S(2)}) %all-to-all-start.2) | async-done | bytes 294944 | tf_op jit(solution)/shard_map/all_to_all | solution.py:430
  178.8 0.7 copy-done
  179.6 2.8 %unpack.1 = (f32[16,128,128]{2,1,0:T(8,128)}, f32[16,128]{1,0:T(8,128)}, f32[16,128]{1,0:T(8,128)}, f32[16,128]{1,0:T(8,128)}) custom-call(bf16[8,16,1152]{2,1,0:T(8,128)(2,1)} %copy-done), custom_call_target="tpu_custom_call" | custom-call | flops 1000000 | bytes 1000000 | tf_op jit(solution)/shard_map/unpack/pallas_call | solution.py:309
  (14 shorter events, 0.1 us)
Async XLA Ops:
  15.0 30.6 %collective-permute-start.13 = (bf16[4,256,2048]{2,1,0:T(8,128)(2,1)}, bf16[4,256,2048]{2,1,0:T(8,128)(2,1)}, u32[]{:S(2)}, u32[]{:S(2)}) collective-permute-start(bf16[4,256,2048]{2,1,0:T(8,128)(2,1)} %fwd.3), channel_id=1, source_target_pairs={{0,1},{1,0},{2,3},{3,2},{4,5},{5,4},{6,7},{7,6},{8,9},{9,8},{10,11... | collective-permute-start | bytes 12582920 | tf_op jit(solution)/shard_map/ppermute | solution.py:422
  15.1 27.0 %collective-permute-start.1 = (bf16[256,2048]{1,0:T(8,128)(2,1)}, bf16[256,2048]{1,0:T(8,128)(2,1)S(1)}, u32[]{:S(2)}, u32[]{:S(2)}) collective-permute-start(bf16[256,2048]{1,0:T(8,128)(2,1)} %rest_5_.1), channel_id=1, source_target_pairs={{0,2},{2,4},{4,6},{6,0},{1,3},{3,5},{5,7},{7,1},{8,10},{10,12},{12... | collective-permute-start | bytes 3145736 | tf_op jit(solution)/shard_map/ppermute | solution.py:422
  16.8 25.8 %collective-permute-start.3 = (bf16[256,2048]{1,0:T(8,128)(2,1)}, bf16[256,2048]{1,0:T(8,128)(2,1)S(1)}, u32[]{:S(2)}, u32[]{:S(2)}) collective-permute-start(bf16[256,2048]{1,0:T(8,128)(2,1)} %rest_5_.1), channel_id=1, source_target_pairs={{0,6},{2,0},{4,2},{6,4},{1,7},{3,1},{5,3},{7,5},{8,14},{10,8},{12,... | collective-permute-start | bytes 3145736 | tf_op jit(solution)/shard_map/ppermute | solution.py:422
  18.4 56.4 %collective-permute-start = (bf16[256,2048]{1,0:T(8,128)(2,1)}, bf16[256,2048]{1,0:T(8,128)(2,1)}, u32[]{:S(2)}, u32[]{:S(2)}) collective-permute-start(bf16[256,2048]{1,0:T(8,128)(2,1)} %rest_5_.1), channel_id=1, source_target_pairs={{0,1},{1,0},{2,3},{3,2},{4,5},{5,4},{6,7},{7,6},{8,9},{9,8},{10,11... | collective-permute-start | bytes 3145736 | tf_op jit(solution)/shard_map/ppermute | solution.py:422
  42.1 17.1 %copy-start.1 = (bf16[256,2048]{1,0:T(8,128)(2,1)}, bf16[256,2048]{1,0:T(8,128)(2,1)S(1)}, u32[]{:S(2)}) copy-start(bf16[256,2048]{1,0:T(8,128)(2,1)S(1)} %collective-permute-done.1.rest_6_) | copy-start | bytes 3145732
  42.1 32.1 %collective-permute-start.5 = (bf16[128,2048]{1,0:T(8,128)(2,1)S(1)}, bf16[128,2048]{1,0:T(8,128)(2,1)}, u32[]{:S(2)}, u32[]{:S(2)}) collective-permute-start(bf16[128,2048]{1,0:T(8,128)(2,1)S(1)} %slice.40), channel_id=1, source_target_pairs={{0,2},{2,4},{4,6},{6,0},{1,3},{3,5},{5,7},{7,1},{8,10},{10,12},{12... | collective-permute-start | bytes 1572872 | tf_op jit(solution)/shard_map/ppermute | solution.py:422
  42.6 16.6 %copy-start.2 = (bf16[256,2048]{1,0:T(8,128)(2,1)}, bf16[256,2048]{1,0:T(8,128)(2,1)S(1)}, u32[]{:S(2)}) copy-start(bf16[256,2048]{1,0:T(8,128)(2,1)S(1)} %collective-permute-done.3.rest_7_) | copy-start | bytes 3145732
  42.7 31.7 %collective-permute-start.7 = (bf16[128,2048]{1,0:T(8,128)(2,1)S(1)}, bf16[128,2048]{1,0:T(8,128)(2,1)}, u32[]{:S(2)}, u32[]{:S(2)}) collective-permute-start(bf16[128,2048]{1,0:T(8,128)(2,1)S(1)} %slice.41), channel_id=1, source_target_pairs={{0,6},{2,0},{4,2},{6,4},{1,7},{3,1},{5,3},{7,5},{8,14},{10,8},{12,... | collective-permute-start | bytes 1572872 | tf_op jit(solution)/shard_map/ppermute | solution.py:422
  45.6 31.6 %collective-permute-start.2 = (bf16[256,2048]{1,0:T(8,128)(2,1)S(1)}, bf16[256,2048]{1,0:T(8,128)(2,1)}, u32[]{:S(2)}, u32[]{:S(2)}) collective-permute-start(bf16[256,2048]{1,0:T(8,128)(2,1)S(1)} %collective-permute-done.1.rest_6_), channel_id=1, source_target_pairs={{0,1},{1,0},{2,3},{3,2},{4,5},{5,4},{6,7},{7,6},{8,9},{9,8},{10,11... | collective-permute-start | bytes 3145736 | tf_op jit(solution)/shard_map/ppermute | solution.py:422
  45.6 31.6 %collective-permute-start.4 = (bf16[256,2048]{1,0:T(8,128)(2,1)S(1)}, bf16[256,2048]{1,0:T(8,128)(2,1)}, u32[]{:S(2)}, u32[]{:S(2)}) collective-permute-start(bf16[256,2048]{1,0:T(8,128)(2,1)S(1)} %collective-permute-done.3.rest_7_), channel_id=1, source_target_pairs={{0,1},{1,0},{2,3},{3,2},{4,5},{5,4},{6,7},{7,6},{8,9},{9,8},{10,11... | collective-permute-start | bytes 3145736 | tf_op jit(solution)/shard_map/ppermute | solution.py:422
  64.8 63.5 %all-to-all-start = ((bf16[64,16,2048]{2,1,0:T(8,128)(2,1)}), bf16[64,16,2048]{2,1,0:T(8,128)(2,1)}, u32[]{:S(2)}, u32[]{:S(2)}) async-start(bf16[64,16,2048]{2,1,0:T(8,128)(2,1)} %bitcast.28), calls=%async_computation | async-start | bytes 8388608 | tf_op jit(solution)/shard_map/all_to_all | solution.py:470
  74.2 2.2 %collective-permute-start.6 = (bf16[128,2048]{1,0:T(8,128)(2,1)}, bf16[128,2048]{1,0:T(8,128)(2,1)S(1)}, u32[]{:S(2)}, u32[]{:S(2)}) collective-permute-start(bf16[128,2048]{1,0:T(8,128)(2,1)} %collective-permute-done.5.rest_8_), channel_id=1, source_target_pairs={{0,1},{1,0},{2,3},{3,2},{4,5},{5,4},{6,7},{7,6},{8,9},{9,8},{10,11... | collective-permute-start | bytes 1572872 | tf_op jit(solution)/shard_map/ppermute | solution.py:422
  74.3 2.8 %collective-permute-start.8 = (bf16[128,2048]{1,0:T(8,128)(2,1)}, bf16[128,2048]{1,0:T(8,128)(2,1)S(1)}, u32[]{:S(2)}, u32[]{:S(2)}) collective-permute-start(bf16[128,2048]{1,0:T(8,128)(2,1)} %collective-permute-done.7.rest_9_), channel_id=1, source_target_pairs={{0,1},{1,0},{2,3},{3,2},{4,5},{5,4},{6,7},{7,6},{8,9},{9,8},{10,11... | collective-permute-start | bytes 1572872 | tf_op jit(solution)/shard_map/ppermute | solution.py:422
  76.4 0.8 copy-start.3
  77.2 0.8 copy-start.4
  108.0 1.5 collective-permute-start.9
  110.5 15.1 %collective-permute-start.10 = (bf16[16,1152]{1,0:T(8,128)(2,1)S(1)}, bf16[16,1152]{1,0:T(8,128)(2,1)S(1)}, u32[]{:S(2)}, u32[]{:S(2)}) collective-permute-start(bf16[16,1152]{1,0:T(8,128)(2,1)S(1)} %get-tuple-element.25), channel_id=1, source_target_pairs={{0,6},{2,0},{4,2},{6,4},{1,7},{3,1},{5,3},{7,5},{8,14},{10,8},{12,... | collective-permute-start | bytes 110600 | tf_op jit(solution)/shard_map/ppermute | solution.py:422
  113.5 13.9 %collective-permute-start.11 = (bf16[16,1152]{1,0:T(8,128)(2,1)S(1)}, bf16[16,1152]{1,0:T(8,128)(2,1)S(1)}, u32[]{:S(2)}, u32[]{:S(2)}) collective-permute-start(bf16[16,1152]{1,0:T(8,128)(2,1)S(1)} %get-tuple-element.26), channel_id=1, source_target_pairs={{0,2},{2,4},{4,6},{6,0},{1,3},{3,5},{5,7},{7,1},{8,10},{10,12},{12... | collective-permute-start | bytes 110600 | tf_op jit(solution)/shard_map/ppermute | solution.py:422
  113.5 13.9 %collective-permute-start.12 = (bf16[16,1152]{1,0:T(8,128)(2,1)S(1)}, bf16[16,1152]{1,0:T(8,128)(2,1)S(1)}, u32[]{:S(2)}, u32[]{:S(2)}) collective-permute-start(bf16[16,1152]{1,0:T(8,128)(2,1)S(1)} %get-tuple-element.27), channel_id=1, source_target_pairs={{0,4},{2,6},{4,0},{6,2},{1,5},{3,7},{5,1},{7,3},{8,12},{10,14},{12... | collective-permute-start | bytes 110600 | tf_op jit(solution)/shard_map/ppermute | solution.py:422
  160.8 18.1 %all-to-all-start.2 = ((bf16[8,16,1152]{2,1,0:T(8,128)(2,1)}), bf16[8,16,1152]{2,1,0:T(8,128)(2,1)S(1)}, u32[]{:S(2)}, u32[]{:S(2)}) async-start(bf16[8,16,1152]{2,1,0:T(8,128)(2,1)} %broadcast_in_dim.21), calls=%async_computation.2 | async-start | bytes 589824 | tf_op jit(solution)/shard_map/all_to_all | solution.py:430
  178.8 0.7 copy-start
